TPU v7x, 256 devices: a whole 4x4x8 slice. The times are simulated.
256 devices in a mesh: gr: 2 (over z_hi), sp: 16 (over z_lo, y), tp: 8 (over x, core).
Axes of the slice: x: 4, y: 4, z: 8 (z_hi: 2, z_lo: 4; z = z_hi * 4 + z_lo), core: 2. Of those that a mesh axis runs over, the one named last changes fastest.
Arguments:
- tokens: bfloat16 [8, 3072, 4096], P('gr', 'sp', 'tp'), may hold values from -6.5 to 6.5
- first_token_input: bfloat16 [8, 4096], P('gr', 'sp'), may hold values from -6 to 6
- forget_weight: bfloat16 [4096, 4096], P(None, 'tp'), may hold values from -0.1171875 to 0.1171875
- value_weight: bfloat16 [4096, 4096], P(None, 'tp'), may hold values from -0.375 to 0.375
- query_weight: bfloat16 [4096, 4096], P('sp', 'tp'), may hold values from -0.09375 to 0.09375
- output_gate_weight: bfloat16 [4096, 4096], P('sp', 'tp'), may hold values from -0.09375 to 0.09375
- forget_bound_slack: float32 [4096], P('tp'), may hold values from 0.00016276042 to 0.8, as said below
- additional_damping_exponent: float32 [8, 3072, 32], P('gr', 'sp', 'tp'), may hold values from -2.2 to 0, as said below
- read_norm_scale: float32 [128], replicated, may hold values from 0.1 to 1.9
Outputs:
- cache: bfloat16 [8, 32, 128, 128], P('gr', 'tp', 'sp')
- first_read: bfloat16 [8, 4096], P('gr', 'tp')
Inputs may be any that keep to these rules, and one draw needn't show every extreme that they name: `forget_bound_slack`: positive gaps, one per channel. `additional_damping_exponent`: non-positive log-decays.
All inputs are finite; a program needn't handle non-finite values.
Results may differ from a plain program's by a relative error of at most 0.018.
Values may be sent and summed in bfloat16 or wider, within the bound.
No kernel may reach another device: no remote copies, remote signals or barrier semaphores. Data moves between devices by JAX's collectives and lax.ppermute only.
A program may use at most 64 MiB of HBM per device.

v0:
```python
import jax
import jax.numpy as jnp
from jax import lax
from jax.sharding import PartitionSpec as P


def from_everyone(shard, axis):
    count = lax.axis_size(axis)
    return lax.all_to_all(
        jnp.broadcast_to(shard[None], (count, *shard.shape)), axis, 0, 0, tiled=True
    )


def folded_in_pairs(pieces, combine):
    while len(jax.tree.leaves(pieces)[0]) > 1:
        pieces = jax.vmap(combine)(*(pieces[side::2] for side in (0, 1)))
    return pieces[0]


def prefix(shard, axis, combine, identity):
    count, position = (lax.axis_size(axis), lax.axis_index(axis))
    passed = jnp.arange(count) > position

    def kept(part, zero, own):
        part = jnp.where(
            passed.reshape(-1, *(1 for _ in own.shape)), part, jnp.asarray(zero, own.dtype)
        )
        return part[::-1]

    pieces = from_everyone(shard, axis)
    return folded_in_pairs(kept(pieces, identity, shard), combine)


def cut_along(shard, dim, count):
    shape = shard.shape
    blocks = shard.reshape(*shape[:dim], count, shape[dim] // count, *shape[dim + 1 :])
    return jnp.moveaxis(blocks, dim, 0)


def sent_and_summed(shard, axis, dim):
    count = lax.axis_size(axis)
    blocks = lax.all_to_all(cut_along(shard, dim, count), axis, 0, 0, tiled=True)
    return jnp.sum(blocks.astype(jnp.float32), axis=0)


def of_everyone(shard, axis):
    everything = from_everyone(shard, axis)
    return jnp.sum(everything, axis=0)


def packed_total(arrays, axis):
    ends = [0]
    for a in arrays:
        ends.append(ends[-1] + a.size)
    total = of_everyone(jnp.concatenate([a.ravel() for a in arrays]), axis)
    return tuple((total[b:e].reshape(a.shape) for a, b, e in zip(arrays, ends, ends[1:])))


def add_sums(earlier, later_part):
    return earlier + later_part


def per_device(
    tokens,
    first_token_input,
    forget_weight,
    value_weight,
    query_weight,
    output_gate_weight,
    forget_bound_slack,
    additional_damping_exponent,
    read_norm_scale,
):
    seq_count, block_len, width_part = tokens.shape
    head_dim = read_norm_scale.shape[0]
    local_heads = additional_damping_exponent.shape[2]
    channels = local_heads * head_dim
    flat_rows = tokens.reshape(seq_count * block_len, width_part)
    segment = lax.all_gather(flat_rows, "tp", axis=1, tiled=True)
    forget_acc = jnp.dot(segment, forget_weight, preferred_element_type=jnp.float32)
    value_acc = jnp.dot(segment, value_weight, preferred_element_type=jnp.float32)
    forget = forget_acc.astype(jnp.bfloat16).reshape(seq_count, block_len, channels)
    values = value_acc.astype(jnp.bfloat16).reshape(seq_count, block_len, local_heads, head_dim)
    sp_count = lax.axis_size("sp")
    rows_here = head_dim // sp_count
    row_start = lax.axis_index("sp") * rows_here
    valve_sampler_seeds = forget_bound_slack * jax.nn.sigmoid(-forget.astype(jnp.float32))
    damping_exponent = jnp.log1p(-valve_sampler_seeds) + jnp.repeat(
        additional_damping_exponent, head_dim, axis=2
    )
    totals = jnp.sum(damping_exponent, axis=1)
    later_sum = prefix(totals, "sp", add_sums, jnp.zeros_like(totals))
    within = totals[:, None, :] - jnp.cumsum(damping_exponent, axis=1)
    weighted = (valve_sampler_seeds * jnp.exp(within + later_sum[:, None, :])).astype(jnp.bfloat16)
    weighted = weighted.reshape(seq_count, block_len, local_heads, head_dim)
    state_terms = jnp.einsum(
        "slha,slhb->shab", weighted, values, preferred_element_type=jnp.float32
    )
    state_sum = sent_and_summed(state_terms.astype(jnp.bfloat16), "sp", 2)
    cache_rows = state_sum.astype(jnp.bfloat16)
    slab_rows = first_token_input.shape[1]
    row_first = lax.axis_index("sp") * slab_rows
    forget_rows = lax.dynamic_slice_in_dim(forget_weight, row_first, slab_rows, 0)
    value_rows = lax.dynamic_slice_in_dim(value_weight, row_first, slab_rows, 0)
    new_sums = packed_total(
        (
            jnp.dot(first_token_input, query_weight, preferred_element_type=jnp.float32),
            jnp.dot(first_token_input, output_gate_weight, preferred_element_type=jnp.float32),
            jnp.dot(first_token_input, forget_rows, preferred_element_type=jnp.float32),
            jnp.dot(first_token_input, value_rows, preferred_element_type=jnp.float32),
        ),
        "sp",
    )
    new_query, new_gate, new_forget, new_value = [
        summed.astype(jnp.bfloat16) for summed in new_sums
    ]
    new_keys = (forget_bound_slack * jax.nn.sigmoid(-new_forget.astype(jnp.float32))).reshape(
        seq_count, local_heads, head_dim
    )
    own_keys = lax.dynamic_slice_in_dim(new_keys, row_start, rows_here, 2)
    own_query = lax.dynamic_slice_in_dim(
        new_query.astype(jnp.float32).reshape(seq_count, local_heads, head_dim),
        row_start,
        rows_here,
        2,
    )
    value_new = new_value.astype(jnp.float32).reshape(seq_count, local_heads, head_dim)
    updated = (1.0 - own_keys)[..., None] * cache_rows.astype(jnp.float32) + own_keys[
        ..., None
    ] * value_new[:, :, None, :]
    read_part = jnp.einsum("sha,shab->shb", own_query, updated, precision=lax.Precision.HIGHEST)
    read_sum = of_everyone(read_part, "sp")
    scaled = (
        read_sum
        * lax.rsqrt(jnp.mean(read_sum * read_sum, axis=-1, keepdims=True) + 1e-06)
        * read_norm_scale
    )
    first_read = (
        scaled.reshape(seq_count, channels) * jax.nn.silu(new_gate.astype(jnp.float32))
    ).astype(jnp.bfloat16)
    return (cache_rows, first_read)


def solution(mesh):
    placed = (
        P("gr", "sp", "tp"),
        P("gr", "sp"),
        P(None, "tp"),
        P(None, "tp"),
        P("sp", "tp"),
        P("sp", "tp"),
        P("tp"),
        P("gr", "sp", "tp"),
        P(),
    )
    return jax.shard_map(
        per_device,
        mesh=mesh,
        in_specs=placed,
        out_specs=(P("gr", "tp", "sp", None), P("gr", "tp")),
        check_vma=False,
    )
```

profile of v0, /device:TPU:2, one launch (start us, length us, event | category | flops | bytes accessed | tf_op | source)
XLA Modules:
  0.0 156.7 jit_solution(15677566617659732985)
XLA Ops:
  8.9 1.1 convolution_bitcast_fusion.2
  10.1 1.1 convolution_bitcast_fusion.1
  11.2 1.1 convolution_bitcast_fusion
  12.5 1.0 broadcast_in_dim.20
  13.5 1.8 %reshape.149 = f32[4,192,512]{2,1,0:T(8,128)} reshape(f32[4,192,4,128]{3,2,1,0:T(4,128)S(1)} %broadcast_in_dim.20) | data formatting | bytes 3145728 | tf_op jit(solution)/shard_map/reshape | solution.py:88
  15.3 40.1 %all-gather.2.cloned.1.call-done = bf16[768,4096]{1,0:T(8,128)(2,1)} async-done(((bf16[768,512]{1,0:T(8,128)(2,1)}), bf16[768,4096]{1,0:T(8,128)(2,1)}) %all-gather.2.cloned.1.call-update) | async-done | bytes 6291472 | tf_op jit(solution)/shard_map/all_gather | solution.py:79
  55.3 7.4 %convolution_convert_fusion = bf16[768,512]{1,0:T(8,128)(2,1)S(1)} fusion(bf16[768,4096]{1,0:T(8,128)(2,1)} %all-gather.2.cloned.1.call-done, bf16[4096,512]{1,0:T(8,128)(2,1)} %param.12), kind=kOutput, calls=%fused_computation.10 | convolution fusion | flops 3221618688 | bytes 11272192 | tf_op jit(solution)/shard_map/dot_general | solution.py:81
  62.7 1.1 reshape.153
  63.9 7.0 %add_divide_fusion = f32[768,512]{1,0:T(8,128)S(1)} fusion(bf16[768,4096]{1,0:T(8,128)(2,1)} %all-gather.2.cloned.1.call-done, bf16[4096,512]{1,0:T(8,128)(2,1)} %param.11), kind=kOutput, calls=%fused_computation.9 | convolution fusion | flops 3222798336 | bytes 12058624 | tf_op jit(solution)/shard_map/dot_general | solution.py:80
  71.5 2.4 %add_reduce_fusion = f32[4,4,128]{2,1,0:T(4,128)S(1)} fusion(f32[4,192,4,128]{3,2,1,0:T(4,128)S(1)} %div.22, f32[4,192,4]{2,1,0:T(8,128)} %copy-done.2, f32[4,128]{1,0:T(4,128)S(1)} %bitcast.77), kind=kLoop, calls=%fused_computation.8 | loop fusion | flops 1570816 | bytes 1595392 | tf_op jit(solution)/shard_map/reduce_sum | solution.py:91
  74.6 7.4 %all-to-all-start = ((f32[16,4,512]{2,1,0:T(4,128)}), f32[16,4,512]{2,1,0:T(4,128)S(1)}, u32[]{:S(2)}, u32[]{:S(2)}) async-start(f32[16,4,512]{2,1,0:T(4,128)} %broadcast_in_dim.22), calls=%async_computation | async-start | bytes 262144 | tf_op jit(solution)/shard_map/all_to_all | solution.py:9
  82.0 2.0 %add_bitcast_fusion = f32[4,512,192]{1,2,0:T(8,128)S(1)} fusion(f32[4,192,512]{2,1,0:T(8,128)} %reshape.149, f32[4,192,512]{2,1,0:T(8,128)S(1)} %bitcast.70, f32[512]{0:T(512)S(1)} %copy-done.5), kind=kLoop, calls=%fused_computation.7 | loop fusion | flops 1179648 | bytes 4720640 | tf_op jit(solution)/shard_map/transpose
  84.3 1.6 %fusion = f32[4,512,2,128]{1,2,3,0:T(2,128)S(1)} fusion(f32[4,512,2,128]{1,3,2,0:T(8,128)S(1)} %bitcast.72), kind=kOutput, calls=%fused_computation | output fusion | flops 66584576 | bytes 4194304 | tf_op jit(solution)/shard_map/reduce-window
  85.9 1.3 copy-done.1
  87.3 2.3 %broadcast_add_fusion = f32[4,512,2,128]{1,2,3,0:T(2,128)S(1)} fusion(f32[4,512,2,128]{1,2,3,0:T(2,128)} %copy-done.1, f32[4,512,2]{1,2,0:T(2,128)S(1)} %slice.107), kind=kLoop, calls=%fused_computation.18 | loop fusion | flops 524288 | bytes 4210688 | tf_op jit(solution)/shard_map/reduce_window_sum
  89.7 1.7 %copy.32 = f32[4,512,2,128]{1,3,2,0:T(8,128)} copy(f32[4,512,2,128]{1,2,3,0:T(2,128)S(1)} %broadcast_add_fusion) | data formatting | bytes 4194304 | tf_op jit(solution)/shard_map/reduce_window_sum
  91.4 1.2 broadcast_in_dim.24
  92.6 7.5 %all-to-all-start.2 = ((f32[16,1,8192]{2,1,0:T(1,128)}), f32[16,1,8192]{2,1,0:T(1,128)S(1)}, u32[]{:S(2)}, u32[]{:S(2)}) async-start(f32[16,1,8192]{2,1,0:T(1,128)} %broadcast_in_dim.24), calls=%async_computation.2 | async-start | bytes 1048576 | tf_op jit(solution)/shard_map/all_to_all | solution.py:9
  100.3 2.1 %fusion.6 = bf16[4,4,16,8,128]{4,3,2,1,0:T(8,128)(2,1)S(1)} fusion(bf16[4,192,4,128]{3,2,1,0:T(4,128)(2,1)S(1)} %copy-done.3, f32[4,256,512]{2,1,0:T(8,128)} %bitcast.73, f32[4,192,512]{2,1,0:T(8,128)S(1)} %bitcast.71, f32[4,512]{1,0:T(4,128)S(1)} %fusion.22, f32[4,512]{1,0:T(4,128)S(1)} %bitcast.76, f32[512]{0:T(512)S(1)} %copy-done.5), kind=kOutput, calls=%fused_computation.13 | convolution fusion | flops 102891520 | bytes 4474880 | tf_op jit(solution)/shard_map/slha,slhb->shab/dot_general | solution.py:96
  103.3 12.0 %all-to-all-done.2 = f32[16,1,8192]{2,1,0:T(1,128)S(1)} async-done(((f32[16,1,8192]{2,1,0:T(1,128)}), f32[16,1,8192]{2,1,0:T(1,128)S(1)}, u32[]{:S(2)}, u32[]{:S(2)}) %all-to-all-start.2) | async-done | bytes 524320 | tf_op jit(solution)/shard_map/all_to_all | solution.py:9
  115.3 4.6 %all-to-all-start.1 = ((bf16[16,4,4,8,128]{4,3,2,1,0:T(8,128)(2,1)}), bf16[16,4,4,8,128]{4,3,2,1,0:T(8,128)(2,1)S(1)}, u32[]{:S(2)}, u32[]{:S(2)}) async-start(bf16[16,4,4,8,128]{4,3,2,1,0:T(8,128)(2,1)} %bitcast.68), calls=%async_computation.1 | async-start | bytes 1048576 | tf_op jit(solution)/shard_map/all_to_all | solution.py:42
  120.6 14.1 %all-to-all-done.1 = bf16[16,4,4,8,128]{4,3,2,1,0:T(8,128)(2,1)S(1)} async-done(((bf16[16,4,4,8,128]{4,3,2,1,0:T(8,128)(2,1)}), bf16[16,4,4,8,128]{4,3,2,1,0:T(8,128)(2,1)S(1)}, u32[]{:S(2)}, u32[]{:S(2)}) %all-to-all-start.1) | async-done | bytes 524320 | tf_op jit(solution)/shard_map/all_to_all | solution.py:42
  135.7 4.4 %all-to-all-start.3 = ((f32[16,4,4,128]{3,2,1,0:T(4,128)}), f32[16,4,4,128]{3,2,1,0:T(4,128)S(1)}, u32[]{:S(2)}, u32[]{:S(2)}) async-start(f32[16,4,4,128]{3,2,1,0:T(4,128)} %broadcast_in_dim.25), calls=%async_computation.3 | async-start | bytes 262144 | tf_op jit(solution)/shard_map/all_to_all | solution.py:9
  140.2 8.9 %all-to-all-done.3 = f32[16,4,4,128]{3,2,1,0:T(4,128)S(1)} async-done(((f32[16,4,4,128]{3,2,1,0:T(4,128)}), f32[16,4,4,128]{3,2,1,0:T(4,128)S(1)}, u32[]{:S(2)}, u32[]{:S(2)}) %all-to-all-start.3) | async-done | bytes 131104 | tf_op jit(solution)/shard_map/all_to_all | solution.py:9
  (61 shorter events, 7.2 us)
Async XLA Ops:
  7.2 1.0 copy-start
  7.2 4.0 %copy-start.4 = (bf16[4,256]{1,0:T(4,128)(2,1)S(1)}, bf16[4,256]{1,0:T(4,128)(2,1)}, u32[]{:S(2)}) copy-start(bf16[4,256]{1,0:T(4,128)(2,1)} %param.10) | copy-start | bytes 6148
  7.2 5.1 %copy-start.7 = (f32[4,192,4]{1,2,0:T(4,128)S(1)}, f32[4,192,4]{1,2,0:T(4,128)}, u32[]{:S(2)}) copy-start(f32[4,192,4]{1,2,0:T(4,128)} %param.16) | copy-start | bytes 36868
  7.2 48.1 %all-gather.2.cloned.1.call-start = ((), (), s32[]{:S(2)}) async-start(), calls=%async_computation.4 | async-start | bytes 7077888 | tf_op jit(solution)/shard_map/all_gather | solution.py:79
  12.5 2.8 %copy-start.2 = (f32[4,192,4]{2,1,0:T(8,128)}, f32[4,192,4]{2,1,0:T(8,128)S(1)}, u32[]{:S(2)}) copy-start(f32[4,192,4]{2,1,0:T(8,128)S(1)} %copy.30) | copy-start | bytes 36868
  70.8 0.7 copy-start.5
  74.6 16.8 %all-to-all-start = ((f32[16,4,512]{2,1,0:T(4,128)}), f32[16,4,512]{2,1,0:T(4,128)S(1)}, u32[]{:S(2)}, u32[]{:S(2)}) async-start(f32[16,4,512]{2,1,0:T(4,128)} %broadcast_in_dim.22), calls=%async_computation | async-start | bytes 262144 | tf_op jit(solution)/shard_map/all_to_all | solution.py:9
  85.9 1.3 copy-start.1
  91.4 8.9 %copy-start.3 = (bf16[4,192,4,128]{3,2,1,0:T(4,128)(2,1)S(1)}, bf16[4,192,4,128]{3,2,1,0:T(4,128)(2,1)}, u32[]{:S(2)}) copy-start(bf16[4,192,4,128]{3,2,1,0:T(4,128)(2,1)} %reshape.153) | copy-start | bytes 2359300
  92.6 22.8 %all-to-all-start.2 = ((f32[16,1,8192]{2,1,0:T(1,128)}), f32[16,1,8192]{2,1,0:T(1,128)S(1)}, u32[]{:S(2)}, u32[]{:S(2)}) async-start(f32[16,1,8192]{2,1,0:T(1,128)} %broadcast_in_dim.24), calls=%async_computation.2 | async-start | bytes 1048576 | tf_op jit(solution)/shard_map/all_to_all | solution.py:9
  115.3 24.8 %copy-start.8 = (f32[128]{0:T(128)S(1)}, f32[128]{0:T(128)}, u32[]{:S(2)}) copy-start(f32[128]{0:T(128)} %param.17) | copy-start | bytes 1540
  115.3 19.3 %all-to-all-start.1 = ((bf16[16,4,4,8,128]{4,3,2,1,0:T(8,128)(2,1)}), bf16[16,4,4,8,128]{4,3,2,1,0:T(8,128)(2,1)S(1)}, u32[]{:S(2)}, u32[]{:S(2)}) async-start(bf16[16,4,4,8,128]{4,3,2,1,0:T(8,128)(2,1)} %bitcast.68), calls=%async_computation.1 | async-start | bytes 1048576 | tf_op jit(solution)/shard_map/all_to_all | solution.py:42
  134.8 15.1 %copy-start.6 = (bf16[4,4,8,128]{3,2,1,0:T(8,128)(2,1)}, bf16[4,4,8,128]{3,2,1,0:T(8,128)(2,1)S(1)}, u32[]{:S(2)}) copy-start(bf16[4,4,8,128]{3,2,1,0:T(8,128)(2,1)S(1)} %reduce_sum.49) | copy-start | bytes 98308
  135.7 13.4 %all-to-all-start.3 = ((f32[16,4,4,128]{3,2,1,0:T(4,128)}), f32[16,4,4,128]{3,2,1,0:T(4,128)S(1)}, u32[]{:S(2)}, u32[]{:S(2)}) async-start(f32[16,4,4,128]{3,2,1,0:T(4,128)} %broadcast_in_dim.25), calls=%async_computation.3 | async-start | bytes 262144 | tf_op jit(solution)/shard_map/all_to_all | solution.py:9
Sparse Core Ops, SparseCore 0:
  9.8 45.4 all-gather.1
where the time goes:
time: 157 us
  waiting for transfers between devices  75.7 us (48%)
  starting transfers between devices  24 us (15%)
  matrix products  20.8 us (13%)
  between operations  14.3 us (9%)
  local copies, waits for them, and re-layouts  11.9 us (8%)
  other arithmetic  10 us (6%)
    all_gather x1, waiting for transfers between devices, per_device(): segment = lax.all_gather(flat_rows, 'tp', axis=1, tiled=True)  40.1 us
    all_to_all x3, waiting for transfers between devices, from_everyone(): lax.all_to_all(jnp.broadcast_to(shard[None], (count, *shard.shape)), axis...  20.9 us
    all_to_all x3, starting transfers between devices, from_everyone(): lax.all_to_all(jnp.broadcast_to(shard[None], (count, *shard.shape)), axis...  19.3 us
    all_to_all x1, waiting for transfers between devices, sent_and_summed(): lax.all_to_all(cut_along(shard, dim, count), axis, 0, 0, tiled=True)  14.1 us
    dot_general x1, matrix products, per_device(): jnp.dot(segment, value_weight, preferred_element_type=jnp.float32)  7.4 us
    dot_general x1, matrix products, per_device(): jnp.dot(segment, forget_weight, preferred_element_type=jnp.float32)  6.97 us
    all_to_all x1, starting transfers between devices, sent_and_summed(): lax.all_to_all(cut_along(shard, dim, count), axis, 0, 0, tiled=True)  4.63 us
    another operation x3, other arithmetic  4.02 us
  transfers between devices with their start and end apart: 5, of which 4 were waited for; matrix products, arithmetic and copies ran while one was open for 12% of the time, Pallas kernels for 0%

commit v1 on v0

v1 whole, which is shorter than its diff:
```python
import functools

import jax
import jax.numpy as jnp
from jax import lax
from jax.experimental import pallas as pl
from jax.experimental.pallas import tpu as pltpu
from jax.sharding import PartitionSpec as P


BF = jnp.bfloat16
F32 = jnp.float32


def three_terms(x):
    high = x.astype(BF)
    rest = x - high.astype(F32)
    middle = rest.astype(BF)
    low = (rest - middle.astype(F32)).astype(BF)
    return high, middle, low


VMEM = pl.BlockSpec(memory_space=pltpu.VMEM)


def in_vmem(kernel, out_shape, *arrays, in_specs=None, scratch=(), flops=0):
    return pl.pallas_call(
        kernel,
        in_specs=in_specs or [VMEM] * len(arrays),
        out_specs=jax.tree.map(lambda _: VMEM, out_shape),
        out_shape=out_shape,
        scratch_shapes=scratch,
        compiler_params=pltpu.CompilerParams(vmem_limit_bytes=12 << 20),
        cost_estimate=pl.CostEstimate(flops=flops, transcendentals=0, bytes_accessed=0),
    )(*arrays)


def copied(pairs, sems):
    copies = [pltpu.make_async_copy(*pair, sems.at[n]) for n, pair in enumerate(pairs)]
    for copy in copies:
        copy.start()
    for copy in copies:
        copy.wait()


def from_hbm(kernel, shapes, *arrays):
    return pl.pallas_call(
        kernel,
        in_specs=[pl.BlockSpec(memory_space=pltpu.HBM)] * len(arrays),
        out_specs=[VMEM] * len(shapes),
        out_shape=[pltpu.VMEM(shape, BF) for shape in shapes],
        scratch_shapes=[pltpu.SemaphoreType.DMA((len(shapes),))],
        compiler_params=pltpu.CompilerParams(vmem_limit_bytes=1 << 20),
    )(*(pltpu.with_memory_space_constraint(a, pltpu.HBM) for a in arrays))


def load_kernel(*refs):
    count = len(refs) // 2
    copied(list(zip(refs[:count], refs[count:-1])), refs[-1])


def load(*arrays):
    return from_hbm(load_kernel, [a.shape for a in arrays], *arrays)


def split_kernel(tokens_ref, *refs):
    seqs = tokens_ref.shape[0] // (len(refs) - 1)
    copied(
        [(tokens_ref.at[pl.ds(n * seqs, seqs)], out) for n, out in enumerate(refs[:-1])], refs[-1]
    )


def split(tokens, count):
    shape = (tokens.shape[0] // count, *tokens.shape[1:])
    return from_hbm(split_kernel, [shape] * count, tokens)


def block_of(tp, by, other):
    count = lax.axis_size("tp")
    return lax.rem((tp ^ 1 if other else tp) + count - 2 * by, count)


def products(pieces, sources, w_ref):
    tp = lax.axis_index("tp")
    total = None
    for piece, source in zip(pieces, sources):
        width = piece.shape[1]
        start = pl.multiple_of(block_of(tp, *source) * width, width)
        part = jnp.dot(piece[...], w_ref[pl.ds(start, width), :], preferred_element_type=F32)
        total = part if total is None else total + part
    return total


def project_kernel(*refs, sources, has_sums):
    count = len(sources)
    pieces, (wf_ref, wv_ref, *refs) = refs[:count], refs[count:]
    for n, w_ref in enumerate((wf_ref, wv_ref)):
        result = products(pieces, sources, w_ref)
        refs[-2 + n][...] = refs[n][...] + result if has_sums else result


def project(pieces, sources, weights, sums=()):
    rows, width = pieces[0].shape
    channels = weights[0].shape[1]
    return in_vmem(
        functools.partial(project_kernel, sources=sources, has_sums=bool(sums)),
        [jax.ShapeDtypeStruct((rows, channels), F32)] * 2,
        *pieces,
        *weights,
        *sums,
        flops=4 * len(pieces) * rows * width * channels,
    )


def state_kernel(*refs, sources, groups, head_dim):
    count = len(sources)
    pieces, refs = refs[: groups * count], refs[groups * count :]
    wf_ref, wv_ref, *refs = refs
    sums, (slack_ref, damp_ref, out_ref, f_acc, v_acc) = refs[: 2 * groups], refs[2 * groups :]
    rows = pieces[0].shape[0]
    for g in range(groups):
        here = pl.ds(g * rows, rows)
        group = pieces[g * count : (g + 1) * count]
        f_acc[here, :] = sums[2 * g][...] + products(group, sources, wf_ref)
        v_acc[here, :] = sums[2 * g + 1][...] + products(group, sources, wv_ref)
    parts = out_ref.shape[0]
    seqs, heads, length = damp_ref.shape
    channels = heads * head_dim
    row = lax.broadcasted_iota(jnp.int32, (length, length), 0)
    column = lax.broadcasted_iota(jnp.int32, (length, length), 1)
    later = jnp.where(column > row, 1.0, 0.0).astype(BF)
    head = lax.broadcasted_iota(jnp.int32, (heads, channels), 0)
    channel = lax.broadcasted_iota(jnp.int32, (heads, channels), 1)
    spread = jnp.where(channel // head_dim == head, 1.0, 0.0).astype(BF)
    over_rows = (((0,), (0,)), ((), ()))
    totals = []
    for s in range(seqs):
        here = pl.ds(s * length, length)
        forget = f_acc[here, :].astype(BF).astype(F32)
        values = v_acc[here, :].astype(BF)
        gate = slack_ref[...] * jax.nn.sigmoid(-forget)
        damping = sum(
            lax.dot_general(t, spread, over_rows, preferred_element_type=F32)
            for t in three_terms(damp_ref[s])
        )
        decay = jnp.log1p(-gate) + damping
        within = sum(jnp.dot(later, t, preferred_element_type=F32) for t in three_terms(decay))
        weighted = (gate * jnp.exp(within)).astype(BF)
        total = within[:1, :] + decay[:1, :]
        for h in range(heads):
            cols = slice(h * head_dim, (h + 1) * head_dim)
            state = lax.dot_general(
                weighted[:, cols], values[:, cols], over_rows, preferred_element_type=F32
            )
            totals.append(total[:, cols])
            out_ref[:, s * heads + h] = state.astype(BF).reshape(parts, head_dim // parts, head_dim)
    pairs = seqs * heads
    terms = [t.astype(F32) for t in three_terms(jnp.concatenate(totals))]
    packed = jnp.concatenate([*terms, jnp.zeros((head_dim - 3 * pairs, head_dim), F32)])
    out_ref[:, pairs] = packed.T.astype(BF).reshape(parts, head_dim // parts, head_dim)


def states(pieces, sources, weights, sums, slack, damp, parts):
    rows, width = pieces[0].shape
    channels = weights[0].shape[1]
    seqs, heads, _ = damp.shape
    head_dim = channels // heads
    groups = len(pieces) // len(sources)
    return in_vmem(
        functools.partial(state_kernel, sources=sources, groups=groups, head_dim=head_dim),
        jax.ShapeDtypeStruct((parts, seqs * heads + 1, head_dim // parts, head_dim), BF),
        *pieces,
        *weights,
        *sums,
        slack,
        damp,
        scratch=[pltpu.VMEM((groups * rows, channels), F32)] * 2,
        flops=12 * len(pieces) * rows * width * channels,
    )


def combine_kernel(got_ref, query_ref, keys_ref, value_ref, cache_ref, read_ref):
    parts, pairs = got_ref.shape[0], got_ref.shape[1] - 1
    rows, head_dim = got_ref.shape[2:]
    after = jnp.zeros((rows, head_dim), F32)
    sums = [jnp.zeros((rows, head_dim), F32)] * pairs
    for src in range(parts - 1, -1, -1):
        scale = jnp.exp(after)
        for j in range(pairs):
            sums[j] = sums[j] + scale[:, j : j + 1] * got_ref[src, j].astype(F32)
        packed = got_ref[src, pairs].astype(F32)
        after = after + (
            packed
            + pltpu.roll(packed, head_dim - pairs, 1)
            + pltpu.roll(packed, head_dim - 2 * pairs, 1)
        )
    reads = []
    for j in range(pairs):
        rounded = sums[j].astype(BF)
        cache_ref[j] = rounded
        keys = keys_ref[:, j : j + 1]
        updated = (1.0 - keys) * rounded.astype(F32) + keys * value_ref[j : j + 1, :]
        reads.append(jnp.sum(query_ref[:, j : j + 1] * updated, axis=0, keepdims=True))
    reads = jnp.concatenate(reads)
    for p in range(parts):
        read_ref[p] = reads


def combine(got, query, keys, value):
    parts, tiles, rows, head_dim = got.shape
    return in_vmem(
        combine_kernel,
        [
            jax.ShapeDtypeStruct((tiles - 1, rows, head_dim), BF),
            jax.ShapeDtypeStruct((parts, tiles - 1, head_dim), F32),
        ],
        got,
        query,
        keys,
        value,
    )


def finish_kernel(got_ref, norm_ref, gate_ref, out_ref):
    heads = out_ref.shape[1] // got_ref.shape[2]
    head_dim = got_ref.shape[2]
    read = got_ref[0]
    for src in range(1, got_ref.shape[0]):
        read = read + got_ref[src]
    scaled = read * lax.rsqrt(jnp.mean(read * read, axis=1, keepdims=True) + 1e-06) * norm_ref[...]
    result = (scaled * gate_ref[...]).astype(BF)
    for s in range(out_ref.shape[0]):
        for h in range(heads):
            j = s * heads + h
            out_ref[s : s + 1, h * head_dim : (h + 1) * head_dim] = result[j : j + 1, :]


def new_token_kernel(x_ref, q_ref, g_ref, f_hbm, v_hbm, out_ref, f_rows, v_rows, sems):
    x = x_ref[...]
    seqs, slab = x.shape
    here = pl.ds(pl.multiple_of(lax.axis_index("sp") * slab, slab), slab)
    copied([(f_hbm.at[here], f_rows), (v_hbm.at[here], v_rows)], sems)
    for n, w in enumerate((q_ref, g_ref, f_rows, v_rows)):
        y = jnp.dot(x, w[...], preferred_element_type=F32)
        for p in range(out_ref.shape[0]):
            out_ref[p, n * seqs : (n + 1) * seqs, :] = y


def prepare_kernel(got_ref, slack_ref, query_ref, keys_ref, value_ref, gate_ref):
    pairs, head_dim = value_ref.shape
    rows = query_ref.shape[0]
    seqs = got_ref.shape[1] // 4
    heads = pairs // seqs
    total = got_ref[0]
    for src in range(1, got_ref.shape[0]):
        total = total + got_ref[src]
    rounded = total.astype(BF).astype(F32)

    def by_head(x):
        return jnp.concatenate(
            [
                x[s : s + 1, h * head_dim : (h + 1) * head_dim]
                for s in range(x.shape[0])
                for h in range(heads)
            ]
        )

    query, gate, forget, value = (rounded[n * seqs : (n + 1) * seqs] for n in range(4))
    keys = slack_ref[...] * jax.nn.sigmoid(-forget)
    value_ref[...] = by_head(value)
    gate_ref[...] = by_head(gate * jax.nn.sigmoid(gate))
    own = lax.axis_index("sp") * rows + lax.broadcasted_iota(jnp.int32, (rows, head_dim), 0)
    chosen = jnp.where(lax.broadcasted_iota(jnp.int32, (rows, head_dim), 1) == own, 1.0, 0.0).astype(BF)

    def own_rows(x):
        return sum(
            lax.dot_general(chosen, t, (((1,), (1,)), ((), ())), preferred_element_type=F32)
            for t in three_terms(x)
        )

    query_ref[...] = own_rows(by_head(query))
    keys_ref[...] = own_rows(by_head(keys))


def per_device(
    tokens,
    first_token_input,
    forget_weight,
    value_weight,
    query_weight,
    output_gate_weight,
    forget_bound_slack,
    additional_damping_exponent,
    read_norm_scale,
):
    seqs, length, width = tokens.shape
    head_dim = read_norm_scale.shape[0]
    heads = additional_damping_exponent.shape[2]
    channels = heads * head_dim
    sp_count = lax.axis_size("sp")
    tp_count = lax.axis_size("tp")
    chips = tp_count // 2
    slack = forget_bound_slack.reshape(1, channels)

    def shifted(x, by):
        pairs = [(2 * c + k, 2 * ((c + by) % chips) + k) for c in range(chips) for k in (0, 1)]
        return lax.ppermute(x, "tp", pairs)

    def sibling(x):
        return lax.ppermute(x, "tp", [(i, i ^ 1) for i in range(tp_count)])

    def exchange(x):
        return lax.all_to_all(x, "sp", 0, 0, tiled=True)

    rows = seqs // 2 * length
    own_a, own_b = (x.reshape(rows, width) for x in split(tokens, 2))
    right_a, left_a = shifted(own_a, 1), shifted(own_a, -1)
    right_b, left_b = shifted(own_b, 1), shifted(own_b, -1)
    other_a, other_b = sibling(own_a), sibling(own_b)

    partial = in_vmem(
        new_token_kernel,
        jax.ShapeDtypeStruct((sp_count, 4 * seqs, channels), F32),
        first_token_input,
        query_weight,
        output_gate_weight,
        pltpu.with_memory_space_constraint(forget_weight, pltpu.HBM),
        pltpu.with_memory_space_constraint(value_weight, pltpu.HBM),
        in_specs=[VMEM] * 3 + [pl.BlockSpec(memory_space=pltpu.HBM)] * 2,
        scratch=[pltpu.VMEM(query_weight.shape, BF)] * 2 + [pltpu.SemaphoreType.DMA((2,))],
    )
    new_sums = exchange(partial)
    row_count = head_dim // sp_count
    pairs = seqs * heads
    query_rows, key_rows, value_new, gate_new = in_vmem(
        prepare_kernel,
        [jax.ShapeDtypeStruct((row_count, pairs), F32)] * 2
        + [jax.ShapeDtypeStruct((pairs, head_dim), F32)] * 2,
        new_sums,
        slack,
    )

    weights = load(forget_weight, value_weight)
    weights = [pltpu.with_memory_space_constraint(w, pltpu.VMEM) for w in weights]

    def projected(pieces, sources, sums=()):
        return project(pieces, sources, weights, sums)

    far_a = shifted(right_a, 1)
    other_right_a, other_left_a = sibling(right_a), sibling(left_a)
    far_b = shifted(left_b, -1)
    other_right_b, other_left_b = sibling(right_b), sibling(left_b)
    other_far_a, other_far_b = sibling(far_a), sibling(far_b)

    here = ((0, False), (0, True))
    near = ((1, False), (-1, False))
    other_near = ((1, True), (-1, True))
    sums_a = projected([own_a, other_a], here)
    sums_b = projected([own_b, other_b], here)
    sums_a = projected([right_a, left_a], near, sums_a)
    sums_a = projected([other_right_a, other_left_a], other_near, sums_a)
    sums_b = projected([right_b, left_b], near, sums_b)
    sums_b = projected([other_right_b, other_left_b], other_near, sums_b)

    out = states(
        [far_a, other_far_a, far_b, other_far_b],
        ((2, False), (2, True)),
        weights,
        [*sums_a, *sums_b],
        slack,
        additional_damping_exponent.transpose(0, 2, 1),
        sp_count,
    )
    got = exchange(out)
    cache, read = combine(got, query_rows, key_rows, value_new)
    got = exchange(read)
    first_read = in_vmem(
        finish_kernel,
        jax.ShapeDtypeStruct((seqs, channels), BF),
        got,
        read_norm_scale.reshape(1, head_dim),
        gate_new,
    )
    return cache.reshape(seqs, heads, row_count, head_dim), first_read


def solution(mesh):
    placed = (
        P("gr", "sp", "tp"),
        P("gr", "sp"),
        P(None, "tp"),
        P(None, "tp"),
        P("sp", "tp"),
        P("sp", "tp"),
        P("tp"),
        P("gr", "sp", "tp"),
        P(),
    )

    return jax.shard_map(
        per_device,
        mesh=mesh,
        in_specs=placed,
        out_specs=(P("gr", "tp", "sp", None), P("gr", "tp")),
        check_vma=False,
    )
```

time: 157 us -> 100 us (0.64)
  waiting for transfers between devices: 75.7 us -> 34.6 us
  Pallas kernels: 0 us -> 24.2 us
  matrix products: 20.8 us -> 0 us
  between operations: 14.3 us -> 0.84 us
  blocking collectives: 0 us -> 13.4 us
  other arithmetic: 10 us -> 0 us
  local copies, waits for them, and re-layouts: 11.9 us -> 2.6 us
    all_gather x1 -> x0, waiting for transfers between devices: 40.1 us -> none  [per_device(): segment = lax.all_gather(flat_rows, 'tp', axis=1, tiled=True)]
    pallas_call x0 -> x13, Pallas kernels: none -> 24.2 us  [the longest x11 19.6 us: in_vmem(): pl.pallas_call(kernel, in_specs=in_specs or [VMEM] * len(arrays), out_spe...]
    dot_general x8 -> x0, matrix products: 20.8 us -> none  [the longest x1 7.4 us: per_device(): jnp.dot(segment, value_weight, preferred_element_type=jnp.float32)]
    all_to_all x4 -> x2, waiting for transfers between devices: 35 us -> 16.2 us  [exchange(): return lax.all_to_all(x, 'sp', 0, 0, tiled=True)]
    ppermute x0 -> x14, waiting for transfers between devices: none -> 18.4 us  [the longest x6 18.4 us: shifted(): return lax.ppermute(x, 'tp', pairs)]
    all_to_all x0 -> x1, blocking collectives: none -> 13.4 us  [exchange(): return lax.all_to_all(x, 'sp', 0, 0, tiled=True)]
    ppermute x0 -> x14, starting transfers between devices: none -> 7.99 us  [the longest x6 6.69 us: shifted(): return lax.ppermute(x, 'tp', pairs)]
    all_to_all x4 -> x2, starting transfers between devices: 23.9 us -> 16.1 us  [exchange(): return lax.all_to_all(x, 'sp', 0, 0, tiled=True)]
  transfers between devices with their start and end apart: 5 -> 16, of which waited for: 4 -> 4; matrix products, arithmetic and copies ran while one was open for 12% -> 0% of each run, Pallas kernels for 0% -> 21%
where the time goes in v1:
time: 100 us; the launch traced here: 99.7 us
  waiting for transfers between devices  34.6 us (35%)
  Pallas kernels  24.2 us (24%)
  starting transfers between devices  24.1 us (24%)
  blocking collectives  13.4 us (13%)
  local copies, waits for them, and re-layouts  2.6 us (3%)
    pallas_call x11, Pallas kernels, in_vmem(): pl.pallas_call(kernel, in_specs=in_specs or [VMEM] * len(arrays), out_spe...  19.6 us
    ppermute x6, waiting for transfers between devices, shifted(): return lax.ppermute(x, 'tp', pairs)  18.4 us
    all_to_all x2, waiting for transfers between devices, exchange(): return lax.all_to_all(x, 'sp', 0, 0, tiled=True)  16.2 us
    all_to_all x2, starting transfers between devices, exchange(): return lax.all_to_all(x, 'sp', 0, 0, tiled=True)  16.1 us
    all_to_all x1, blocking collectives, exchange(): return lax.all_to_all(x, 'sp', 0, 0, tiled=True)  13.4 us
    ppermute x6, starting transfers between devices, shifted(): return lax.ppermute(x, 'tp', pairs)  6.69 us
    pallas_call x2, Pallas kernels, from_hbm(): pl.pallas_call(kernel, in_specs=[pl.BlockSpec(memory_space=pltpu.HBM)] *...  4.61 us
    unnamed x12, local copies, waits for them, and re-layouts  2.6 us
  transfers between devices with their start and end apart: 16, of which 4 were waited for; matrix products, arithmetic and copies ran while one was open for 0% of the time, Pallas kernels for 21%

profile of v1, /device:TPU:2, one launch (start us, length us, event | category | flops | bytes accessed | tf_op | source)
XLA Modules:
  0.0 99.7 jit_solution(10607707428691705776)
XLA Ops:
  0.6 1.1 %shard_map.104 = (bf16[2,192,512]{2,1,0:T(8,128)(2,1)S(1)}, bf16[2,192,512]{2,1,0:T(8,128)(2,1)S(1)}) custom-call(bf16[4,192,512]{2,1,0:T(8,128)(2,1)} %tokens_ref.1), custom_call_target="tpu_custom_call" | custom-call | tf_op jit(solution)/shard_map/pallas_call | solution.py:47
  1.9 2.3 %collective-permute-start.3 = (bf16[384,512]{1,0:T(8,128)(2,1)S(1)}, bf16[384,512]{1,0:T(8,128)(2,1)S(1)}, u32[]{:S(2)}, u32[]{:S(2)}) collective-permute-start(bf16[384,512]{1,0:T(8,128)(2,1)S(1)} %bitcast.11), channel_id=1, source_target_pairs={{0,6},{1,7},{2,0},{3,1},{4,2},{5,3},{6,4},{7,5},{8,14},{9,15},{10,... | collective-permute-start | bytes 1179656 | tf_op jit(solution)/shard_map/ppermute | solution.py:307
  4.2 1.3 %collective-permute-start.10 = (bf16[384,512]{1,0:T(8,128)(2,1)S(1)}, bf16[384,512]{1,0:T(8,128)(2,1)}, u32[]{:S(2)}, u32[]{:S(2)}) collective-permute-start(bf16[384,512]{1,0:T(8,128)(2,1)S(1)} %bitcast.12), channel_id=1, source_target_pairs={{0,2},{1,3},{2,4},{3,5},{4,6},{5,7},{6,0},{7,1},{8,10},{9,11},{10,... | collective-permute-start | bytes 1179656 | tf_op jit(solution)/shard_map/ppermute | solution.py:307
  5.5 0.8 collective-permute-start.7
  6.3 7.6 %collective-permute-done.3.refs_1_ = bf16[384,512]{1,0:T(8,128)(2,1)S(1)} collective-permute-done((bf16[384,512]{1,0:T(8,128)(2,1)S(1)}, bf16[384,512]{1,0:T(8,128)(2,1)S(1)}, u32[]{:S(2)}, u32[]{:S(2)}) %collective-permute-start.3) | collective-permute-done | bytes 393248 | tf_op jit(solution)/shard_map/ppermute | solution.py:307
  13.9 2.2 %collective-permute-done.refs_0_ = bf16[384,512]{1,0:T(8,128)(2,1)S(1)} collective-permute-done((bf16[384,512]{1,0:T(8,128)(2,1)S(1)}, bf16[384,512]{1,0:T(8,128)(2,1)S(1)}, u32[]{:S(2)}, u32[]{:S(2)}) %collective-permute-start) | collective-permute-done | bytes 393248 | tf_op jit(solution)/shard_map/ppermute | solution.py:307
  16.2 8.5 %collective-permute-done.10.refs_0_ = bf16[384,512]{1,0:T(8,128)(2,1)} collective-permute-done((bf16[384,512]{1,0:T(8,128)(2,1)S(1)}, bf16[384,512]{1,0:T(8,128)(2,1)}, u32[]{:S(2)}, u32[]{:S(2)}) %collective-permute-start.10) | collective-permute-done | bytes 393248 | tf_op jit(solution)/shard_map/ppermute | solution.py:307
  24.7 2.3 %collective-permute-start.4 = (bf16[384,512]{1,0:T(8,128)(2,1)S(1)}, bf16[384,512]{1,0:T(8,128)(2,1)}, u32[]{:S(2)}, u32[]{:S(2)}) collective-permute-start(bf16[384,512]{1,0:T(8,128)(2,1)S(1)} %collective-permute-done.3.refs_1_), channel_id=1, source_target_pairs={{0,6},{1,7},{2,0},{3,1},{4,2},{5,3},{6,4},{7,5},{8,14},{9,15},{10,... | collective-permute-start | bytes 1179656 | tf_op jit(solution)/shard_map/ppermute | solution.py:307
  27.0 0.9 copy-done
  27.9 0.9 copy-done.1
  29.6 2.1 %shard_map.113 = f32[16,16,512]{2,1,0:T(8,128)} custom-call(bf16[4,256]{1,0:T(4,128)(2,1)S(1)} %copy-done.2, bf16[256,512]{1,0:T(8,128)(2,1)S(1)} %copy-done, bf16[256,512]{1,0:T(8,128)(2,1)S(1)} %copy-done.1, bf16[4096,512]{1,0:T(8,128)(2,1)} %f_hbm.1, bf16[4096,512]{1,0:T(8,128)(2,1)} %v_hbm.1), custom_call_target="tpu_custom_call" | custom-call | tf_op jit(solution)/shard_map/pallas_call | solution.py:27
  31.7 8.6 %all-to-all-start.1 = ((f32[16,16,512]{2,1,0:T(8,128)}), f32[16,16,512]{2,1,0:T(8,128)S(1)}, u32[]{:S(2)}, u32[]{:S(2)}) async-start(f32[16,16,512]{2,1,0:T(8,128)} %shard_map.113), calls=%async_computation.1 | async-start | bytes 1048576 | tf_op jit(solution)/shard_map/all_to_all | solution.py:313
  41.0 3.5 %shard_map.105 = (bf16[4096,512]{1,0:T(8,128)(2,1)S(1)}, bf16[4096,512]{1,0:T(8,128)(2,1)S(1)}) custom-call(bf16[4096,512]{1,0:T(8,128)(2,1)} %f_hbm.1, bf16[4096,512]{1,0:T(8,128)(2,1)} %v_hbm.1), custom_call_target="tpu_custom_call" | custom-call | tf_op jit(solution)/shard_map/pallas_call | solution.py:47
  45.1 1.0 shard_map.109
  46.1 1.0 shard_map.106
  47.1 2.0 %shard_map.110 = (f32[384,512]{1,0:T(8,128)S(1)}, f32[384,512]{1,0:T(8,128)S(1)}) custom-call(bf16[384,512]{1,0:T(8,128)(2,1)} %collective-permute-done.10.refs_0_, bf16[384,512]{1,0:T(8,128)(2,1)S(1)} %collective-permute-done.3.refs_1_, bf16[4096,512]{1,0:T(8,128)(2,1)S(1)} %get-tuple-element.26.refs_2_.refs_4_, ...), custom_call_target="tpu_custom_call" | custom-call | flops 805306368 | tf_op jit(solution)/shard_map/pallas_call | solution.py:27
  49.0 1.0 shard_map.107
  50.0 2.1 %shard_map.111 = (f32[384,512]{1,0:T(8,128)S(1)}, f32[384,512]{1,0:T(8,128)S(1)}) custom-call(bf16[384,512]{1,0:T(8,128)(2,1)} %collective-permute-done.11.refs_0_, bf16[384,512]{1,0:T(8,128)(2,1)} %collective-permute-done.12.refs_1_, bf16[4096,512]{1,0:T(8,128)(2,1)S(1)} %get-tuple-element.26.refs_2_.refs_4_, ...), custom_call_target="tpu_custom_call" | custom-call | flops 805306368 | tf_op jit(solution)/shard_map/pallas_call | solution.py:27
  52.2 1.0 %shard_map.108 = (f32[384,512]{1,0:T(8,128)S(1)}, f32[384,512]{1,0:T(8,128)S(1)}) custom-call(bf16[384,512]{1,0:T(8,128)(2,1)S(1)} %collective-permute-done.6.refs_0_, bf16[384,512]{1,0:T(8,128)(2,1)S(1)} %collective-permute-done.8.refs_1_, bf16[4096,512]{1,0:T(8,128)(2,1)S(1)} %get-tuple-element.26.refs_2_.refs_4_, ...), custom_call_target="tpu_custom_call" | custom-call | flops 805306368 | tf_op jit(solution)/shard_map/pallas_call | solution.py:27
  53.3 6.7 %shard_map.112 = bf16[16,17,8,128]{3,2,1,0:T(8,128)(2,1)} custom-call(bf16[384,512]{1,0:T(8,128)(2,1)} %collective-permute-done.1.refs_0_, bf16[384,512]{1,0:T(8,128)(2,1)S(1)} %collective-permute-done.2.refs_1_, bf16[384,512]{1,0:T(8,128)(2,1)} %collective-permute-done.4.refs_2_, bf16[384,512]{1,0:T(8,128)(2,1)S(1)} %collective-permute-done.5.refs_3_, ...), custom_call_target="tpu_custom_call" | custom-call | flops 4831838208 | tf_op jit(solution)/shard_map/pallas_call | solution.py:27
  60.0 7.5 %all-to-all-start = ((bf16[16,17,8,128]{3,2,1,0:T(8,128)(2,1)}), bf16[16,17,8,128]{3,2,1,0:T(8,128)(2,1)S(1)}, u32[]{:S(2)}, u32[]{:S(2)}) async-start(bf16[16,17,8,128]{3,2,1,0:T(8,128)(2,1)} %shard_map.112), calls=%async_computation | async-start | bytes 1114112 | tf_op jit(solution)/shard_map/all_to_all | solution.py:313
  67.7 16.2 %all-to-all-done.got_ref = bf16[16,17,8,128]{3,2,1,0:T(8,128)(2,1)S(1)} async-done(((bf16[16,17,8,128]{3,2,1,0:T(8,128)(2,1)}), bf16[16,17,8,128]{3,2,1,0:T(8,128)(2,1)S(1)}, u32[]{:S(2)}, u32[]{:S(2)}) %all-to-all-start) | async-done | bytes 557088 | tf_op jit(solution)/shard_map/all_to_all | solution.py:313
  83.8 1.8 %shard_map.115 = (bf16[16,8,128]{2,1,0:T(8,128)(2,1)}, f32[16,16,128]{2,1,0:T(8,128)S(1)}) custom-call(bf16[16,17,8,128]{3,2,1,0:T(8,128)(2,1)S(1)} %all-to-all-done.got_ref, f32[8,16]{1,0:T(8,128)S(1)} %get-tuple-element.40.query_ref, f32[8,16]{1,0:T(8,128)S(1)} %get-tuple-element.41.keys_ref, f32[16,128]{1,0:T(8,128)S(1)} %get-tuple-element.42.value_ref), custom_call_target="tpu_custom_call" | custom-call | tf_op jit(solution)/shard_map/pallas_call | solution.py:27
  85.6 13.4 %all_to_all.15.got_ref = f32[16,16,128]{2,1,0:T(8,128)S(1)} all-to-all(f32[16,16,128]{2,1,0:T(8,128)S(1)} %get-tuple-element.44), channel_id=1, replica_groups=mesh['gr'=2,'sp'=16,'tp'=8] {'sp'}, dimensions={0} | all-to-all | bytes 262144 | tf_op jit(solution)/shard_map/all_to_all | solution.py:313
  (34 shorter events, 2.9 us)
Async XLA Ops:
  1.8 3.7 %collective-permute-start.13 = (bf16[384,512]{1,0:T(8,128)(2,1)S(1)}, bf16[384,512]{1,0:T(8,128)(2,1)S(1)}, u32[]{:S(2)}, u32[]{:S(2)}) collective-permute-start(bf16[384,512]{1,0:T(8,128)(2,1)S(1)} %bitcast.10), channel_id=1, source_target_pairs={{0,1},{1,0},{2,3},{3,2},{4,5},{5,4},{6,7},{7,6},{8,9},{9,8},{10,11... | collective-permute-start | bytes 1179656 | tf_op jit(solution)/shard_map/ppermute | solution.py:310
  1.9 12.1 %collective-permute-start.3 = (bf16[384,512]{1,0:T(8,128)(2,1)S(1)}, bf16[384,512]{1,0:T(8,128)(2,1)S(1)}, u32[]{:S(2)}, u32[]{:S(2)}) collective-permute-start(bf16[384,512]{1,0:T(8,128)(2,1)S(1)} %bitcast.11), channel_id=1, source_target_pairs={{0,6},{1,7},{2,0},{3,1},{4,2},{5,3},{6,4},{7,5},{8,14},{9,15},{10,... | collective-permute-start | bytes 1179656 | tf_op jit(solution)/shard_map/ppermute | solution.py:307
  4.2 12.0 %collective-permute-start = (bf16[384,512]{1,0:T(8,128)(2,1)S(1)}, bf16[384,512]{1,0:T(8,128)(2,1)S(1)}, u32[]{:S(2)}, u32[]{:S(2)}) collective-permute-start(bf16[384,512]{1,0:T(8,128)(2,1)S(1)} %bitcast.6), channel_id=1, source_target_pairs={{0,2},{1,3},{2,4},{3,5},{4,6},{5,7},{6,0},{7,1},{8,10},{9,11},{10,... | collective-permute-start | bytes 1179656 | tf_op jit(solution)/shard_map/ppermute | solution.py:307
  4.2 20.5 %collective-permute-start.10 = (bf16[384,512]{1,0:T(8,128)(2,1)S(1)}, bf16[384,512]{1,0:T(8,128)(2,1)}, u32[]{:S(2)}, u32[]{:S(2)}) collective-permute-start(bf16[384,512]{1,0:T(8,128)(2,1)S(1)} %bitcast.12), channel_id=1, source_target_pairs={{0,2},{1,3},{2,4},{3,5},{4,6},{5,7},{6,0},{7,1},{8,10},{9,11},{10,... | collective-permute-start | bytes 1179656 | tf_op jit(solution)/shard_map/ppermute | solution.py:307
  5.5 21.5 %collective-permute-start.9 = (bf16[384,512]{1,0:T(8,128)(2,1)S(1)}, bf16[384,512]{1,0:T(8,128)(2,1)S(1)}, u32[]{:S(2)}, u32[]{:S(2)}) collective-permute-start(bf16[384,512]{1,0:T(8,128)(2,1)S(1)} %bitcast.7), channel_id=1, source_target_pairs={{0,1},{1,0},{2,3},{3,2},{4,5},{5,4},{6,7},{7,6},{8,9},{9,8},{10,11... | collective-permute-start | bytes 1179656 | tf_op jit(solution)/shard_map/ppermute | solution.py:310
  5.5 34.9 %collective-permute-start.7 = (bf16[384,512]{1,0:T(8,128)(2,1)S(1)}, bf16[384,512]{1,0:T(8,128)(2,1)S(1)}, u32[]{:S(2)}, u32[]{:S(2)}) collective-permute-start(bf16[384,512]{1,0:T(8,128)(2,1)S(1)} %bitcast.8), channel_id=1, source_target_pairs={{0,6},{1,7},{2,0},{3,1},{4,2},{5,3},{6,4},{7,5},{8,14},{9,15},{10,... | collective-permute-start | bytes 1179656 | tf_op jit(solution)/shard_map/ppermute | solution.py:307
  13.9 26.8 %collective-permute-start.12 = (bf16[384,512]{1,0:T(8,128)(2,1)S(1)}, bf16[384,512]{1,0:T(8,128)(2,1)}, u32[]{:S(2)}, u32[]{:S(2)}) collective-permute-start(bf16[384,512]{1,0:T(8,128)(2,1)S(1)} %collective-permute-done.3.refs_1_), channel_id=1, source_target_pairs={{0,1},{1,0},{2,3},{3,2},{4,5},{5,4},{6,7},{7,6},{8,9},{9,8},{10,11... | collective-permute-start | bytes 1179656 | tf_op jit(solution)/shard_map/ppermute | solution.py:310
  16.2 28.3 %collective-permute-start.1 = (bf16[384,512]{1,0:T(8,128)(2,1)S(1)}, bf16[384,512]{1,0:T(8,128)(2,1)}, u32[]{:S(2)}, u32[]{:S(2)}) collective-permute-start(bf16[384,512]{1,0:T(8,128)(2,1)S(1)} %collective-permute-done.refs_0_), channel_id=1, source_target_pairs={{0,2},{1,3},{2,4},{3,5},{4,6},{5,7},{6,0},{7,1},{8,10},{9,11},{10,... | collective-permute-start | bytes 1179656 | tf_op jit(solution)/shard_map/ppermute | solution.py:307
  24.7 20.1 %collective-permute-start.4 = (bf16[384,512]{1,0:T(8,128)(2,1)S(1)}, bf16[384,512]{1,0:T(8,128)(2,1)}, u32[]{:S(2)}, u32[]{:S(2)}) collective-permute-start(bf16[384,512]{1,0:T(8,128)(2,1)S(1)} %collective-permute-done.3.refs_1_), channel_id=1, source_target_pairs={{0,6},{1,7},{2,0},{3,1},{4,2},{5,3},{6,4},{7,5},{8,14},{9,15},{10,... | collective-permute-start | bytes 1179656 | tf_op jit(solution)/shard_map/ppermute | solution.py:307
  27.0 23.1 %collective-permute-start.11 = (bf16[384,512]{1,0:T(8,128)(2,1)}, bf16[384,512]{1,0:T(8,128)(2,1)}, u32[]{:S(2)}, u32[]{:S(2)}) collective-permute-start(bf16[384,512]{1,0:T(8,128)(2,1)} %collective-permute-done.10.refs_0_), channel_id=1, source_target_pairs={{0,1},{1,0},{2,3},{3,2},{4,5},{5,4},{6,7},{7,6},{8,9},{9,8},{10,11... | collective-permute-start | bytes 1179656 | tf_op jit(solution)/shard_map/ppermute | solution.py:310
  27.0 1.0 copy-start
  27.9 0.9 copy-start.1
  28.9 0.7 copy-start.2
  31.7 28.3 %all-to-all-start.1 = ((f32[16,16,512]{2,1,0:T(8,128)}), f32[16,16,512]{2,1,0:T(8,128)S(1)}, u32[]{:S(2)}, u32[]{:S(2)}) async-start(f32[16,16,512]{2,1,0:T(8,128)} %shard_map.113), calls=%async_computation.1 | async-start | bytes 1048576 | tf_op jit(solution)/shard_map/all_to_all | solution.py:313
  40.4 11.8 %collective-permute-start.6 = (bf16[384,512]{1,0:T(8,128)(2,1)S(1)}, bf16[384,512]{1,0:T(8,128)(2,1)S(1)}, u32[]{:S(2)}, u32[]{:S(2)}) collective-permute-start(bf16[384,512]{1,0:T(8,128)(2,1)S(1)} %collective-permute-done.refs_0_), channel_id=1, source_target_pairs={{0,1},{1,0},{2,3},{3,2},{4,5},{5,4},{6,7},{7,6},{8,9},{9,8},{10,11... | collective-permute-start | bytes 1179656 | tf_op jit(solution)/shard_map/ppermute | solution.py:310
  40.7 11.5 %collective-permute-start.8 = (bf16[384,512]{1,0:T(8,128)(2,1)S(1)}, bf16[384,512]{1,0:T(8,128)(2,1)S(1)}, u32[]{:S(2)}, u32[]{:S(2)}) collective-permute-start(bf16[384,512]{1,0:T(8,128)(2,1)S(1)} %collective-permute-done.7.refs_1_), channel_id=1, source_target_pairs={{0,1},{1,0},{2,3},{3,2},{4,5},{5,4},{6,7},{7,6},{8,9},{9,8},{10,11... | collective-permute-start | bytes 1179656 | tf_op jit(solution)/shard_map/ppermute | solution.py:310
  44.5 8.7 %collective-permute-start.2 = (bf16[384,512]{1,0:T(8,128)(2,1)}, bf16[384,512]{1,0:T(8,128)(2,1)S(1)}, u32[]{:S(2)}, u32[]{:S(2)}) collective-permute-start(bf16[384,512]{1,0:T(8,128)(2,1)} %collective-permute-done.1.refs_0_), channel_id=1, source_target_pairs={{0,1},{1,0},{2,3},{3,2},{4,5},{5,4},{6,7},{7,6},{8,9},{9,8},{10,11... | collective-permute-start | bytes 1179656 | tf_op jit(solution)/shard_map/ppermute | solution.py:310
  44.8 8.4 %collective-permute-start.5 = (bf16[384,512]{1,0:T(8,128)(2,1)}, bf16[384,512]{1,0:T(8,128)(2,1)S(1)}, u32[]{:S(2)}, u32[]{:S(2)}) collective-permute-start(bf16[384,512]{1,0:T(8,128)(2,1)} %collective-permute-done.4.refs_2_), channel_id=1, source_target_pairs={{0,1},{1,0},{2,3},{3,2},{4,5},{5,4},{6,7},{7,6},{8,9},{9,8},{10,11... | collective-permute-start | bytes 1179656 | tf_op jit(solution)/shard_map/ppermute | solution.py:310
  52.2 1.1 %copy-start.3 = (f32[512]{0:T(512)S(1)}, f32[512]{0:T(512)}, u32[]{:S(2)}) copy-start(f32[512]{0:T(512)} %param.15) | copy-start | bytes 6148
  52.2 1.1 %copy-start.5 = (f32[4,192,4]{1,2,0:T(4,128)S(1)}, f32[4,192,4]{1,2,0:T(4,128)}, u32[]{:S(2)}) copy-start(f32[4,192,4]{1,2,0:T(4,128)} %param.16) | copy-start | bytes 36868
  53.2 45.8 %copy-start.4 = (f32[128]{0:T(128)S(1)}, f32[128]{0:T(128)}, u32[]{:S(2)}) copy-start(f32[128]{0:T(128)} %param.17) | copy-start | bytes 1540
  60.0 23.9 %all-to-all-start = ((bf16[16,17,8,128]{3,2,1,0:T(8,128)(2,1)}), bf16[16,17,8,128]{3,2,1,0:T(8,128)(2,1)S(1)}, u32[]{:S(2)}, u32[]{:S(2)}) async-start(bf16[16,17,8,128]{3,2,1,0:T(8,128)(2,1)} %shard_map.112), calls=%async_computation | async-start | bytes 1114112 | tf_op jit(solution)/shard_map/all_to_all | solution.py:313

commit v2 on v1

--- a/solution.py
+++ b/solution.py
@@ -235,13 +235,13 @@
             out_ref[s : s + 1, h * head_dim : (h + 1) * head_dim] = result[j : j + 1, :]
 
 
-def new_token_kernel(x_ref, q_ref, g_ref, f_hbm, v_hbm, out_ref, f_rows, v_rows, sems):
-    x = x_ref[...]
-    seqs, slab = x.shape
+def new_token_kernel(x_ref, q_hbm, g_hbm, f_hbm, v_hbm, out_ref, x_here, rows, sems):
+    seqs, slab = x_ref.shape
     here = pl.ds(pl.multiple_of(lax.axis_index("sp") * slab, slab), slab)
-    copied([(f_hbm.at[here], f_rows), (v_hbm.at[here], v_rows)], sems)
-    for n, w in enumerate((q_ref, g_ref, f_rows, v_rows)):
-        y = jnp.dot(x, w[...], preferred_element_type=F32)
+    sources = (q_hbm, g_hbm, f_hbm.at[here], v_hbm.at[here])
+    copied([(w, rows.at[n]) for n, w in enumerate(sources)] + [(x_ref, x_here)], sems)
+    for n in range(len(sources)):
+        y = jnp.dot(x_here[...], rows[n], preferred_element_type=F32)
         for p in range(out_ref.shape[0]):
             out_ref[p, n * seqs : (n + 1) * seqs, :] = y
 
@@ -321,13 +321,22 @@
     partial = in_vmem(
         new_token_kernel,
         jax.ShapeDtypeStruct((sp_count, 4 * seqs, channels), F32),
-        first_token_input,
-        query_weight,
-        output_gate_weight,
-        pltpu.with_memory_space_constraint(forget_weight, pltpu.HBM),
-        pltpu.with_memory_space_constraint(value_weight, pltpu.HBM),
-        in_specs=[VMEM] * 3 + [pl.BlockSpec(memory_space=pltpu.HBM)] * 2,
-        scratch=[pltpu.VMEM(query_weight.shape, BF)] * 2 + [pltpu.SemaphoreType.DMA((2,))],
+        *(
+            pltpu.with_memory_space_constraint(x, pltpu.HBM)
+            for x in (
+                first_token_input,
+                query_weight,
+                output_gate_weight,
+                forget_weight,
+                value_weight,
+            )
+        ),
+        in_specs=[pl.BlockSpec(memory_space=pltpu.HBM)] * 5,
+        scratch=[
+            pltpu.VMEM(first_token_input.shape, BF),
+            pltpu.VMEM((4, *query_weight.shape), BF),
+            pltpu.SemaphoreType.DMA((5,)),
+        ],
     )
     new_sums = exchange(partial)
     row_count = head_dim // sp_count

time: 100 us -> 97.8 us (0.978)
  local copies, waits for them, and re-layouts: 2.6 us -> 0.02 us
    unnamed x12 -> x6, local copies, waits for them, and re-layouts: 2.6 us -> 0.02 us
where the time goes in v2:
time: 97.8 us; the launch traced here: 97.3 us
  waiting for transfers between devices  34.6 us (35%)
  Pallas kernels  24.4 us (25%)
  starting transfers between devices  24.1 us (25%)
  blocking collectives  13.4 us (14%)
    pallas_call x11, Pallas kernels, in_vmem(): pl.pallas_call(kernel, in_specs=in_specs or [VMEM] * len(arrays), out_spe...  19.7 us
    ppermute x6, waiting for transfers between devices, shifted(): return lax.ppermute(x, 'tp', pairs)  18.4 us
    all_to_all x2, waiting for transfers between devices, exchange(): return lax.all_to_all(x, 'sp', 0, 0, tiled=True)  16.2 us
    all_to_all x2, starting transfers between devices, exchange(): return lax.all_to_all(x, 'sp', 0, 0, tiled=True)  16.2 us
    all_to_all x1, blocking collectives, exchange(): return lax.all_to_all(x, 'sp', 0, 0, tiled=True)  13.4 us
    ppermute x6, starting transfers between devices, shifted(): return lax.ppermute(x, 'tp', pairs)  6.69 us
    pallas_call x2, Pallas kernels, from_hbm(): pl.pallas_call(kernel, in_specs=[pl.BlockSpec(memory_space=pltpu.HBM)] *...  4.61 us
  transfers between devices with their start and end apart: 16, of which 4 were waited for; matrix products, arithmetic and copies ran while one was open for 0% of the time, Pallas kernels for 21%

profile of v2, /device:TPU:2, one launch (start us, length us, event | category | flops | bytes accessed | tf_op | source)
XLA Modules:
  0.0 97.3 jit_solution(5890089026024390728)
XLA Ops:
  0.6 1.1 %shard_map.104 = (bf16[2,192,512]{2,1,0:T(8,128)(2,1)S(1)}, bf16[2,192,512]{2,1,0:T(8,128)(2,1)S(1)}) custom-call(bf16[4,192,512]{2,1,0:T(8,128)(2,1)} %tokens_ref.1), custom_call_target="tpu_custom_call" | custom-call | tf_op jit(solution)/shard_map/pallas_call | solution.py:47
  1.9 2.3 %collective-permute-start.3 = (bf16[384,512]{1,0:T(8,128)(2,1)S(1)}, bf16[384,512]{1,0:T(8,128)(2,1)S(1)}, u32[]{:S(2)}, u32[]{:S(2)}) collective-permute-start(bf16[384,512]{1,0:T(8,128)(2,1)S(1)} %bitcast.11), channel_id=1, source_target_pairs={{0,6},{1,7},{2,0},{3,1},{4,2},{5,3},{6,4},{7,5},{8,14},{9,15},{10,... | collective-permute-start | bytes 1179656 | tf_op jit(solution)/shard_map/ppermute | solution.py:307
  4.2 1.3 %collective-permute-start.10 = (bf16[384,512]{1,0:T(8,128)(2,1)S(1)}, bf16[384,512]{1,0:T(8,128)(2,1)}, u32[]{:S(2)}, u32[]{:S(2)}) collective-permute-start(bf16[384,512]{1,0:T(8,128)(2,1)S(1)} %bitcast.12), channel_id=1, source_target_pairs={{0,2},{1,3},{2,4},{3,5},{4,6},{5,7},{6,0},{7,1},{8,10},{9,11},{10,... | collective-permute-start | bytes 1179656 | tf_op jit(solution)/shard_map/ppermute | solution.py:307
  5.5 0.8 collective-permute-start.7
  6.3 7.6 %collective-permute-done.3.refs_1_ = bf16[384,512]{1,0:T(8,128)(2,1)S(1)} collective-permute-done((bf16[384,512]{1,0:T(8,128)(2,1)S(1)}, bf16[384,512]{1,0:T(8,128)(2,1)S(1)}, u32[]{:S(2)}, u32[]{:S(2)}) %collective-permute-start.3) | collective-permute-done | bytes 393248 | tf_op jit(solution)/shard_map/ppermute | solution.py:307
  13.9 2.2 %collective-permute-done.refs_0_ = bf16[384,512]{1,0:T(8,128)(2,1)S(1)} collective-permute-done((bf16[384,512]{1,0:T(8,128)(2,1)S(1)}, bf16[384,512]{1,0:T(8,128)(2,1)S(1)}, u32[]{:S(2)}, u32[]{:S(2)}) %collective-permute-start) | collective-permute-done | bytes 393248 | tf_op jit(solution)/shard_map/ppermute | solution.py:307
  16.2 8.5 %collective-permute-done.10.refs_0_ = bf16[384,512]{1,0:T(8,128)(2,1)} collective-permute-done((bf16[384,512]{1,0:T(8,128)(2,1)S(1)}, bf16[384,512]{1,0:T(8,128)(2,1)}, u32[]{:S(2)}, u32[]{:S(2)}) %collective-permute-start.10) | collective-permute-done | bytes 393248 | tf_op jit(solution)/shard_map/ppermute | solution.py:307
  24.7 2.3 %collective-permute-start.4 = (bf16[384,512]{1,0:T(8,128)(2,1)S(1)}, bf16[384,512]{1,0:T(8,128)(2,1)}, u32[]{:S(2)}, u32[]{:S(2)}) collective-permute-start(bf16[384,512]{1,0:T(8,128)(2,1)S(1)} %collective-permute-done.3.refs_1_), channel_id=1, source_target_pairs={{0,6},{1,7},{2,0},{3,1},{4,2},{5,3},{6,4},{7,5},{8,14},{9,15},{10,... | collective-permute-start | bytes 1179656 | tf_op jit(solution)/shard_map/ppermute | solution.py:307
  27.0 2.3 %shard_map.113 = f32[16,16,512]{2,1,0:T(8,128)} custom-call(bf16[4,256]{1,0:T(4,128)(2,1)} %x_ref.1, bf16[256,512]{1,0:T(8,128)(2,1)} %q_hbm.1, bf16[256,512]{1,0:T(8,128)(2,1)} %g_hbm.1, bf16[4096,512]{1,0:T(8,128)(2,1)} %f_hbm.1, bf16[4096,512]{1,0:T(8,128)(2,1)} %v_hbm.1), custom_call_target="tpu_custom_call" | custom-call | tf_op jit(solution)/shard_map/pallas_call | solution.py:27
  29.3 8.6 %all-to-all-start.1 = ((f32[16,16,512]{2,1,0:T(8,128)}), f32[16,16,512]{2,1,0:T(8,128)S(1)}, u32[]{:S(2)}, u32[]{:S(2)}) async-start(f32[16,16,512]{2,1,0:T(8,128)} %shard_map.113), calls=%async_computation.1 | async-start | bytes 1048576 | tf_op jit(solution)/shard_map/all_to_all | solution.py:313
  38.0 0.3 collective-permute-start.6
  38.6 3.5 %shard_map.105 = (bf16[4096,512]{1,0:T(8,128)(2,1)S(1)}, bf16[4096,512]{1,0:T(8,128)(2,1)S(1)}) custom-call(bf16[4096,512]{1,0:T(8,128)(2,1)} %f_hbm.1, bf16[4096,512]{1,0:T(8,128)(2,1)} %v_hbm.1), custom_call_target="tpu_custom_call" | custom-call | tf_op jit(solution)/shard_map/pallas_call | solution.py:47
  42.7 1.0 shard_map.109
  43.7 1.0 %shard_map.106 = (f32[384,512]{1,0:T(8,128)S(1)}, f32[384,512]{1,0:T(8,128)S(1)}) custom-call(bf16[384,512]{1,0:T(8,128)(2,1)S(1)} %bitcast.9, bf16[384,512]{1,0:T(8,128)(2,1)S(1)} %collective-permute-done.9.refs_1_, bf16[4096,512]{1,0:T(8,128)(2,1)S(1)} %get-tuple-element.26.refs_2_.refs_4_, bf16[4096,512]{1,0:T(8,128)(2,1)S(1)} %get-tuple-element.27.refs_3_.refs_5_), custom_call_target="tpu_custom_call" | custom-call | flops 805306368 | tf_op jit(solution)/shard_map/pallas_call | solution.py:27
  44.7 2.0 %shard_map.110 = (f32[384,512]{1,0:T(8,128)S(1)}, f32[384,512]{1,0:T(8,128)S(1)}) custom-call(bf16[384,512]{1,0:T(8,128)(2,1)} %collective-permute-done.10.refs_0_, bf16[384,512]{1,0:T(8,128)(2,1)S(1)} %collective-permute-done.3.refs_1_, bf16[4096,512]{1,0:T(8,128)(2,1)S(1)} %get-tuple-element.26.refs_2_.refs_4_, ...), custom_call_target="tpu_custom_call" | custom-call | flops 805306368 | tf_op jit(solution)/shard_map/pallas_call | solution.py:27
  46.6 1.0 %shard_map.107 = (f32[384,512]{1,0:T(8,128)S(1)}, f32[384,512]{1,0:T(8,128)S(1)}) custom-call(bf16[384,512]{1,0:T(8,128)(2,1)S(1)} %collective-permute-done.refs_0_, bf16[384,512]{1,0:T(8,128)(2,1)S(1)} %collective-permute-done.7.refs_1_, bf16[4096,512]{1,0:T(8,128)(2,1)S(1)} %get-tuple-element.26.refs_2_.refs_4_, ...), custom_call_target="tpu_custom_call" | custom-call | flops 805306368 | tf_op jit(solution)/shard_map/pallas_call | solution.py:27
  47.7 2.1 %shard_map.111 = (f32[384,512]{1,0:T(8,128)S(1)}, f32[384,512]{1,0:T(8,128)S(1)}) custom-call(bf16[384,512]{1,0:T(8,128)(2,1)} %collective-permute-done.11.refs_0_, bf16[384,512]{1,0:T(8,128)(2,1)} %collective-permute-done.12.refs_1_, bf16[4096,512]{1,0:T(8,128)(2,1)S(1)} %get-tuple-element.26.refs_2_.refs_4_, ...), custom_call_target="tpu_custom_call" | custom-call | flops 805306368 | tf_op jit(solution)/shard_map/pallas_call | solution.py:27
  49.8 1.0 %shard_map.108 = (f32[384,512]{1,0:T(8,128)S(1)}, f32[384,512]{1,0:T(8,128)S(1)}) custom-call(bf16[384,512]{1,0:T(8,128)(2,1)S(1)} %collective-permute-done.6.refs_0_, bf16[384,512]{1,0:T(8,128)(2,1)S(1)} %collective-permute-done.8.refs_1_, bf16[4096,512]{1,0:T(8,128)(2,1)S(1)} %get-tuple-element.26.refs_2_.refs_4_, ...), custom_call_target="tpu_custom_call" | custom-call | flops 805306368 | tf_op jit(solution)/shard_map/pallas_call | solution.py:27
  50.9 6.7 %shard_map.112 = bf16[16,17,8,128]{3,2,1,0:T(8,128)(2,1)} custom-call(bf16[384,512]{1,0:T(8,128)(2,1)} %collective-permute-done.1.refs_0_, bf16[384,512]{1,0:T(8,128)(2,1)S(1)} %collective-permute-done.2.refs_1_, bf16[384,512]{1,0:T(8,128)(2,1)} %collective-permute-done.4.refs_2_, bf16[384,512]{1,0:T(8,128)(2,1)S(1)} %collective-permute-done.5.refs_3_, ...), custom_call_target="tpu_custom_call" | custom-call | flops 4831838208 | tf_op jit(solution)/shard_map/pallas_call | solution.py:27
  57.6 7.5 %all-to-all-start = ((bf16[16,17,8,128]{3,2,1,0:T(8,128)(2,1)}), bf16[16,17,8,128]{3,2,1,0:T(8,128)(2,1)S(1)}, u32[]{:S(2)}, u32[]{:S(2)}) async-start(bf16[16,17,8,128]{3,2,1,0:T(8,128)(2,1)} %shard_map.112), calls=%async_computation | async-start | bytes 1114112 | tf_op jit(solution)/shard_map/all_to_all | solution.py:313
  65.3 16.2 %all-to-all-done.got_ref = bf16[16,17,8,128]{3,2,1,0:T(8,128)(2,1)S(1)} async-done(((bf16[16,17,8,128]{3,2,1,0:T(8,128)(2,1)}), bf16[16,17,8,128]{3,2,1,0:T(8,128)(2,1)S(1)}, u32[]{:S(2)}, u32[]{:S(2)}) %all-to-all-start) | async-done | bytes 557088 | tf_op jit(solution)/shard_map/all_to_all | solution.py:313
  81.5 1.8 %shard_map.115 = (bf16[16,8,128]{2,1,0:T(8,128)(2,1)}, f32[16,16,128]{2,1,0:T(8,128)S(1)}) custom-call(bf16[16,17,8,128]{3,2,1,0:T(8,128)(2,1)S(1)} %all-to-all-done.got_ref, f32[8,16]{1,0:T(8,128)S(1)} %get-tuple-element.40.query_ref, f32[8,16]{1,0:T(8,128)S(1)} %get-tuple-element.41.keys_ref, f32[16,128]{1,0:T(8,128)S(1)} %get-tuple-element.42.value_ref), custom_call_target="tpu_custom_call" | custom-call | tf_op jit(solution)/shard_map/pallas_call | solution.py:27
  83.3 13.4 %all_to_all.15.got_ref = f32[16,16,128]{2,1,0:T(8,128)S(1)} all-to-all(f32[16,16,128]{2,1,0:T(8,128)S(1)} %get-tuple-element.44), channel_id=1, replica_groups=mesh['gr'=2,'sp'=16,'tp'=8] {'sp'}, dimensions={0} | all-to-all | bytes 262144 | tf_op jit(solution)/shard_map/all_to_all | solution.py:313
  96.6 0.7 shard_map.116
  (28 shorter events, 1.2 us)
Async XLA Ops:
  1.8 3.7 %collective-permute-start.13 = (bf16[384,512]{1,0:T(8,128)(2,1)S(1)}, bf16[384,512]{1,0:T(8,128)(2,1)S(1)}, u32[]{:S(2)}, u32[]{:S(2)}) collective-permute-start(bf16[384,512]{1,0:T(8,128)(2,1)S(1)} %bitcast.10), channel_id=1, source_target_pairs={{0,1},{1,0},{2,3},{3,2},{4,5},{5,4},{6,7},{7,6},{8,9},{9,8},{10,11... | collective-permute-start | bytes 1179656 | tf_op jit(solution)/shard_map/ppermute | solution.py:310
  1.9 12.1 %collective-permute-start.3 = (bf16[384,512]{1,0:T(8,128)(2,1)S(1)}, bf16[384,512]{1,0:T(8,128)(2,1)S(1)}, u32[]{:S(2)}, u32[]{:S(2)}) collective-permute-start(bf16[384,512]{1,0:T(8,128)(2,1)S(1)} %bitcast.11), channel_id=1, source_target_pairs={{0,6},{1,7},{2,0},{3,1},{4,2},{5,3},{6,4},{7,5},{8,14},{9,15},{10,... | collective-permute-start | bytes 1179656 | tf_op jit(solution)/shard_map/ppermute | solution.py:307
  4.2 12.0 %collective-permute-start = (bf16[384,512]{1,0:T(8,128)(2,1)S(1)}, bf16[384,512]{1,0:T(8,128)(2,1)S(1)}, u32[]{:S(2)}, u32[]{:S(2)}) collective-permute-start(bf16[384,512]{1,0:T(8,128)(2,1)S(1)} %bitcast.6), channel_id=1, source_target_pairs={{0,2},{1,3},{2,4},{3,5},{4,6},{5,7},{6,0},{7,1},{8,10},{9,11},{10,... | collective-permute-start | bytes 1179656 | tf_op jit(solution)/shard_map/ppermute | solution.py:307
  4.2 20.5 %collective-permute-start.10 = (bf16[384,512]{1,0:T(8,128)(2,1)S(1)}, bf16[384,512]{1,0:T(8,128)(2,1)}, u32[]{:S(2)}, u32[]{:S(2)}) collective-permute-start(bf16[384,512]{1,0:T(8,128)(2,1)S(1)} %bitcast.12), channel_id=1, source_target_pairs={{0,2},{1,3},{2,4},{3,5},{4,6},{5,7},{6,0},{7,1},{8,10},{9,11},{10,... | collective-permute-start | bytes 1179656 | tf_op jit(solution)/shard_map/ppermute | solution.py:307
  5.5 21.5 %collective-permute-start.9 = (bf16[384,512]{1,0:T(8,128)(2,1)S(1)}, bf16[384,512]{1,0:T(8,128)(2,1)S(1)}, u32[]{:S(2)}, u32[]{:S(2)}) collective-permute-start(bf16[384,512]{1,0:T(8,128)(2,1)S(1)} %bitcast.7), channel_id=1, source_target_pairs={{0,1},{1,0},{2,3},{3,2},{4,5},{5,4},{6,7},{7,6},{8,9},{9,8},{10,11... | collective-permute-start | bytes 1179656 | tf_op jit(solution)/shard_map/ppermute | solution.py:310
  5.5 32.5 %collective-permute-start.7 = (bf16[384,512]{1,0:T(8,128)(2,1)S(1)}, bf16[384,512]{1,0:T(8,128)(2,1)S(1)}, u32[]{:S(2)}, u32[]{:S(2)}) collective-permute-start(bf16[384,512]{1,0:T(8,128)(2,1)S(1)} %bitcast.8), channel_id=1, source_target_pairs={{0,6},{1,7},{2,0},{3,1},{4,2},{5,3},{6,4},{7,5},{8,14},{9,15},{10,... | collective-permute-start | bytes 1179656 | tf_op jit(solution)/shard_map/ppermute | solution.py:307
  13.9 24.4 %collective-permute-start.12 = (bf16[384,512]{1,0:T(8,128)(2,1)S(1)}, bf16[384,512]{1,0:T(8,128)(2,1)}, u32[]{:S(2)}, u32[]{:S(2)}) collective-permute-start(bf16[384,512]{1,0:T(8,128)(2,1)S(1)} %collective-permute-done.3.refs_1_), channel_id=1, source_target_pairs={{0,1},{1,0},{2,3},{3,2},{4,5},{5,4},{6,7},{7,6},{8,9},{9,8},{10,11... | collective-permute-start | bytes 1179656 | tf_op jit(solution)/shard_map/ppermute | solution.py:310
  16.2 25.9 %collective-permute-start.1 = (bf16[384,512]{1,0:T(8,128)(2,1)S(1)}, bf16[384,512]{1,0:T(8,128)(2,1)}, u32[]{:S(2)}, u32[]{:S(2)}) collective-permute-start(bf16[384,512]{1,0:T(8,128)(2,1)S(1)} %collective-permute-done.refs_0_), channel_id=1, source_target_pairs={{0,2},{1,3},{2,4},{3,5},{4,6},{5,7},{6,0},{7,1},{8,10},{9,11},{10,... | collective-permute-start | bytes 1179656 | tf_op jit(solution)/shard_map/ppermute | solution.py:307
  24.7 17.7 %collective-permute-start.4 = (bf16[384,512]{1,0:T(8,128)(2,1)S(1)}, bf16[384,512]{1,0:T(8,128)(2,1)}, u32[]{:S(2)}, u32[]{:S(2)}) collective-permute-start(bf16[384,512]{1,0:T(8,128)(2,1)S(1)} %collective-permute-done.3.refs_1_), channel_id=1, source_target_pairs={{0,6},{1,7},{2,0},{3,1},{4,2},{5,3},{6,4},{7,5},{8,14},{9,15},{10,... | collective-permute-start | bytes 1179656 | tf_op jit(solution)/shard_map/ppermute | solution.py:307
  27.0 20.7 %collective-permute-start.11 = (bf16[384,512]{1,0:T(8,128)(2,1)}, bf16[384,512]{1,0:T(8,128)(2,1)}, u32[]{:S(2)}, u32[]{:S(2)}) collective-permute-start(bf16[384,512]{1,0:T(8,128)(2,1)} %collective-permute-done.10.refs_0_), channel_id=1, source_target_pairs={{0,1},{1,0},{2,3},{3,2},{4,5},{5,4},{6,7},{7,6},{8,9},{9,8},{10,11... | collective-permute-start | bytes 1179656 | tf_op jit(solution)/shard_map/ppermute | solution.py:310
  29.3 28.3 %all-to-all-start.1 = ((f32[16,16,512]{2,1,0:T(8,128)}), f32[16,16,512]{2,1,0:T(8,128)S(1)}, u32[]{:S(2)}, u32[]{:S(2)}) async-start(f32[16,16,512]{2,1,0:T(8,128)} %shard_map.113), calls=%async_computation.1 | async-start | bytes 1048576 | tf_op jit(solution)/shard_map/all_to_all | solution.py:313
  38.0 11.8 %collective-permute-start.6 = (bf16[384,512]{1,0:T(8,128)(2,1)S(1)}, bf16[384,512]{1,0:T(8,128)(2,1)S(1)}, u32[]{:S(2)}, u32[]{:S(2)}) collective-permute-start(bf16[384,512]{1,0:T(8,128)(2,1)S(1)} %collective-permute-done.refs_0_), channel_id=1, source_target_pairs={{0,1},{1,0},{2,3},{3,2},{4,5},{5,4},{6,7},{7,6},{8,9},{9,8},{10,11... | collective-permute-start | bytes 1179656 | tf_op jit(solution)/shard_map/ppermute | solution.py:310
  38.3 11.5 %collective-permute-start.8 = (bf16[384,512]{1,0:T(8,128)(2,1)S(1)}, bf16[384,512]{1,0:T(8,128)(2,1)S(1)}, u32[]{:S(2)}, u32[]{:S(2)}) collective-permute-start(bf16[384,512]{1,0:T(8,128)(2,1)S(1)} %collective-permute-done.7.refs_1_), channel_id=1, source_target_pairs={{0,1},{1,0},{2,3},{3,2},{4,5},{5,4},{6,7},{7,6},{8,9},{9,8},{10,11... | collective-permute-start | bytes 1179656 | tf_op jit(solution)/shard_map/ppermute | solution.py:310
  42.1 8.7 %collective-permute-start.2 = (bf16[384,512]{1,0:T(8,128)(2,1)}, bf16[384,512]{1,0:T(8,128)(2,1)S(1)}, u32[]{:S(2)}, u32[]{:S(2)}) collective-permute-start(bf16[384,512]{1,0:T(8,128)(2,1)} %collective-permute-done.1.refs_0_), channel_id=1, source_target_pairs={{0,1},{1,0},{2,3},{3,2},{4,5},{5,4},{6,7},{7,6},{8,9},{9,8},{10,11... | collective-permute-start | bytes 1179656 | tf_op jit(solution)/shard_map/ppermute | solution.py:310
  42.4 8.4 %collective-permute-start.5 = (bf16[384,512]{1,0:T(8,128)(2,1)}, bf16[384,512]{1,0:T(8,128)(2,1)S(1)}, u32[]{:S(2)}, u32[]{:S(2)}) collective-permute-start(bf16[384,512]{1,0:T(8,128)(2,1)} %collective-permute-done.4.refs_2_), channel_id=1, source_target_pairs={{0,1},{1,0},{2,3},{3,2},{4,5},{5,4},{6,7},{7,6},{8,9},{9,8},{10,11... | collective-permute-start | bytes 1179656 | tf_op jit(solution)/shard_map/ppermute | solution.py:310
  49.8 1.0 %copy-start = (f32[512]{0:T(512)S(1)}, f32[512]{0:T(512)}, u32[]{:S(2)}) copy-start(f32[512]{0:T(512)} %param.15) | copy-start | bytes 6148
  49.8 1.0 %copy-start.2 = (f32[4,192,4]{1,2,0:T(4,128)S(1)}, f32[4,192,4]{1,2,0:T(4,128)}, u32[]{:S(2)}) copy-start(f32[4,192,4]{1,2,0:T(4,128)} %param.16) | copy-start | bytes 36868
  50.9 45.8 %copy-start.1 = (f32[128]{0:T(128)S(1)}, f32[128]{0:T(128)}, u32[]{:S(2)}) copy-start(f32[128]{0:T(128)} %param.17) | copy-start | bytes 1540
  57.6 23.9 %all-to-all-start = ((bf16[16,17,8,128]{3,2,1,0:T(8,128)(2,1)}), bf16[16,17,8,128]{3,2,1,0:T(8,128)(2,1)S(1)}, u32[]{:S(2)}, u32[]{:S(2)}) async-start(bf16[16,17,8,128]{3,2,1,0:T(8,128)(2,1)} %shard_map.112), calls=%async_computation | async-start | bytes 1114112 | tf_op jit(solution)/shard_map/all_to_all | solution.py:313

commit v3 on v2

--- a/solution.py
+++ b/solution.py
@@ -54,15 +54,6 @@
     )(*(pltpu.with_memory_space_constraint(a, pltpu.HBM) for a in arrays))
 
 
-def load_kernel(*refs):
-    count = len(refs) // 2
-    copied(list(zip(refs[:count], refs[count:-1])), refs[-1])
-
-
-def load(*arrays):
-    return from_hbm(load_kernel, [a.shape for a in arrays], *arrays)
-
-
 def split_kernel(tokens_ref, *refs):
     seqs = tokens_ref.shape[0] // (len(refs) - 1)
     copied(
@@ -91,38 +82,74 @@
     return total
 
 
-def project_kernel(*refs, sources, has_sums):
-    count = len(sources)
-    pieces, (wf_ref, wv_ref, *refs) = refs[:count], refs[count:]
-    for n, w_ref in enumerate((wf_ref, wv_ref)):
-        result = products(pieces, sources, w_ref)
-        refs[-2 + n][...] = refs[n][...] + result if has_sums else result
-
-
-def project(pieces, sources, weights, sums=()):
-    rows, width = pieces[0].shape
-    channels = weights[0].shape[1]
+def add_products(pieces, plan, weights, sums, outs):
+    rows = pieces[0].shape[0]
+    for half, sources in enumerate(plan):
+        here = pl.ds(half * rows, rows)
+        some, pieces = pieces[: len(sources)], pieces[len(sources) :]
+        for n, (w_ref, out) in enumerate(zip(weights, outs)):
+            result = products(some, sources, w_ref)
+            out[here, :] = sums[n][here, :] + result if sums else result
+
+
+def project_kernel(*refs, plan):
+    count = sum(map(len, plan))
+    add_products(refs[:count], plan, refs[count : count + 2], refs[-4:-2], refs[-2:])
+
+
+def project(pieces, plan, weights, sums):
     return in_vmem(
-        functools.partial(project_kernel, sources=sources, has_sums=bool(sums)),
-        [jax.ShapeDtypeStruct((rows, channels), F32)] * 2,
+        functools.partial(project_kernel, plan=plan),
+        [jax.ShapeDtypeStruct(s.shape, F32) for s in sums],
         *pieces,
         *weights,
         *sums,
-        flops=4 * len(pieces) * rows * width * channels,
-    )
-
-
-def state_kernel(*refs, sources, groups, head_dim):
-    count = len(sources)
-    pieces, refs = refs[: groups * count], refs[groups * count :]
-    wf_ref, wv_ref, *refs = refs
-    sums, (slack_ref, damp_ref, out_ref, f_acc, v_acc) = refs[: 2 * groups], refs[2 * groups :]
-    rows = pieces[0].shape[0]
-    for g in range(groups):
-        here = pl.ds(g * rows, rows)
-        group = pieces[g * count : (g + 1) * count]
-        f_acc[here, :] = sums[2 * g][...] + products(group, sources, wf_ref)
-        v_acc[here, :] = sums[2 * g + 1][...] + products(group, sources, wv_ref)
+        flops=4 * len(pieces) * pieces[0].size * weights[0].shape[1],
+    )
+
+
+def load_kernel(*refs, plan):
+    count = sum(map(len, plan))
+    pieces, (wf_hbm, wv_hbm, wf_ref, wv_ref, *outs, sems) = refs[:count], refs[count:]
+    chips = lax.axis_size("tp") // 2
+    depth = wf_ref.shape[0] // chips
+    chip = lax.axis_index("tp") // 2
+    copies = []
+    for step in range(chips):
+        here = pl.ds(pl.multiple_of(lax.rem(chip + step, chips) * depth, depth), depth)
+        for n, (source, target) in enumerate(((wf_hbm, wf_ref), (wv_hbm, wv_ref))):
+            copies.append(
+                pltpu.make_async_copy(source.at[here], target.at[here], sems.at[2 * step + n])
+            )
+    for copy in copies:
+        copy.start()
+    for copy in copies[:2]:
+        copy.wait()
+    add_products(pieces, plan, (wf_ref, wv_ref), (), outs)
+    for copy in copies[2:]:
+        copy.wait()
+
+
+def load_and_project(pieces, plan, weights):
+    rows = len(plan) * pieces[0].shape[0]
+    out = jax.ShapeDtypeStruct((rows, weights[0].shape[1]), F32)
+    *weights, f, v = pl.pallas_call(
+        functools.partial(load_kernel, plan=plan),
+        in_specs=[VMEM] * len(pieces) + [pl.BlockSpec(memory_space=pltpu.HBM)] * 2,
+        out_specs=[VMEM] * 4,
+        out_shape=[pltpu.VMEM(w.shape, BF) for w in weights] + [out] * 2,
+        scratch_shapes=[pltpu.SemaphoreType.DMA((lax.axis_size("tp"),))],
+        compiler_params=pltpu.CompilerParams(vmem_limit_bytes=12 << 20),
+        name="load",
+    )(*pieces, *(pltpu.with_memory_space_constraint(w, pltpu.HBM) for w in weights))
+    return [pltpu.with_memory_space_constraint(w, pltpu.VMEM) for w in weights], [f, v]
+
+
+def state_kernel(*refs, plan, head_dim):
+    count = sum(map(len, plan))
+    pieces, (wf_ref, wv_ref, f_in, v_in, *refs) = refs[:count], refs[count:]
+    slack_ref, damp_ref, out_ref, f_acc, v_acc = refs
+    add_products(pieces, plan, (wf_ref, wv_ref), (f_in, v_in), (f_acc, v_acc))
     parts = out_ref.shape[0]
     seqs, heads, length = damp_ref.shape
     channels = heads * head_dim
@@ -138,12 +165,12 @@
         here = pl.ds(s * length, length)
         forget = f_acc[here, :].astype(BF).astype(F32)
         values = v_acc[here, :].astype(BF)
-        gate = slack_ref[...] * jax.nn.sigmoid(-forget)
+        gate = slack_ref[...] / (1.0 + jnp.exp(forget))
         damping = sum(
             lax.dot_general(t, spread, over_rows, preferred_element_type=F32)
             for t in three_terms(damp_ref[s])
         )
-        decay = jnp.log1p(-gate) + damping
+        decay = jnp.log(1.0 - gate) + damping
         within = sum(jnp.dot(later, t, preferred_element_type=F32) for t in three_terms(decay))
         weighted = (gate * jnp.exp(within)).astype(BF)
         total = within[:1, :] + decay[:1, :]
@@ -160,22 +187,19 @@
     out_ref[:, pairs] = packed.T.astype(BF).reshape(parts, head_dim // parts, head_dim)
 
 
-def states(pieces, sources, weights, sums, slack, damp, parts):
-    rows, width = pieces[0].shape
-    channels = weights[0].shape[1]
+def states(pieces, plan, weights, sums, slack, damp, parts):
     seqs, heads, _ = damp.shape
-    head_dim = channels // heads
-    groups = len(pieces) // len(sources)
+    head_dim = weights[0].shape[1] // heads
     return in_vmem(
-        functools.partial(state_kernel, sources=sources, groups=groups, head_dim=head_dim),
+        functools.partial(state_kernel, plan=plan, head_dim=head_dim),
         jax.ShapeDtypeStruct((parts, seqs * heads + 1, head_dim // parts, head_dim), BF),
         *pieces,
         *weights,
         *sums,
         slack,
         damp,
-        scratch=[pltpu.VMEM((groups * rows, channels), F32)] * 2,
-        flops=12 * len(pieces) * rows * width * channels,
+        scratch=[pltpu.VMEM(s.shape, F32) for s in sums],
+        flops=12 * len(pieces) * pieces[0].size * weights[0].shape[1],
     )
 
 
@@ -349,33 +373,26 @@
         slack,
     )
 
-    weights = load(forget_weight, value_weight)
-    weights = [pltpu.with_memory_space_constraint(w, pltpu.VMEM) for w in weights]
-
-    def projected(pieces, sources, sums=()):
-        return project(pieces, sources, weights, sums)
-
-    far_a = shifted(right_a, 1)
+    far_a, far_b = shifted(right_a, 1), shifted(left_b, -1)
     other_right_a, other_left_a = sibling(right_a), sibling(left_a)
-    far_b = shifted(left_b, -1)
     other_right_b, other_left_b = sibling(right_b), sibling(left_b)
     other_far_a, other_far_b = sibling(far_a), sibling(far_b)
 
-    here = ((0, False), (0, True))
-    near = ((1, False), (-1, False))
-    other_near = ((1, True), (-1, True))
-    sums_a = projected([own_a, other_a], here)
-    sums_b = projected([own_b, other_b], here)
-    sums_a = projected([right_a, left_a], near, sums_a)
-    sums_a = projected([other_right_a, other_left_a], other_near, sums_a)
-    sums_b = projected([right_b, left_b], near, sums_b)
-    sums_b = projected([other_right_b, other_left_b], other_near, sums_b)
-
+    def both(by):
+        return ((by, False), (by, True))
+
+    weights, sums = load_and_project(
+        [own_a, other_a, own_b, other_b], (both(0), both(0)), (forget_weight, value_weight)
+    )
+    pieces = [right_a, other_right_a, left_b, other_left_b]
+    sums = project(pieces, (both(1), both(-1)), weights, sums)
+    pieces = [left_a, other_left_a, right_b, other_right_b]
+    sums = project(pieces, (both(-1), both(1)), weights, sums)
     out = states(
         [far_a, other_far_a, far_b, other_far_b],
-        ((2, False), (2, True)),
+        (both(2), both(2)),
         weights,
-        [*sums_a, *sums_b],
+        sums,
         slack,
         additional_damping_exponent.transpose(0, 2, 1),
         sp_count,

time: 97.8 us -> 94.5 us (0.966)
  waiting for transfers between devices: 34.6 us -> 29.3 us
  starting transfers between devices: 24.1 us -> 26.5 us
  Pallas kernels: 24.4 us -> 22.1 us
  local copies, waits for them, and re-layouts: 0.02 us -> 1.77 us
    ppermute x6, waiting for transfers between devices: 18.4 us -> 13 us  [shifted(): return lax.ppermute(x, 'tp', pairs)]
    pallas_call x0 -> x1, Pallas kernels: none -> 3.52 us  [load_and_project(): pl.pallas_call(functools.partial(load_kernel, plan=plan), in_specs=[VMEM]...]
    pallas_call x2 -> x1, Pallas kernels: 4.61 us -> 1.13 us  [from_hbm(): pl.pallas_call(kernel, in_specs=[pl.BlockSpec(memory_space=pltpu.HBM)] *...]
    pallas_call x11 -> x7, Pallas kernels: 19.7 us -> 17.4 us  [in_vmem(): pl.pallas_call(kernel, in_specs=in_specs or [VMEM] * len(arrays), out_spe...]
    ppermute x6, starting transfers between devices: 6.69 us -> 8.92 us  [shifted(): return lax.ppermute(x, 'tp', pairs)]
    unnamed x6 -> x14, local copies, waits for them, and re-layouts: 0.02 us -> 1.77 us
  transfers between devices with their start and end apart: 16 -> 16, of which waited for: 4 -> 5; matrix products, arithmetic and copies ran while one was open for 0% -> 0% of each run, Pallas kernels for 21% -> 20%
where the time goes in v3:
time: 94.5 us; the launch traced here: 93.8 us
  waiting for transfers between devices  29.3 us (31%)
  starting transfers between devices  26.5 us (28%)
  Pallas kernels  22.1 us (23%)
  blocking collectives  13.4 us (14%)
  local copies, waits for them, and re-layouts  1.77 us (2%)
    pallas_call x7, Pallas kernels, in_vmem(): pl.pallas_call(kernel, in_specs=in_specs or [VMEM] * len(arrays), out_spe...  17.4 us
    all_to_all x2, starting transfers between devices, exchange(): return lax.all_to_all(x, 'sp', 0, 0, tiled=True)  16.3 us
    all_to_all x2, waiting for transfers between devices, exchange(): return lax.all_to_all(x, 'sp', 0, 0, tiled=True)  16.2 us
    all_to_all x1, blocking collectives, exchange(): return lax.all_to_all(x, 'sp', 0, 0, tiled=True)  13.4 us
    ppermute x6, waiting for transfers between devices, shifted(): return lax.ppermute(x, 'tp', pairs)  13 us
    ppermute x6, starting transfers between devices, shifted(): return lax.ppermute(x, 'tp', pairs)  8.92 us
    pallas_call x1, Pallas kernels, load_and_project(): pl.pallas_call(functools.partial(load_kernel, plan=plan), in_specs=[VMEM]...  3.52 us
  transfers between devices with their start and end apart: 16, of which 5 were waited for; matrix products, arithmetic and copies ran while one was open for 0% of the time, Pallas kernels for 20%

profile of v3, /device:TPU:2, one launch (start us, length us, event | category | flops | bytes accessed | tf_op | source)
XLA Modules:
  0.0 93.8 jit_solution(12712661717763419285)
XLA Ops:
  0.6 1.1 %shard_map.104 = (bf16[2,192,512]{2,1,0:T(8,128)(2,1)S(1)}, bf16[2,192,512]{2,1,0:T(8,128)(2,1)S(1)}) custom-call(bf16[4,192,512]{2,1,0:T(8,128)(2,1)} %tokens_ref.1), custom_call_target="tpu_custom_call" | custom-call | tf_op jit(solution)/shard_map/pallas_call | solution.py:47
  1.9 1.6 %collective-permute-start = (bf16[384,512]{1,0:T(8,128)(2,1)S(1)}, bf16[384,512]{1,0:T(8,128)(2,1)S(1)}, u32[]{:S(2)}, u32[]{:S(2)}) collective-permute-start(bf16[384,512]{1,0:T(8,128)(2,1)S(1)} %bitcast.7), channel_id=1, source_target_pairs={{0,2},{1,3},{2,4},{3,5},{4,6},{5,7},{6,0},{7,1},{8,10},{9,11},{10,... | collective-permute-start | bytes 1179656 | tf_op jit(solution)/shard_map/ppermute | solution.py:331
  3.6 1.0 %collective-permute-start.3 = (bf16[384,512]{1,0:T(8,128)(2,1)S(1)}, bf16[384,512]{1,0:T(8,128)(2,1)S(1)}, u32[]{:S(2)}, u32[]{:S(2)}) collective-permute-start(bf16[384,512]{1,0:T(8,128)(2,1)S(1)} %bitcast.11), channel_id=1, source_target_pairs={{0,6},{1,7},{2,0},{3,1},{4,2},{5,3},{6,4},{7,5},{8,14},{9,15},{10,... | collective-permute-start | bytes 1179656 | tf_op jit(solution)/shard_map/ppermute | solution.py:331
  4.6 1.0 %collective-permute-start.10 = (bf16[384,512]{1,0:T(8,128)(2,1)S(1)}, bf16[384,512]{1,0:T(8,128)(2,1)S(1)}, u32[]{:S(2)}, u32[]{:S(2)}) collective-permute-start(bf16[384,512]{1,0:T(8,128)(2,1)S(1)} %bitcast.12), channel_id=1, source_target_pairs={{0,2},{1,3},{2,4},{3,5},{4,6},{5,7},{6,0},{7,1},{8,10},{9,11},{10,... | collective-permute-start | bytes 1179656 | tf_op jit(solution)/shard_map/ppermute | solution.py:331
  5.6 2.0 %collective-permute-start.8 = (bf16[384,512]{1,0:T(8,128)(2,1)S(1)}, bf16[384,512]{1,0:T(8,128)(2,1)S(1)}, u32[]{:S(2)}, u32[]{:S(2)}) collective-permute-start(bf16[384,512]{1,0:T(8,128)(2,1)S(1)} %bitcast.8), channel_id=1, source_target_pairs={{0,6},{1,7},{2,0},{3,1},{4,2},{5,3},{6,4},{7,5},{8,14},{9,15},{10,... | collective-permute-start | bytes 1179656 | tf_op jit(solution)/shard_map/ppermute | solution.py:331
  7.6 6.6 %collective-permute-done.refs_0_ = bf16[384,512]{1,0:T(8,128)(2,1)S(1)} collective-permute-done((bf16[384,512]{1,0:T(8,128)(2,1)S(1)}, bf16[384,512]{1,0:T(8,128)(2,1)S(1)}, u32[]{:S(2)}, u32[]{:S(2)}) %collective-permute-start) | collective-permute-done | bytes 393248 | tf_op jit(solution)/shard_map/ppermute | solution.py:331
  14.2 1.3 %collective-permute-start.1 = (bf16[384,512]{1,0:T(8,128)(2,1)S(1)}, bf16[384,512]{1,0:T(8,128)(2,1)}, u32[]{:S(2)}, u32[]{:S(2)}) collective-permute-start(bf16[384,512]{1,0:T(8,128)(2,1)S(1)} %collective-permute-done.refs_0_), channel_id=1, source_target_pairs={{0,2},{1,3},{2,4},{3,5},{4,6},{5,7},{6,0},{7,1},{8,10},{9,11},{10,... | collective-permute-start | bytes 1179656 | tf_op jit(solution)/shard_map/ppermute | solution.py:331
  15.6 2.0 %collective-permute-start.4 = (bf16[384,512]{1,0:T(8,128)(2,1)S(1)}, bf16[384,512]{1,0:T(8,128)(2,1)}, u32[]{:S(2)}, u32[]{:S(2)}) collective-permute-start(bf16[384,512]{1,0:T(8,128)(2,1)S(1)} %collective-permute-done.3.refs_2_), channel_id=1, source_target_pairs={{0,6},{1,7},{2,0},{3,1},{4,2},{5,3},{6,4},{7,5},{8,14},{9,15},{10,... | collective-permute-start | bytes 1179656 | tf_op jit(solution)/shard_map/ppermute | solution.py:331
  17.6 5.0 %collective-permute-done.10.refs_2_ = bf16[384,512]{1,0:T(8,128)(2,1)S(1)} collective-permute-done((bf16[384,512]{1,0:T(8,128)(2,1)S(1)}, bf16[384,512]{1,0:T(8,128)(2,1)S(1)}, u32[]{:S(2)}, u32[]{:S(2)}) %collective-permute-start.10) | collective-permute-done | bytes 393248 | tf_op jit(solution)/shard_map/ppermute | solution.py:331
  22.6 1.4 %collective-permute-done.8.refs_0_ = bf16[384,512]{1,0:T(8,128)(2,1)S(1)} collective-permute-done((bf16[384,512]{1,0:T(8,128)(2,1)S(1)}, bf16[384,512]{1,0:T(8,128)(2,1)S(1)}, u32[]{:S(2)}, u32[]{:S(2)}) %collective-permute-start.8) | collective-permute-done | bytes 393248 | tf_op jit(solution)/shard_map/ppermute | solution.py:331
  24.0 0.7 copy-done.2
  24.8 0.5 collective-permute-start.9
  25.3 2.3 %shard_map.108 = f32[16,16,512]{2,1,0:T(8,128)} custom-call(bf16[4,256]{1,0:T(4,128)(2,1)} %x_ref.1, bf16[256,512]{1,0:T(8,128)(2,1)} %q_hbm.1, bf16[256,512]{1,0:T(8,128)(2,1)} %g_hbm.1, bf16[4096,512]{1,0:T(8,128)(2,1)} %f_hbm.1, bf16[4096,512]{1,0:T(8,128)(2,1)} %v_hbm.1), custom_call_target="tpu_custom_call" | custom-call | tf_op jit(solution)/shard_map/pallas_call | solution.py:27
  27.6 8.6 %all-to-all-start.1 = ((f32[16,16,512]{2,1,0:T(8,128)}), f32[16,16,512]{2,1,0:T(8,128)S(1)}, u32[]{:S(2)}, u32[]{:S(2)}) async-start(f32[16,16,512]{2,1,0:T(8,128)} %shard_map.108), calls=%async_computation.1 | async-start | bytes 1048576 | tf_op jit(solution)/shard_map/all_to_all | solution.py:337
  36.9 1.0 %copy-done.1 = bf16[384,512]{1,0:T(8,128)(2,1)S(1)} copy-done((bf16[384,512]{1,0:T(8,128)(2,1)S(1)}, bf16[384,512]{1,0:T(8,128)(2,1)}, u32[]{:S(2)}) %copy-start.1) | copy-done | bytes 393240
  37.9 3.5 %load.1 = (bf16[4096,512]{1,0:T(8,128)(2,1)S(1)}, bf16[4096,512]{1,0:T(8,128)(2,1)S(1)}, f32[768,512]{1,0:T(8,128)S(1)}, f32[768,512]{1,0:T(8,128)S(1)}) custom-call(bf16[384,512]{1,0:T(8,128)(2,1)S(1)} %bitcast.9, bf16[384,512]{1,0:T(8,128)(2,1)S(1)} %collective-permute-done.6.refs_1_, bf16[384,512]{1,0:T(8,128)(2,1)S(1)} %bitcast.13, ...), custom_call_target="tpu_custom_call" | custom-call | tf_op jit(solution)/shard_map/load/pallas_call | solution.py:136
  41.4 2.8 %shard_map.105 = (f32[768,512]{1,0:T(8,128)S(1)}, f32[768,512]{1,0:T(8,128)S(1)}) custom-call(bf16[384,512]{1,0:T(8,128)(2,1)S(1)} %collective-permute-done.refs_0_, bf16[384,512]{1,0:T(8,128)(2,1)S(1)} %copy-done.3, bf16[384,512]{1,0:T(8,128)(2,1)S(1)} %collective-permute-done.3.refs_2_, bf16[384,512]{1,0:T(8,128)(2,1)} %collective-permute-done.13.refs_3_, ...), custom_call_target="tpu_custom_call" | custom-call | flops 1610612736 | tf_op jit(solution)/shard_map/pallas_call | solution.py:27
  44.3 2.9 %shard_map.106 = (f32[768,512]{1,0:T(8,128)S(1)}, f32[768,512]{1,0:T(8,128)S(1)}) custom-call(bf16[384,512]{1,0:T(8,128)(2,1)S(1)} %collective-permute-done.8.refs_0_, bf16[384,512]{1,0:T(8,128)(2,1)} %collective-permute-done.9.refs_1_, bf16[384,512]{1,0:T(8,128)(2,1)S(1)} %collective-permute-done.10.refs_2_, ...), custom_call_target="tpu_custom_call" | custom-call | flops 1610612736 | tf_op jit(solution)/shard_map/pallas_call | solution.py:27
  47.2 6.7 %shard_map.107 = bf16[16,17,8,128]{3,2,1,0:T(8,128)(2,1)} custom-call(bf16[384,512]{1,0:T(8,128)(2,1)} %collective-permute-done.1.refs_0_, bf16[384,512]{1,0:T(8,128)(2,1)S(1)} %collective-permute-done.2.refs_1_, bf16[384,512]{1,0:T(8,128)(2,1)} %collective-permute-done.4.refs_2_, bf16[384,512]{1,0:T(8,128)(2,1)S(1)} %collective-permute-done.5.refs_3_, ...), custom_call_target="tpu_custom_call" | custom-call | flops 4831838208 | tf_op jit(solution)/shard_map/pallas_call | solution.py:27
  53.9 7.6 %all-to-all-start = ((bf16[16,17,8,128]{3,2,1,0:T(8,128)(2,1)}), bf16[16,17,8,128]{3,2,1,0:T(8,128)(2,1)S(1)}, u32[]{:S(2)}, u32[]{:S(2)}) async-start(bf16[16,17,8,128]{3,2,1,0:T(8,128)(2,1)} %shard_map.107), calls=%async_computation | async-start | bytes 1114112 | tf_op jit(solution)/shard_map/all_to_all | solution.py:337
  61.8 16.2 %all-to-all-done.got_ref = bf16[16,17,8,128]{3,2,1,0:T(8,128)(2,1)S(1)} async-done(((bf16[16,17,8,128]{3,2,1,0:T(8,128)(2,1)}), bf16[16,17,8,128]{3,2,1,0:T(8,128)(2,1)S(1)}, u32[]{:S(2)}, u32[]{:S(2)}) %all-to-all-start) | async-done | bytes 557088 | tf_op jit(solution)/shard_map/all_to_all | solution.py:337
  77.9 1.8 %shard_map.110 = (bf16[16,8,128]{2,1,0:T(8,128)(2,1)}, f32[16,16,128]{2,1,0:T(8,128)S(1)}) custom-call(bf16[16,17,8,128]{3,2,1,0:T(8,128)(2,1)S(1)} %all-to-all-done.got_ref, f32[8,16]{1,0:T(8,128)S(1)} %get-tuple-element.28.query_ref, f32[8,16]{1,0:T(8,128)S(1)} %get-tuple-element.29.keys_ref, f32[16,128]{1,0:T(8,128)S(1)} %get-tuple-element.30.value_ref), custom_call_target="tpu_custom_call" | custom-call | tf_op jit(solution)/shard_map/pallas_call | solution.py:27
  79.7 13.4 %all_to_all.15.got_ref = f32[16,16,128]{2,1,0:T(8,128)S(1)} all-to-all(f32[16,16,128]{2,1,0:T(8,128)S(1)} %get-tuple-element.32), channel_id=1, replica_groups=mesh['gr'=2,'sp'=16,'tp'=8] {'sp'}, dimensions={0} | all-to-all | bytes 262144 | tf_op jit(solution)/shard_map/all_to_all | solution.py:337
  93.1 0.7 shard_map.111
  (32 shorter events, 1.1 us)
Async XLA Ops:
  1.8 3.8 %collective-permute-start.6 = (bf16[384,512]{1,0:T(8,128)(2,1)S(1)}, bf16[384,512]{1,0:T(8,128)(2,1)S(1)}, u32[]{:S(2)}, u32[]{:S(2)}) collective-permute-start(bf16[384,512]{1,0:T(8,128)(2,1)S(1)} %bitcast.6), channel_id=1, source_target_pairs={{0,1},{1,0},{2,3},{3,2},{4,5},{5,4},{6,7},{7,6},{8,9},{9,8},{10,11... | collective-permute-start | bytes 1179656 | tf_op jit(solution)/shard_map/ppermute | solution.py:334
  1.9 12.3 %collective-permute-start = (bf16[384,512]{1,0:T(8,128)(2,1)S(1)}, bf16[384,512]{1,0:T(8,128)(2,1)S(1)}, u32[]{:S(2)}, u32[]{:S(2)}) collective-permute-start(bf16[384,512]{1,0:T(8,128)(2,1)S(1)} %bitcast.7), channel_id=1, source_target_pairs={{0,2},{1,3},{2,4},{3,5},{4,6},{5,7},{6,0},{7,1},{8,10},{9,11},{10,... | collective-permute-start | bytes 1179656 | tf_op jit(solution)/shard_map/ppermute | solution.py:331
  3.4 10.7 %collective-permute-start.7 = (bf16[384,512]{1,0:T(8,128)(2,1)S(1)}, bf16[384,512]{1,0:T(8,128)(2,1)S(1)}, u32[]{:S(2)}, u32[]{:S(2)}) collective-permute-start(bf16[384,512]{1,0:T(8,128)(2,1)S(1)} %bitcast.10), channel_id=1, source_target_pairs={{0,1},{1,0},{2,3},{3,2},{4,5},{5,4},{6,7},{7,6},{8,9},{9,8},{10,11... | collective-permute-start | bytes 1179656 | tf_op jit(solution)/shard_map/ppermute | solution.py:334
  3.6 12.0 %collective-permute-start.3 = (bf16[384,512]{1,0:T(8,128)(2,1)S(1)}, bf16[384,512]{1,0:T(8,128)(2,1)S(1)}, u32[]{:S(2)}, u32[]{:S(2)}) collective-permute-start(bf16[384,512]{1,0:T(8,128)(2,1)S(1)} %bitcast.11), channel_id=1, source_target_pairs={{0,6},{1,7},{2,0},{3,1},{4,2},{5,3},{6,4},{7,5},{8,14},{9,15},{10,... | collective-permute-start | bytes 1179656 | tf_op jit(solution)/shard_map/ppermute | solution.py:331
  4.6 18.0 %collective-permute-start.10 = (bf16[384,512]{1,0:T(8,128)(2,1)S(1)}, bf16[384,512]{1,0:T(8,128)(2,1)S(1)}, u32[]{:S(2)}, u32[]{:S(2)}) collective-permute-start(bf16[384,512]{1,0:T(8,128)(2,1)S(1)} %bitcast.12), channel_id=1, source_target_pairs={{0,2},{1,3},{2,4},{3,5},{4,6},{5,7},{6,0},{7,1},{8,10},{9,11},{10,... | collective-permute-start | bytes 1179656 | tf_op jit(solution)/shard_map/ppermute | solution.py:331
  5.6 18.4 %collective-permute-start.8 = (bf16[384,512]{1,0:T(8,128)(2,1)S(1)}, bf16[384,512]{1,0:T(8,128)(2,1)S(1)}, u32[]{:S(2)}, u32[]{:S(2)}) collective-permute-start(bf16[384,512]{1,0:T(8,128)(2,1)S(1)} %bitcast.8), channel_id=1, source_target_pairs={{0,6},{1,7},{2,0},{3,1},{4,2},{5,3},{6,4},{7,5},{8,14},{9,15},{10,... | collective-permute-start | bytes 1179656 | tf_op jit(solution)/shard_map/ppermute | solution.py:331
  14.2 9.8 %collective-permute-start.12 = (bf16[384,512]{1,0:T(8,128)(2,1)S(1)}, bf16[384,512]{1,0:T(8,128)(2,1)S(1)}, u32[]{:S(2)}, u32[]{:S(2)}) collective-permute-start(bf16[384,512]{1,0:T(8,128)(2,1)S(1)} %collective-permute-done.refs_0_), channel_id=1, source_target_pairs={{0,1},{1,0},{2,3},{3,2},{4,5},{5,4},{6,7},{7,6},{8,9},{9,8},{10,11... | collective-permute-start | bytes 1179656 | tf_op jit(solution)/shard_map/ppermute | solution.py:334
  14.2 13.4 %copy-start = (bf16[384,512]{1,0:T(8,128)(2,1)}, bf16[384,512]{1,0:T(8,128)(2,1)S(1)}, u32[]{:S(2)}) copy-start(bf16[384,512]{1,0:T(8,128)(2,1)S(1)} %collective-permute-done.7.refs_3_) | copy-start | bytes 1179652
  14.2 22.1 %collective-permute-start.1 = (bf16[384,512]{1,0:T(8,128)(2,1)S(1)}, bf16[384,512]{1,0:T(8,128)(2,1)}, u32[]{:S(2)}, u32[]{:S(2)}) collective-permute-start(bf16[384,512]{1,0:T(8,128)(2,1)S(1)} %collective-permute-done.refs_0_), channel_id=1, source_target_pairs={{0,2},{1,3},{2,4},{3,5},{4,6},{5,7},{6,0},{7,1},{8,10},{9,11},{10,... | collective-permute-start | bytes 1179656 | tf_op jit(solution)/shard_map/ppermute | solution.py:331
  15.6 20.8 %collective-permute-start.4 = (bf16[384,512]{1,0:T(8,128)(2,1)S(1)}, bf16[384,512]{1,0:T(8,128)(2,1)}, u32[]{:S(2)}, u32[]{:S(2)}) collective-permute-start(bf16[384,512]{1,0:T(8,128)(2,1)S(1)} %collective-permute-done.3.refs_2_), channel_id=1, source_target_pairs={{0,6},{1,7},{2,0},{3,1},{4,2},{5,3},{6,4},{7,5},{8,14},{9,15},{10,... | collective-permute-start | bytes 1179656 | tf_op jit(solution)/shard_map/ppermute | solution.py:331
  22.6 18.8 %collective-permute-start.13 = (bf16[384,512]{1,0:T(8,128)(2,1)S(1)}, bf16[384,512]{1,0:T(8,128)(2,1)}, u32[]{:S(2)}, u32[]{:S(2)}) collective-permute-start(bf16[384,512]{1,0:T(8,128)(2,1)S(1)} %collective-permute-done.3.refs_2_), channel_id=1, source_target_pairs={{0,1},{1,0},{2,3},{3,2},{4,5},{5,4},{6,7},{7,6},{8,9},{9,8},{10,11... | collective-permute-start | bytes 1179656 | tf_op jit(solution)/shard_map/ppermute | solution.py:334
  24.0 20.2 %collective-permute-start.11 = (bf16[384,512]{1,0:T(8,128)(2,1)S(1)}, bf16[384,512]{1,0:T(8,128)(2,1)}, u32[]{:S(2)}, u32[]{:S(2)}) collective-permute-start(bf16[384,512]{1,0:T(8,128)(2,1)S(1)} %collective-permute-done.10.refs_2_), channel_id=1, source_target_pairs={{0,1},{1,0},{2,3},{3,2},{4,5},{5,4},{6,7},{7,6},{8,9},{9,8},{10,11... | collective-permute-start | bytes 1179656 | tf_op jit(solution)/shard_map/ppermute | solution.py:334
  24.0 0.8 copy-start.2
  24.8 19.5 %collective-permute-start.9 = (bf16[384,512]{1,0:T(8,128)(2,1)S(1)}, bf16[384,512]{1,0:T(8,128)(2,1)}, u32[]{:S(2)}, u32[]{:S(2)}) collective-permute-start(bf16[384,512]{1,0:T(8,128)(2,1)S(1)} %collective-permute-done.8.refs_0_), channel_id=1, source_target_pairs={{0,1},{1,0},{2,3},{3,2},{4,5},{5,4},{6,7},{7,6},{8,9},{9,8},{10,11... | collective-permute-start | bytes 1179656 | tf_op jit(solution)/shard_map/ppermute | solution.py:334
  27.6 26.3 %all-to-all-start.1 = ((f32[16,16,512]{2,1,0:T(8,128)}), f32[16,16,512]{2,1,0:T(8,128)S(1)}, u32[]{:S(2)}, u32[]{:S(2)}) async-start(f32[16,16,512]{2,1,0:T(8,128)} %shard_map.108), calls=%async_computation.1 | async-start | bytes 1048576 | tf_op jit(solution)/shard_map/all_to_all | solution.py:337
  36.3 10.9 %collective-permute-start.2 = (bf16[384,512]{1,0:T(8,128)(2,1)}, bf16[384,512]{1,0:T(8,128)(2,1)S(1)}, u32[]{:S(2)}, u32[]{:S(2)}) collective-permute-start(bf16[384,512]{1,0:T(8,128)(2,1)} %collective-permute-done.1.refs_0_), channel_id=1, source_target_pairs={{0,1},{1,0},{2,3},{3,2},{4,5},{5,4},{6,7},{7,6},{8,9},{9,8},{10,11... | collective-permute-start | bytes 1179656 | tf_op jit(solution)/shard_map/ppermute | solution.py:334
  36.4 10.8 %collective-permute-start.5 = (bf16[384,512]{1,0:T(8,128)(2,1)}, bf16[384,512]{1,0:T(8,128)(2,1)S(1)}, u32[]{:S(2)}, u32[]{:S(2)}) collective-permute-start(bf16[384,512]{1,0:T(8,128)(2,1)} %collective-permute-done.4.refs_2_), channel_id=1, source_target_pairs={{0,1},{1,0},{2,3},{3,2},{4,5},{5,4},{6,7},{7,6},{8,9},{9,8},{10,11... | collective-permute-start | bytes 1179656 | tf_op jit(solution)/shard_map/ppermute | solution.py:334
  36.9 1.0 %copy-start.1 = (bf16[384,512]{1,0:T(8,128)(2,1)S(1)}, bf16[384,512]{1,0:T(8,128)(2,1)}, u32[]{:S(2)}) copy-start(bf16[384,512]{1,0:T(8,128)(2,1)} %copy-done) | copy-start | bytes 1179652
  37.9 3.5 %copy-start.3 = (bf16[384,512]{1,0:T(8,128)(2,1)S(1)}, bf16[384,512]{1,0:T(8,128)(2,1)}, u32[]{:S(2)}) copy-start(bf16[384,512]{1,0:T(8,128)(2,1)} %copy-done.2) | copy-start | bytes 1179652
  44.2 3.0 %copy-start.4 = (f32[512]{0:T(512)S(1)}, f32[512]{0:T(512)}, u32[]{:S(2)}) copy-start(f32[512]{0:T(512)} %param.15) | copy-start | bytes 6148
  44.3 3.0 %copy-start.6 = (f32[4,192,4]{1,2,0:T(4,128)S(1)}, f32[4,192,4]{1,2,0:T(4,128)}, u32[]{:S(2)}) copy-start(f32[4,192,4]{1,2,0:T(4,128)} %param.16) | copy-start | bytes 36868
  53.9 39.2 %copy-start.5 = (f32[128]{0:T(128)S(1)}, f32[128]{0:T(128)}, u32[]{:S(2)}) copy-start(f32[128]{0:T(128)} %param.17) | copy-start | bytes 1540
  53.9 24.0 %all-to-all-start = ((bf16[16,17,8,128]{3,2,1,0:T(8,128)(2,1)}), bf16[16,17,8,128]{3,2,1,0:T(8,128)(2,1)S(1)}, u32[]{:S(2)}, u32[]{:S(2)}) async-start(bf16[16,17,8,128]{3,2,1,0:T(8,128)(2,1)} %shard_map.107), calls=%async_computation | async-start | bytes 1114112 | tf_op jit(solution)/shard_map/all_to_all | solution.py:337

commit v4 on v3

--- a/solution.py
+++ b/solution.py
@@ -153,33 +153,41 @@
     parts = out_ref.shape[0]
     seqs, heads, length = damp_ref.shape
     channels = heads * head_dim
-    row = lax.broadcasted_iota(jnp.int32, (length, length), 0)
-    column = lax.broadcasted_iota(jnp.int32, (length, length), 1)
-    later = jnp.where(column > row, 1.0, 0.0).astype(BF)
-    head = lax.broadcasted_iota(jnp.int32, (heads, channels), 0)
-    channel = lax.broadcasted_iota(jnp.int32, (heads, channels), 1)
+    tall = length + 8
+    row = lax.broadcasted_iota(jnp.int32, (tall, length), 0)
+    column = lax.broadcasted_iota(jnp.int32, (tall, length), 1)
+    later = jnp.where((column > row) | (row >= length), 1.0, 0.0).astype(BF)
+    head = lax.broadcasted_iota(jnp.int32, (3 * heads, channels), 0) % heads
+    channel = lax.broadcasted_iota(jnp.int32, (3 * heads, channels), 1)
     spread = jnp.where(channel // head_dim == head, 1.0, 0.0).astype(BF)
     over_rows = (((0,), (0,)), ((), ()))
+    over_columns = (((1,), (1,)), ((), ()))
     totals = []
     for s in range(seqs):
         here = pl.ds(s * length, length)
         forget = f_acc[here, :].astype(BF).astype(F32)
         values = v_acc[here, :].astype(BF)
         gate = slack_ref[...] / (1.0 + jnp.exp(forget))
-        damping = sum(
-            lax.dot_general(t, spread, over_rows, preferred_element_type=F32)
-            for t in three_terms(damp_ref[s])
+        high, middle, _ = three_terms(jnp.log(1.0 - gate))
+        damping = lax.dot_general(
+            later,
+            jnp.concatenate(three_terms(damp_ref[s])),
+            over_columns,
+            preferred_element_type=F32,
         )
-        decay = jnp.log(1.0 - gate) + damping
-        within = sum(jnp.dot(later, t, preferred_element_type=F32) for t in three_terms(decay))
-        weighted = (gate * jnp.exp(within)).astype(BF)
-        total = within[:1, :] + decay[:1, :]
+        damping = damping[:, :heads] + damping[:, heads : 2 * heads] + damping[:, 2 * heads :]
+        sums = jnp.dot(
+            jnp.concatenate([later, *three_terms(damping)], axis=1),
+            jnp.concatenate([high, spread]),
+            preferred_element_type=F32,
+        ) + jnp.dot(later, middle, preferred_element_type=F32)
+        weighted = (gate * jnp.exp(sums[:length])).astype(BF)
         for h in range(heads):
             cols = slice(h * head_dim, (h + 1) * head_dim)
             state = lax.dot_general(
                 weighted[:, cols], values[:, cols], over_rows, preferred_element_type=F32
             )
-            totals.append(total[:, cols])
+            totals.append(sums[length : length + 1, cols])
             out_ref[:, s * heads + h] = state.astype(BF).reshape(parts, head_dim // parts, head_dim)
     pairs = seqs * heads
     terms = [t.astype(F32) for t in three_terms(jnp.concatenate(totals))]
@@ -235,7 +243,7 @@
     return in_vmem(
         combine_kernel,
         [
-            jax.ShapeDtypeStruct((tiles - 1, rows, head_dim), BF),
+            pltpu.VMEM((tiles - 1, rows, head_dim), BF),
             jax.ShapeDtypeStruct((parts, tiles - 1, head_dim), F32),
         ],
         got,
@@ -384,10 +392,9 @@
     weights, sums = load_and_project(
         [own_a, other_a, own_b, other_b], (both(0), both(0)), (forget_weight, value_weight)
     )
-    pieces = [right_a, other_right_a, left_b, other_left_b]
-    sums = project(pieces, (both(1), both(-1)), weights, sums)
-    pieces = [left_a, other_left_a, right_b, other_right_b]
-    sums = project(pieces, (both(-1), both(1)), weights, sums)
+    pieces = [right_a, other_right_a, left_a, other_left_a]
+    pieces += [right_b, other_right_b, left_b, other_left_b]
+    sums = project(pieces, (both(1) + both(-1), both(1) + both(-1)), weights, sums)
     out = states(
         [far_a, other_far_a, far_b, other_far_b],
         (both(2), both(2)),

time: 94.5 us -> 92.6 us (0.980)
  the two profiles are of different devices: /device:TPU:2 before, /device:TPU:8 now
where the time goes in v4:
time: 92.6 us; the launch traced here: 92.1 us
  waiting for transfers between devices  36.9 us (40%)
  starting transfers between devices  33.2 us (36%)
  Pallas kernels  20.6 us (22%)
    all_to_all x3, starting transfers between devices, exchange(): return lax.all_to_all(x, 'sp', 0, 0, tiled=True)  22.7 us
    all_to_all x3, waiting for transfers between devices, exchange(): return lax.all_to_all(x, 'sp', 0, 0, tiled=True)  21.6 us
    pallas_call x6, Pallas kernels, in_vmem(): pl.pallas_call(kernel, in_specs=in_specs or [VMEM] * len(arrays), out_spe...  16 us
    ppermute x6, waiting for transfers between devices, shifted(): return lax.ppermute(x, 'tp', pairs)  15.2 us
    ppermute x6, starting transfers between devices, shifted(): return lax.ppermute(x, 'tp', pairs)  9.17 us
    pallas_call x1, Pallas kernels, load_and_project(): pl.pallas_call(functools.partial(load_kernel, plan=plan), in_specs=[VMEM]...  3.47 us
  transfers between devices with their start and end apart: 17, of which 6 were waited for; matrix products, arithmetic and copies ran while one was open for 1% of the time, Pallas kernels for 18%

profile of v4, /device:TPU:8, one launch (start us, length us, event | category | flops | bytes accessed | tf_op | source)
XLA Modules:
  0.0 92.1 jit_solution(1109159920249424040)
XLA Ops:
  0.6 1.1 %shard_map.104 = (bf16[2,192,512]{2,1,0:T(8,128)(2,1)S(1)}, bf16[2,192,512]{2,1,0:T(8,128)(2,1)S(1)}) custom-call(bf16[4,192,512]{2,1,0:T(8,128)(2,1)} %tokens_ref.1), custom_call_target="tpu_custom_call" | custom-call | tf_op jit(solution)/shard_map/pallas_call | solution.py:47
  1.9 2.8 %collective-permute-start.3 = (bf16[384,512]{1,0:T(8,128)(2,1)S(1)}, bf16[384,512]{1,0:T(8,128)(2,1)S(1)}, u32[]{:S(2)}, u32[]{:S(2)}) collective-permute-start(bf16[384,512]{1,0:T(8,128)(2,1)S(1)} %bitcast.11), channel_id=1, source_target_pairs={{0,6},{1,7},{2,0},{3,1},{4,2},{5,3},{6,4},{7,5},{8,14},{9,15},{10,... | collective-permute-start | bytes 1179656 | tf_op jit(solution)/shard_map/ppermute | solution.py:339
  4.7 0.1 collective-permute-start.7
  4.8 3.1 %collective-permute-start.9 = (bf16[384,512]{1,0:T(8,128)(2,1)S(1)}, bf16[384,512]{1,0:T(8,128)(2,1)S(1)}, u32[]{:S(2)}, u32[]{:S(2)}) collective-permute-start(bf16[384,512]{1,0:T(8,128)(2,1)S(1)} %bitcast.9), channel_id=1, source_target_pairs={{0,6},{1,7},{2,0},{3,1},{4,2},{5,3},{6,4},{7,5},{8,14},{9,15},{10,... | collective-permute-start | bytes 1179656 | tf_op jit(solution)/shard_map/ppermute | solution.py:339
  8.0 6.3 %collective-permute-done.3.refs_6_ = bf16[384,512]{1,0:T(8,128)(2,1)S(1)} collective-permute-done((bf16[384,512]{1,0:T(8,128)(2,1)S(1)}, bf16[384,512]{1,0:T(8,128)(2,1)S(1)}, u32[]{:S(2)}, u32[]{:S(2)}) %collective-permute-start.3) | collective-permute-done | bytes 393248 | tf_op jit(solution)/shard_map/ppermute | solution.py:339
  14.2 3.7 %collective-permute-done.refs_0_ = bf16[384,512]{1,0:T(8,128)(2,1)S(1)} collective-permute-done((bf16[384,512]{1,0:T(8,128)(2,1)S(1)}, bf16[384,512]{1,0:T(8,128)(2,1)S(1)}, u32[]{:S(2)}, u32[]{:S(2)}) %collective-permute-start) | collective-permute-done | bytes 393248 | tf_op jit(solution)/shard_map/ppermute | solution.py:339
  17.9 3.2 %collective-permute-start.4 = (bf16[384,512]{1,0:T(8,128)(2,1)S(1)}, bf16[384,512]{1,0:T(8,128)(2,1)}, u32[]{:S(2)}, u32[]{:S(2)}) collective-permute-start(bf16[384,512]{1,0:T(8,128)(2,1)S(1)} %collective-permute-done.3.refs_6_), channel_id=1, source_target_pairs={{0,6},{1,7},{2,0},{3,1},{4,2},{5,3},{6,4},{7,5},{8,14},{9,15},{10,... | collective-permute-start | bytes 1179656 | tf_op jit(solution)/shard_map/ppermute | solution.py:339
  21.1 1.5 %collective-permute-done.9.refs_2_ = bf16[384,512]{1,0:T(8,128)(2,1)S(1)} collective-permute-done((bf16[384,512]{1,0:T(8,128)(2,1)S(1)}, bf16[384,512]{1,0:T(8,128)(2,1)S(1)}, u32[]{:S(2)}, u32[]{:S(2)}) %collective-permute-start.9) | collective-permute-done | bytes 393248 | tf_op jit(solution)/shard_map/ppermute | solution.py:339
  22.6 3.8 %collective-permute-done.11.refs_4_ = bf16[384,512]{1,0:T(8,128)(2,1)} collective-permute-done((bf16[384,512]{1,0:T(8,128)(2,1)S(1)}, bf16[384,512]{1,0:T(8,128)(2,1)}, u32[]{:S(2)}, u32[]{:S(2)}) %collective-permute-start.11) | collective-permute-done | bytes 393248 | tf_op jit(solution)/shard_map/ppermute | solution.py:339
  26.4 0.5 collective-permute-start.12
  27.0 2.3 %shard_map.107 = f32[16,16,512]{2,1,0:T(8,128)} custom-call(bf16[4,256]{1,0:T(4,128)(2,1)} %x_ref.1, bf16[256,512]{1,0:T(8,128)(2,1)} %q_hbm.1, bf16[256,512]{1,0:T(8,128)(2,1)} %g_hbm.1, bf16[4096,512]{1,0:T(8,128)(2,1)} %f_hbm.1, bf16[4096,512]{1,0:T(8,128)(2,1)} %v_hbm.1), custom_call_target="tpu_custom_call" | custom-call | tf_op jit(solution)/shard_map/pallas_call | solution.py:27
  29.3 9.0 %all-to-all-start.1 = ((f32[16,16,512]{2,1,0:T(8,128)}), f32[16,16,512]{2,1,0:T(8,128)S(1)}, u32[]{:S(2)}, u32[]{:S(2)}) async-start(f32[16,16,512]{2,1,0:T(8,128)} %shard_map.107), calls=%async_computation.1 | async-start | bytes 1048576 | tf_op jit(solution)/shard_map/all_to_all | solution.py:345
  38.4 0.5 collective-permute-start.5
  38.9 3.5 %load.1 = (bf16[4096,512]{1,0:T(8,128)(2,1)S(1)}, bf16[4096,512]{1,0:T(8,128)(2,1)S(1)}, f32[768,512]{1,0:T(8,128)S(1)}, f32[768,512]{1,0:T(8,128)S(1)}) custom-call(bf16[384,512]{1,0:T(8,128)(2,1)S(1)} %bitcast.10, bf16[384,512]{1,0:T(8,128)(2,1)S(1)} %collective-permute-done.6.refs_1_, bf16[384,512]{1,0:T(8,128)(2,1)S(1)} %bitcast.14, ...), custom_call_target="tpu_custom_call" | custom-call | tf_op jit(solution)/shard_map/load/pallas_call | solution.py:136
  42.5 4.8 %shard_map.105 = (f32[768,512]{1,0:T(8,128)S(1)}, f32[768,512]{1,0:T(8,128)S(1)}) custom-call(bf16[384,512]{1,0:T(8,128)(2,1)S(1)} %collective-permute-done.refs_0_, bf16[384,512]{1,0:T(8,128)(2,1)} %collective-permute-done.8.refs_1_, bf16[384,512]{1,0:T(8,128)(2,1)S(1)} %collective-permute-done.9.refs_2_, bf16[384,512]{1,0:T(8,128)(2,1)} %collective-permute-done.10.refs_3_, ...), custom_call_target="tpu_custom_call" | custom-call | flops 3221225472 | tf_op jit(solution)/shard_map/pallas_call | solution.py:27
  47.3 6.1 %shard_map.106 = bf16[16,17,8,128]{3,2,1,0:T(8,128)(2,1)} custom-call(bf16[384,512]{1,0:T(8,128)(2,1)} %collective-permute-done.1.refs_0_, bf16[384,512]{1,0:T(8,128)(2,1)S(1)} %collective-permute-done.2.refs_1_, bf16[384,512]{1,0:T(8,128)(2,1)} %collective-permute-done.4.refs_2_, bf16[384,512]{1,0:T(8,128)(2,1)S(1)} %collective-permute-done.5.refs_3_, ...), custom_call_target="tpu_custom_call" | custom-call | flops 4831838208 | tf_op jit(solution)/shard_map/pallas_call | solution.py:27
  53.4 7.5 %all-to-all-start = ((bf16[16,17,8,128]{3,2,1,0:T(8,128)(2,1)}), bf16[16,17,8,128]{3,2,1,0:T(8,128)(2,1)S(1)}, u32[]{:S(2)}, u32[]{:S(2)}) async-start(bf16[16,17,8,128]{3,2,1,0:T(8,128)(2,1)} %shard_map.106), calls=%async_computation | async-start | bytes 1114112 | tf_op jit(solution)/shard_map/all_to_all | solution.py:345
  61.0 0.2 shard_map.108
  61.1 14.7 %all-to-all-done.got_ref = bf16[16,17,8,128]{3,2,1,0:T(8,128)(2,1)S(1)} async-done(((bf16[16,17,8,128]{3,2,1,0:T(8,128)(2,1)}), bf16[16,17,8,128]{3,2,1,0:T(8,128)(2,1)S(1)}, u32[]{:S(2)}, u32[]{:S(2)}) %all-to-all-start) | async-done | bytes 557088 | tf_op jit(solution)/shard_map/all_to_all | solution.py:345
  75.8 1.8 %shard_map.109 = (bf16[16,8,128]{2,1,0:T(8,128)(2,1)S(1)}, f32[16,16,128]{2,1,0:T(8,128)}) custom-call(bf16[16,17,8,128]{3,2,1,0:T(8,128)(2,1)S(1)} %all-to-all-done.got_ref, f32[8,16]{1,0:T(8,128)S(1)} %get-tuple-element.24.query_ref, f32[8,16]{1,0:T(8,128)S(1)} %get-tuple-element.25.keys_ref, f32[16,128]{1,0:T(8,128)S(1)} %get-tuple-element.26.value_ref), custom_call_target="tpu_custom_call" | custom-call | tf_op jit(solution)/shard_map/pallas_call | solution.py:27
  77.7 6.2 %all-to-all-start.2 = ((f32[16,16,128]{2,1,0:T(8,128)}), f32[16,16,128]{2,1,0:T(8,128)S(1)}, u32[]{:S(2)}, u32[]{:S(2)}) async-start(f32[16,16,128]{2,1,0:T(8,128)} %get-tuple-element.28), calls=%async_computation.2 | async-start | bytes 262144 | tf_op jit(solution)/shard_map/all_to_all | solution.py:345
  83.8 0.6 copy.11
  84.5 7.0 %all-to-all-done.2.got_ref = f32[16,16,128]{2,1,0:T(8,128)S(1)} async-done(((f32[16,16,128]{2,1,0:T(8,128)}), f32[16,16,128]{2,1,0:T(8,128)S(1)}, u32[]{:S(2)}, u32[]{:S(2)}) %all-to-all-start.2) | async-done | bytes 131104 | tf_op jit(solution)/shard_map/all_to_all | solution.py:345
  91.4 0.7 shard_map.110
  (29 shorter events, 0.3 us)
Async XLA Ops:
  1.8 6.2 %collective-permute-start.6 = (bf16[384,512]{1,0:T(8,128)(2,1)S(1)}, bf16[384,512]{1,0:T(8,128)(2,1)S(1)}, u32[]{:S(2)}, u32[]{:S(2)}) collective-permute-start(bf16[384,512]{1,0:T(8,128)(2,1)S(1)} %bitcast.7), channel_id=1, source_target_pairs={{0,1},{1,0},{2,3},{3,2},{4,5},{5,4},{6,7},{7,6},{8,9},{9,8},{10,11... | collective-permute-start | bytes 1179656 | tf_op jit(solution)/shard_map/ppermute | solution.py:342
  1.9 12.3 %collective-permute-start.3 = (bf16[384,512]{1,0:T(8,128)(2,1)S(1)}, bf16[384,512]{1,0:T(8,128)(2,1)S(1)}, u32[]{:S(2)}, u32[]{:S(2)}) collective-permute-start(bf16[384,512]{1,0:T(8,128)(2,1)S(1)} %bitcast.11), channel_id=1, source_target_pairs={{0,6},{1,7},{2,0},{3,1},{4,2},{5,3},{6,4},{7,5},{8,14},{9,15},{10,... | collective-permute-start | bytes 1179656 | tf_op jit(solution)/shard_map/ppermute | solution.py:339
  4.7 13.2 %collective-permute-start = (bf16[384,512]{1,0:T(8,128)(2,1)S(1)}, bf16[384,512]{1,0:T(8,128)(2,1)S(1)}, u32[]{:S(2)}, u32[]{:S(2)}) collective-permute-start(bf16[384,512]{1,0:T(8,128)(2,1)S(1)} %bitcast.8), channel_id=1, source_target_pairs={{0,2},{1,3},{2,4},{3,5},{4,6},{5,7},{6,0},{7,1},{8,10},{9,11},{10,... | collective-permute-start | bytes 1179656 | tf_op jit(solution)/shard_map/ppermute | solution.py:339
  4.7 13.2 %collective-permute-start.7 = (bf16[384,512]{1,0:T(8,128)(2,1)S(1)}, bf16[384,512]{1,0:T(8,128)(2,1)S(1)}, u32[]{:S(2)}, u32[]{:S(2)}) collective-permute-start(bf16[384,512]{1,0:T(8,128)(2,1)S(1)} %bitcast.12), channel_id=1, source_target_pairs={{0,1},{1,0},{2,3},{3,2},{4,5},{5,4},{6,7},{7,6},{8,9},{9,8},{10,11... | collective-permute-start | bytes 1179656 | tf_op jit(solution)/shard_map/ppermute | solution.py:342
  4.8 17.8 %collective-permute-start.9 = (bf16[384,512]{1,0:T(8,128)(2,1)S(1)}, bf16[384,512]{1,0:T(8,128)(2,1)S(1)}, u32[]{:S(2)}, u32[]{:S(2)}) collective-permute-start(bf16[384,512]{1,0:T(8,128)(2,1)S(1)} %bitcast.9), channel_id=1, source_target_pairs={{0,6},{1,7},{2,0},{3,1},{4,2},{5,3},{6,4},{7,5},{8,14},{9,15},{10,... | collective-permute-start | bytes 1179656 | tf_op jit(solution)/shard_map/ppermute | solution.py:339
  7.9 18.5 %collective-permute-start.11 = (bf16[384,512]{1,0:T(8,128)(2,1)S(1)}, bf16[384,512]{1,0:T(8,128)(2,1)}, u32[]{:S(2)}, u32[]{:S(2)}) collective-permute-start(bf16[384,512]{1,0:T(8,128)(2,1)S(1)} %bitcast.13), channel_id=1, source_target_pairs={{0,2},{1,3},{2,4},{3,5},{4,6},{5,7},{6,0},{7,1},{8,10},{9,11},{10,... | collective-permute-start | bytes 1179656 | tf_op jit(solution)/shard_map/ppermute | solution.py:339
  14.2 12.2 %collective-permute-start.13 = (bf16[384,512]{1,0:T(8,128)(2,1)S(1)}, bf16[384,512]{1,0:T(8,128)(2,1)S(1)}, u32[]{:S(2)}, u32[]{:S(2)}) collective-permute-start(bf16[384,512]{1,0:T(8,128)(2,1)S(1)} %collective-permute-done.3.refs_6_), channel_id=1, source_target_pairs={{0,1},{1,0},{2,3},{3,2},{4,5},{5,4},{6,7},{7,6},{8,9},{9,8},{10,11... | collective-permute-start | bytes 1179656 | tf_op jit(solution)/shard_map/ppermute | solution.py:342
  17.9 20.4 %collective-permute-start.1 = (bf16[384,512]{1,0:T(8,128)(2,1)S(1)}, bf16[384,512]{1,0:T(8,128)(2,1)}, u32[]{:S(2)}, u32[]{:S(2)}) collective-permute-start(bf16[384,512]{1,0:T(8,128)(2,1)S(1)} %collective-permute-done.refs_0_), channel_id=1, source_target_pairs={{0,2},{1,3},{2,4},{3,5},{4,6},{5,7},{6,0},{7,1},{8,10},{9,11},{10,... | collective-permute-start | bytes 1179656 | tf_op jit(solution)/shard_map/ppermute | solution.py:339
  17.9 20.5 %collective-permute-start.4 = (bf16[384,512]{1,0:T(8,128)(2,1)S(1)}, bf16[384,512]{1,0:T(8,128)(2,1)}, u32[]{:S(2)}, u32[]{:S(2)}) collective-permute-start(bf16[384,512]{1,0:T(8,128)(2,1)S(1)} %collective-permute-done.3.refs_6_), channel_id=1, source_target_pairs={{0,6},{1,7},{2,0},{3,1},{4,2},{5,3},{6,4},{7,5},{8,14},{9,15},{10,... | collective-permute-start | bytes 1179656 | tf_op jit(solution)/shard_map/ppermute | solution.py:339
  22.6 19.8 %collective-permute-start.8 = (bf16[384,512]{1,0:T(8,128)(2,1)S(1)}, bf16[384,512]{1,0:T(8,128)(2,1)}, u32[]{:S(2)}, u32[]{:S(2)}) collective-permute-start(bf16[384,512]{1,0:T(8,128)(2,1)S(1)} %collective-permute-done.refs_0_), channel_id=1, source_target_pairs={{0,1},{1,0},{2,3},{3,2},{4,5},{5,4},{6,7},{7,6},{8,9},{9,8},{10,11... | collective-permute-start | bytes 1179656 | tf_op jit(solution)/shard_map/ppermute | solution.py:342
  26.4 16.0 %collective-permute-start.10 = (bf16[384,512]{1,0:T(8,128)(2,1)S(1)}, bf16[384,512]{1,0:T(8,128)(2,1)}, u32[]{:S(2)}, u32[]{:S(2)}) collective-permute-start(bf16[384,512]{1,0:T(8,128)(2,1)S(1)} %collective-permute-done.9.refs_2_), channel_id=1, source_target_pairs={{0,1},{1,0},{2,3},{3,2},{4,5},{5,4},{6,7},{7,6},{8,9},{9,8},{10,11... | collective-permute-start | bytes 1179656 | tf_op jit(solution)/shard_map/ppermute | solution.py:342
  26.4 2.9 %copy-start = (bf16[384,512]{1,0:T(8,128)(2,1)}, bf16[384,512]{1,0:T(8,128)(2,1)S(1)}, u32[]{:S(2)}) copy-start(bf16[384,512]{1,0:T(8,128)(2,1)S(1)} %collective-permute-done.13.refs_7_) | copy-start | bytes 1179652
  26.4 16.0 %collective-permute-start.12 = (bf16[384,512]{1,0:T(8,128)(2,1)}, bf16[384,512]{1,0:T(8,128)(2,1)}, u32[]{:S(2)}, u32[]{:S(2)}) collective-permute-start(bf16[384,512]{1,0:T(8,128)(2,1)} %collective-permute-done.11.refs_4_), channel_id=1, source_target_pairs={{0,1},{1,0},{2,3},{3,2},{4,5},{5,4},{6,7},{7,6},{8,9},{9,8},{10,11... | collective-permute-start | bytes 1179656 | tf_op jit(solution)/shard_map/ppermute | solution.py:342
  29.3 24.1 %all-to-all-start.1 = ((f32[16,16,512]{2,1,0:T(8,128)}), f32[16,16,512]{2,1,0:T(8,128)S(1)}, u32[]{:S(2)}, u32[]{:S(2)}) async-start(f32[16,16,512]{2,1,0:T(8,128)} %shard_map.107), calls=%async_computation.1 | async-start | bytes 1048576 | tf_op jit(solution)/shard_map/all_to_all | solution.py:345
  38.3 4.1 %copy-start.1 = (bf16[384,512]{1,0:T(8,128)(2,1)S(1)}, bf16[384,512]{1,0:T(8,128)(2,1)}, u32[]{:S(2)}) copy-start(bf16[384,512]{1,0:T(8,128)(2,1)} %copy-done) | copy-start | bytes 1179652
  38.3 8.9 %collective-permute-start.2 = (bf16[384,512]{1,0:T(8,128)(2,1)}, bf16[384,512]{1,0:T(8,128)(2,1)S(1)}, u32[]{:S(2)}, u32[]{:S(2)}) collective-permute-start(bf16[384,512]{1,0:T(8,128)(2,1)} %collective-permute-done.1.refs_0_), channel_id=1, source_target_pairs={{0,1},{1,0},{2,3},{3,2},{4,5},{5,4},{6,7},{7,6},{8,9},{9,8},{10,11... | collective-permute-start | bytes 1179656 | tf_op jit(solution)/shard_map/ppermute | solution.py:342
  38.4 8.8 %collective-permute-start.5 = (bf16[384,512]{1,0:T(8,128)(2,1)}, bf16[384,512]{1,0:T(8,128)(2,1)S(1)}, u32[]{:S(2)}, u32[]{:S(2)}) collective-permute-start(bf16[384,512]{1,0:T(8,128)(2,1)} %collective-permute-done.4.refs_2_), channel_id=1, source_target_pairs={{0,1},{1,0},{2,3},{3,2},{4,5},{5,4},{6,7},{7,6},{8,9},{9,8},{10,11... | collective-permute-start | bytes 1179656 | tf_op jit(solution)/shard_map/ppermute | solution.py:342
  42.4 4.8 %copy-start.2 = (f32[512]{0:T(512)S(1)}, f32[512]{0:T(512)}, u32[]{:S(2)}) copy-start(f32[512]{0:T(512)} %param.15) | copy-start | bytes 6148
  42.5 4.8 %copy-start.4 = (f32[4,192,4]{1,2,0:T(4,128)S(1)}, f32[4,192,4]{1,2,0:T(4,128)}, u32[]{:S(2)}) copy-start(f32[4,192,4]{1,2,0:T(4,128)} %param.16) | copy-start | bytes 36868
  47.3 44.1 %copy-start.3 = (f32[128]{0:T(128)S(1)}, f32[128]{0:T(128)}, u32[]{:S(2)}) copy-start(f32[128]{0:T(128)} %param.17) | copy-start | bytes 1540
  53.4 22.4 %all-to-all-start = ((bf16[16,17,8,128]{3,2,1,0:T(8,128)(2,1)}), bf16[16,17,8,128]{3,2,1,0:T(8,128)(2,1)S(1)}, u32[]{:S(2)}, u32[]{:S(2)}) async-start(bf16[16,17,8,128]{3,2,1,0:T(8,128)(2,1)} %shard_map.106), calls=%async_computation | async-start | bytes 1114112 | tf_op jit(solution)/shard_map/all_to_all | solution.py:345
  77.7 13.7 %all-to-all-start.2 = ((f32[16,16,128]{2,1,0:T(8,128)}), f32[16,16,128]{2,1,0:T(8,128)S(1)}, u32[]{:S(2)}, u32[]{:S(2)}) async-start(f32[16,16,128]{2,1,0:T(8,128)} %get-tuple-element.28), calls=%async_computation.2 | async-start | bytes 262144 | tf_op jit(solution)/shard_map/all_to_all | solution.py:345

commit v5 on v4

--- a/solution.py
+++ b/solution.py
@@ -10,6 +10,7 @@
 
 BF = jnp.bfloat16
 F32 = jnp.float32
+NEAR = 4
 
 
 def three_terms(x):
@@ -148,9 +149,9 @@
 def state_kernel(*refs, plan, head_dim):
     count = sum(map(len, plan))
     pieces, (wf_ref, wv_ref, f_in, v_in, *refs) = refs[:count], refs[count:]
-    slack_ref, damp_ref, out_ref, f_acc, v_acc = refs
+    slack_ref, damp_ref, *outs, total_ref, state_ref, f_acc, v_acc, parts_ref = refs
     add_products(pieces, plan, (wf_ref, wv_ref), (f_in, v_in), (f_acc, v_acc))
-    parts = out_ref.shape[0]
+    far, rows = parts_ref.shape[1], parts_ref.shape[3]
     seqs, heads, length = damp_ref.shape
     channels = heads * head_dim
     tall = length + 8
@@ -188,76 +189,135 @@
                 weighted[:, cols], values[:, cols], over_rows, preferred_element_type=F32
             )
             totals.append(sums[length : length + 1, cols])
-            out_ref[:, s * heads + h] = state.astype(BF).reshape(parts, head_dim // parts, head_dim)
+            state = state.astype(BF)
+            state_ref[s * heads + h] = state
+            blocks = state.reshape(far, NEAR, rows, head_dim)
+            for y in range(NEAR):
+                parts_ref[y, :, s * heads + h] = blocks[:, y]
     pairs = seqs * heads
-    terms = [t.astype(F32) for t in three_terms(jnp.concatenate(totals))]
+    totals = jnp.concatenate(totals)
+    for p in range(total_ref.shape[0]):
+        total_ref[p] = totals
+    terms = [t.astype(F32) for t in three_terms(totals)]
     packed = jnp.concatenate([*terms, jnp.zeros((head_dim - 3 * pairs, head_dim), F32)])
-    out_ref[:, pairs] = packed.T.astype(BF).reshape(parts, head_dim // parts, head_dim)
+    blocks = packed.T.astype(BF).reshape(far, NEAR, rows, head_dim)
+    for y in range(NEAR):
+        parts_ref[y, :, pairs] = blocks[:, y]
+    near = lax.rem(lax.axis_index("sp"), NEAR)
+    for step, out in enumerate(outs):
+        out[...] = parts_ref[lax.rem(near + step, NEAR)]
 
 
 def states(pieces, plan, weights, sums, slack, damp, parts):
     seqs, heads, _ = damp.shape
     head_dim = weights[0].shape[1] // heads
-    return in_vmem(
+    pairs = seqs * heads
+    shape = (parts // NEAR, pairs + 1, head_dim // parts, head_dim)
+    *outs, totals, state = in_vmem(
         functools.partial(state_kernel, plan=plan, head_dim=head_dim),
-        jax.ShapeDtypeStruct((parts, seqs * heads + 1, head_dim // parts, head_dim), BF),
+        [jax.ShapeDtypeStruct(shape, BF)] * NEAR
+        + [
+            jax.ShapeDtypeStruct((parts, pairs, head_dim), F32),
+            jax.ShapeDtypeStruct((pairs, head_dim, head_dim), BF),
+        ],
         *pieces,
         *weights,
         *sums,
         slack,
         damp,
-        scratch=[pltpu.VMEM(s.shape, F32) for s in sums],
+        scratch=[pltpu.VMEM(s.shape, F32) for s in sums] + [pltpu.VMEM((NEAR, *shape), BF)],
         flops=12 * len(pieces) * pieces[0].size * weights[0].shape[1],
     )
-
-
-def combine_kernel(got_ref, query_ref, keys_ref, value_ref, cache_ref, read_ref):
-    parts, pairs = got_ref.shape[0], got_ref.shape[1] - 1
-    rows, head_dim = got_ref.shape[2:]
-    after = jnp.zeros((rows, head_dim), F32)
-    sums = [jnp.zeros((rows, head_dim), F32)] * pairs
-    for src in range(parts - 1, -1, -1):
+    return outs, totals, state
+
+
+def unpacked(tile, pairs):
+    tile = tile.astype(F32)
+    lanes = tile.shape[1]
+    return tile + pltpu.roll(tile, lanes - pairs, 1) + pltpu.roll(tile, lanes - 2 * pairs, 1)
+
+
+def joined(tiles, place, count):
+    pairs = tiles[0].shape[0] - 1
+    places = [lax.rem(place + count - step, count) for step in range(count)]
+    totals = [unpacked(tile[pairs], pairs) for tile in tiles]
+    sums = [None] * pairs
+    for here, tile in zip(places, tiles):
+        after = sum(jnp.where(p > here, 1.0, 0.0) * total for p, total in zip(places, totals))
         scale = jnp.exp(after)
         for j in range(pairs):
-            sums[j] = sums[j] + scale[:, j : j + 1] * got_ref[src, j].astype(F32)
-        packed = got_ref[src, pairs].astype(F32)
-        after = after + (
-            packed
-            + pltpu.roll(packed, head_dim - pairs, 1)
-            + pltpu.roll(packed, head_dim - 2 * pairs, 1)
-        )
+            part = scale[:, j : j + 1] * tile[j].astype(F32)
+            sums[j] = part if sums[j] is None else sums[j] + part
+    return sums, sum(totals)
+
+
+def near_kernel(*refs):
+    tiles, outs, parts_ref = refs[:NEAR], refs[NEAR:-1], refs[-1]
+    far, tile_count, rows, lanes = parts_ref.shape
+    pairs = tile_count - 1
+    me = lax.axis_index("sp")
+    lane = lax.broadcasted_iota(jnp.int32, (rows, lanes), 1)
+    for z in range(far):
+        sums, total = joined([t.at[z] for t in tiles], lax.rem(me, NEAR), NEAR)
+        for j in range(pairs):
+            parts_ref[z, j] = sums[j].astype(BF)
+        high, middle, low = (t.astype(F32) for t in three_terms(total))
+        packed = jnp.where(lane < 2 * pairs, pltpu.roll(middle, pairs, 1), pltpu.roll(low, 2 * pairs, 1))
+        packed = jnp.where(lane < pairs, high, packed)
+        parts_ref[z, pairs] = jnp.where(lane < 3 * pairs, packed, 0.0).astype(BF)
+    for step, out in enumerate(outs):
+        out[...] = parts_ref[lax.rem(me // NEAR + step, far)]
+
+
+def join_near(tiles):
+    shape = tiles[0].shape
+    return in_vmem(
+        near_kernel,
+        [jax.ShapeDtypeStruct(shape[1:], BF)] * shape[0],
+        *tiles,
+        scratch=[pltpu.VMEM(shape, BF)],
+    )
+
+
+def far_kernel(*refs):
+    tiles, cache_ref = refs[:-1], refs[-1]
+    sums, _ = joined(tiles, lax.axis_index("sp") // NEAR, len(tiles))
+    for j, part in enumerate(sums):
+        cache_ref[j] = part.astype(BF)
+
+
+def join_far(tiles):
+    tile_count, rows, lanes = tiles[0].shape
+    return in_vmem(far_kernel, pltpu.VMEM((tile_count - 1, rows, lanes), BF), *tiles)
+
+
+def read_kernel(totals_ref, state_ref, query_ref, keys_ref, out_ref):
+    me = lax.axis_index("sp")
+    after = sum(
+        jnp.where(src > me, 1.0, 0.0) * totals_ref[src] for src in range(totals_ref.shape[0])
+    )
+    weights = query_ref[...] * (1.0 - keys_ref[...]) * jnp.exp(after)
+    pairs = weights.shape[0]
+    terms = jnp.concatenate(three_terms(weights))
     reads = []
     for j in range(pairs):
-        rounded = sums[j].astype(BF)
-        cache_ref[j] = rounded
-        keys = keys_ref[:, j : j + 1]
-        updated = (1.0 - keys) * rounded.astype(F32) + keys * value_ref[j : j + 1, :]
-        reads.append(jnp.sum(query_ref[:, j : j + 1] * updated, axis=0, keepdims=True))
+        parts = jnp.dot(terms, state_ref[j], preferred_element_type=F32)
+        reads.append(sum(parts[n : n + 1, :] for n in range(j, 3 * pairs, pairs)))
     reads = jnp.concatenate(reads)
-    for p in range(parts):
-        read_ref[p] = reads
-
-
-def combine(got, query, keys, value):
-    parts, tiles, rows, head_dim = got.shape
-    return in_vmem(
-        combine_kernel,
-        [
-            pltpu.VMEM((tiles - 1, rows, head_dim), BF),
-            jax.ShapeDtypeStruct((parts, tiles - 1, head_dim), F32),
-        ],
-        got,
-        query,
-        keys,
-        value,
-    )
-
-
-def finish_kernel(got_ref, norm_ref, gate_ref, out_ref):
+    for p in range(out_ref.shape[0]):
+        out_ref[p] = reads
+
+
+def read_parts(totals, state, query, keys):
+    return in_vmem(read_kernel, jax.ShapeDtypeStruct(totals.shape, F32), totals, state, query, keys)
+
+
+def finish_kernel(got_ref, query_ref, keys_ref, value_ref, norm_ref, gate_ref, out_ref):
     heads = out_ref.shape[1] // got_ref.shape[2]
     head_dim = got_ref.shape[2]
-    read = got_ref[0]
-    for src in range(1, got_ref.shape[0]):
+    shared = jnp.sum(query_ref[...] * keys_ref[...], axis=1, keepdims=True)
+    read = shared * value_ref[...]
+    for src in range(got_ref.shape[0]):
         read = read + got_ref[src]
     scaled = read * lax.rsqrt(jnp.mean(read * read, axis=1, keepdims=True) + 1e-06) * norm_ref[...]
     result = (scaled * gate_ref[...]).astype(BF)
@@ -280,7 +340,6 @@
 
 def prepare_kernel(got_ref, slack_ref, query_ref, keys_ref, value_ref, gate_ref):
     pairs, head_dim = value_ref.shape
-    rows = query_ref.shape[0]
     seqs = got_ref.shape[1] // 4
     heads = pairs // seqs
     total = got_ref[0]
@@ -301,17 +360,8 @@
     keys = slack_ref[...] * jax.nn.sigmoid(-forget)
     value_ref[...] = by_head(value)
     gate_ref[...] = by_head(gate * jax.nn.sigmoid(gate))
-    own = lax.axis_index("sp") * rows + lax.broadcasted_iota(jnp.int32, (rows, head_dim), 0)
-    chosen = jnp.where(lax.broadcasted_iota(jnp.int32, (rows, head_dim), 1) == own, 1.0, 0.0).astype(BF)
-
-    def own_rows(x):
-        return sum(
-            lax.dot_general(chosen, t, (((1,), (1,)), ((), ())), preferred_element_type=F32)
-            for t in three_terms(x)
-        )
-
-    query_ref[...] = own_rows(by_head(query))
-    keys_ref[...] = own_rows(by_head(keys))
+    query_ref[...] = by_head(query)
+    keys_ref[...] = by_head(keys)
 
 
 def per_device(
@@ -373,12 +423,8 @@
     new_sums = exchange(partial)
     row_count = head_dim // sp_count
     pairs = seqs * heads
-    query_rows, key_rows, value_new, gate_new = in_vmem(
-        prepare_kernel,
-        [jax.ShapeDtypeStruct((row_count, pairs), F32)] * 2
-        + [jax.ShapeDtypeStruct((pairs, head_dim), F32)] * 2,
-        new_sums,
-        slack,
+    query_new, keys_new, value_new, gate_new = in_vmem(
+        prepare_kernel, [jax.ShapeDtypeStruct((pairs, head_dim), F32)] * 4, new_sums, slack
     )
 
     far_a, far_b = shifted(right_a, 1), shifted(left_b, -1)
@@ -395,7 +441,7 @@
     pieces = [right_a, other_right_a, left_a, other_left_a]
     pieces += [right_b, other_right_b, left_b, other_left_b]
     sums = project(pieces, (both(1) + both(-1), both(1) + both(-1)), weights, sums)
-    out = states(
+    parts, totals, state = states(
         [far_a, other_far_a, far_b, other_far_b],
         (both(2), both(2)),
         weights,
@@ -404,13 +450,38 @@
         additional_damping_exponent.transpose(0, 2, 1),
         sp_count,
     )
-    got = exchange(out)
-    cache, read = combine(got, query_rows, key_rows, value_new)
+
+    planes = sp_count // NEAR
+
+    def along_y(step):
+        pairs = [
+            (z * NEAR + y, z * NEAR + (y + step) % NEAR) for z in range(planes) for y in range(NEAR)
+        ]
+        return lax.ppermute(parts[step], "sp", pairs)
+
+    def along_z(step):
+        pairs = [
+            (z * NEAR + y, (z + step) % planes * NEAR + y)
+            for z in range(planes)
+            for y in range(NEAR)
+        ]
+        return lax.ppermute(parts[step], "sp", pairs)
+
+    parts = [parts[0], *(along_y(step) for step in range(1, NEAR))]
+    parts = join_near(parts)
+    parts = [parts[0], *(along_z(step) for step in range(1, planes))]
+    cache = join_far(parts)
+
+    totals = exchange(totals)
+    read = read_parts(totals, state, query_new, keys_new)
     got = exchange(read)
     first_read = in_vmem(
         finish_kernel,
         jax.ShapeDtypeStruct((seqs, channels), BF),
         got,
+        query_new,
+        keys_new,
+        value_new,
         read_norm_scale.reshape(1, head_dim),
         gate_new,
     )

time: 92.6 us -> 95.7 us (1.033)
  starting transfers between devices: 33.2 us -> 41.6 us
  waiting for transfers between devices: 36.9 us -> 30.8 us
    all_to_all x3, waiting for transfers between devices: 21.6 us -> 7.61 us  [exchange(): return lax.all_to_all(x, 'sp', 0, 0, tiled=True)]
    ppermute x0 -> x6, starting transfers between devices: none -> 9.84 us  [the longest x3 5.13 us: along_z(): return lax.ppermute(parts[step], 'sp', pairs)]
    ppermute x0 -> x6, waiting for transfers between devices: none -> 7.97 us  [the longest x3 5.59 us: along_y(): return lax.ppermute(parts[step], 'sp', pairs)]
    all_to_all x3, starting transfers between devices: 22.7 us -> 21.3 us  [exchange(): return lax.all_to_all(x, 'sp', 0, 0, tiled=True)]
    pallas_call x6 -> x8, Pallas kernels: 16 us -> 15.9 us  [in_vmem(): pl.pallas_call(kernel, in_specs=in_specs or [VMEM] * len(arrays), out_spe...]
  transfers between devices with their start and end apart: 17 -> 23, of which waited for: 6 -> 11; matrix products, arithmetic and copies ran while one was open for 1% -> 1% of each run, Pallas kernels for 18% -> 19%
where the time goes in v5:
time: 95.7 us; the launch traced here: 95.2 us
  starting transfers between devices  41.6 us (43%)
  waiting for transfers between devices  30.8 us (32%)
  Pallas kernels  20.5 us (21%)
  local copies, waits for them, and re-layouts  1.41 us (1%)
    all_to_all x3, starting transfers between devices, exchange(): return lax.all_to_all(x, 'sp', 0, 0, tiled=True)  21.3 us
    pallas_call x8, Pallas kernels, in_vmem(): pl.pallas_call(kernel, in_specs=in_specs or [VMEM] * len(arrays), out_spe...  15.9 us
    ppermute x6, waiting for transfers between devices, shifted(): return lax.ppermute(x, 'tp', pairs)  15.2 us
    ppermute x6, starting transfers between devices, shifted(): return lax.ppermute(x, 'tp', pairs)  9.17 us
    all_to_all x3, waiting for transfers between devices, exchange(): return lax.all_to_all(x, 'sp', 0, 0, tiled=True)  7.61 us
    ppermute x3, waiting for transfers between devices, along_y(): return lax.ppermute(parts[step], 'sp', pairs)  5.59 us
    ppermute x3, starting transfers between devices, along_z(): return lax.ppermute(parts[step], 'sp', pairs)  5.13 us
    ppermute x3, starting transfers between devices, along_y(): return lax.ppermute(parts[step], 'sp', pairs)  4.71 us
  transfers between devices with their start and end apart: 23, of which 11 were waited for; matrix products, arithmetic and copies ran while one was open for 1% of the time, Pallas kernels for 19%

profile of v5, /device:TPU:8, one launch (start us, length us, event | category | flops | bytes accessed | tf_op | source)
XLA Modules:
  0.0 95.2 jit_solution(6261201231402904367)
XLA Ops:
  0.6 1.1 %shard_map.104 = (bf16[2,192,512]{2,1,0:T(8,128)(2,1)S(1)}, bf16[2,192,512]{2,1,0:T(8,128)(2,1)S(1)}) custom-call(bf16[4,192,512]{2,1,0:T(8,128)(2,1)} %tokens_ref.1), custom_call_target="tpu_custom_call" | custom-call | tf_op jit(solution)/shard_map/pallas_call | solution.py:48
  1.9 2.8 %collective-permute-start.3 = (bf16[384,512]{1,0:T(8,128)(2,1)S(1)}, bf16[384,512]{1,0:T(8,128)(2,1)S(1)}, u32[]{:S(2)}, u32[]{:S(2)}) collective-permute-start(bf16[384,512]{1,0:T(8,128)(2,1)S(1)} %bitcast.11), channel_id=1, source_target_pairs={{0,6},{1,7},{2,0},{3,1},{4,2},{5,3},{6,4},{7,5},{8,14},{9,15},{10,... | collective-permute-start | bytes 1179656 | tf_op jit(solution)/shard_map/ppermute | solution.py:389
  4.8 3.1 %collective-permute-start.9 = (bf16[384,512]{1,0:T(8,128)(2,1)S(1)}, bf16[384,512]{1,0:T(8,128)(2,1)S(1)}, u32[]{:S(2)}, u32[]{:S(2)}) collective-permute-start(bf16[384,512]{1,0:T(8,128)(2,1)S(1)} %bitcast.9), channel_id=1, source_target_pairs={{0,6},{1,7},{2,0},{3,1},{4,2},{5,3},{6,4},{7,5},{8,14},{9,15},{10,... | collective-permute-start | bytes 1179656 | tf_op jit(solution)/shard_map/ppermute | solution.py:389
  8.0 6.3 %collective-permute-done.3.refs_6_ = bf16[384,512]{1,0:T(8,128)(2,1)S(1)} collective-permute-done((bf16[384,512]{1,0:T(8,128)(2,1)S(1)}, bf16[384,512]{1,0:T(8,128)(2,1)S(1)}, u32[]{:S(2)}, u32[]{:S(2)}) %collective-permute-start.3) | collective-permute-done | bytes 393248 | tf_op jit(solution)/shard_map/ppermute | solution.py:389
  14.2 3.7 %collective-permute-done.refs_0_ = bf16[384,512]{1,0:T(8,128)(2,1)S(1)} collective-permute-done((bf16[384,512]{1,0:T(8,128)(2,1)S(1)}, bf16[384,512]{1,0:T(8,128)(2,1)S(1)}, u32[]{:S(2)}, u32[]{:S(2)}) %collective-permute-start) | collective-permute-done | bytes 393248 | tf_op jit(solution)/shard_map/ppermute | solution.py:389
  17.9 3.2 %collective-permute-start.4 = (bf16[384,512]{1,0:T(8,128)(2,1)S(1)}, bf16[384,512]{1,0:T(8,128)(2,1)}, u32[]{:S(2)}, u32[]{:S(2)}) collective-permute-start(bf16[384,512]{1,0:T(8,128)(2,1)S(1)} %collective-permute-done.3.refs_6_), channel_id=1, source_target_pairs={{0,6},{1,7},{2,0},{3,1},{4,2},{5,3},{6,4},{7,5},{8,14},{9,15},{10,... | collective-permute-start | bytes 1179656 | tf_op jit(solution)/shard_map/ppermute | solution.py:389
  21.1 1.5 %collective-permute-done.9.refs_2_ = bf16[384,512]{1,0:T(8,128)(2,1)S(1)} collective-permute-done((bf16[384,512]{1,0:T(8,128)(2,1)S(1)}, bf16[384,512]{1,0:T(8,128)(2,1)S(1)}, u32[]{:S(2)}, u32[]{:S(2)}) %collective-permute-start.9) | collective-permute-done | bytes 393248 | tf_op jit(solution)/shard_map/ppermute | solution.py:389
  22.6 3.8 %collective-permute-done.11.refs_4_ = bf16[384,512]{1,0:T(8,128)(2,1)} collective-permute-done((bf16[384,512]{1,0:T(8,128)(2,1)S(1)}, bf16[384,512]{1,0:T(8,128)(2,1)}, u32[]{:S(2)}, u32[]{:S(2)}) %collective-permute-start.11) | collective-permute-done | bytes 393248 | tf_op jit(solution)/shard_map/ppermute | solution.py:389
  27.7 2.3 %shard_map.109 = f32[16,16,512]{2,1,0:T(8,128)} custom-call(bf16[4,256]{1,0:T(4,128)(2,1)} %x_ref.1, bf16[256,512]{1,0:T(8,128)(2,1)} %q_hbm.1, bf16[256,512]{1,0:T(8,128)(2,1)} %g_hbm.1, bf16[4096,512]{1,0:T(8,128)(2,1)} %f_hbm.1, bf16[4096,512]{1,0:T(8,128)(2,1)} %v_hbm.1), custom_call_target="tpu_custom_call" | custom-call | tf_op jit(solution)/shard_map/pallas_call | solution.py:28
  30.0 9.0 %all-to-all-start.1 = ((f32[16,16,512]{2,1,0:T(8,128)}), f32[16,16,512]{2,1,0:T(8,128)S(1)}, u32[]{:S(2)}, u32[]{:S(2)}) async-start(f32[16,16,512]{2,1,0:T(8,128)} %shard_map.109), calls=%async_computation.1 | async-start | bytes 1048576 | tf_op jit(solution)/shard_map/all_to_all | solution.py:395
  39.7 3.5 %load.1 = (bf16[4096,512]{1,0:T(8,128)(2,1)S(1)}, bf16[4096,512]{1,0:T(8,128)(2,1)S(1)}, f32[768,512]{1,0:T(8,128)S(1)}, f32[768,512]{1,0:T(8,128)S(1)}) custom-call(bf16[384,512]{1,0:T(8,128)(2,1)S(1)} %bitcast.10, bf16[384,512]{1,0:T(8,128)(2,1)S(1)} %collective-permute-done.6.refs_1_, bf16[384,512]{1,0:T(8,128)(2,1)S(1)} %bitcast.14, ...), custom_call_target="tpu_custom_call" | custom-call | tf_op jit(solution)/shard_map/load/pallas_call | solution.py:137
  43.2 4.8 %shard_map.105 = (f32[768,512]{1,0:T(8,128)S(1)}, f32[768,512]{1,0:T(8,128)S(1)}) custom-call(bf16[384,512]{1,0:T(8,128)(2,1)S(1)} %collective-permute-done.refs_0_, bf16[384,512]{1,0:T(8,128)(2,1)} %collective-permute-done.8.refs_1_, bf16[384,512]{1,0:T(8,128)(2,1)S(1)} %collective-permute-done.9.refs_2_, bf16[384,512]{1,0:T(8,128)(2,1)} %collective-permute-done.10.refs_3_, ...), custom_call_target="tpu_custom_call" | custom-call | flops 3221225472 | tf_op jit(solution)/shard_map/pallas_call | solution.py:28
  48.0 5.9 %shard_map.106 = (bf16[4,17,8,128]{3,2,1,0:T(8,128)(2,1)S(1)}, bf16[4,17,8,128]{3,2,1,0:T(8,128)(2,1)S(1)}, bf16[4,17,8,128]{3,2,1,0:T(8,128)(2,1)S(1)}, bf16[4,...) custom-call(bf16[384,512]{1,0:T(8,128)(2,1)} %collective-permute-done.1.refs_0_, ...), custom_call_target="tpu_custom_call" | custom-call | flops 4831838208 | tf_op jit(solution)/shard_map/pallas_call | solution.py:28
  53.9 7.5 %all-to-all-start = ((f32[16,16,128]{2,1,0:T(8,128)}), f32[16,16,128]{2,1,0:T(8,128)S(1)}, u32[]{:S(2)}, u32[]{:S(2)}) async-start(f32[16,16,128]{2,1,0:T(8,128)} %get-tuple-element.40), calls=%async_computation | async-start | bytes 262144 | tf_op jit(solution)/shard_map/all_to_all | solution.py:395
  61.5 7.6 %all-to-all-done.totals_ref = f32[16,16,128]{2,1,0:T(8,128)S(1)} async-done(((f32[16,16,128]{2,1,0:T(8,128)}), f32[16,16,128]{2,1,0:T(8,128)S(1)}, u32[]{:S(2)}, u32[]{:S(2)}) %all-to-all-start) | async-done | bytes 131104 | tf_op jit(solution)/shard_map/all_to_all | solution.py:395
  70.0 4.8 %all-to-all-start.2 = ((f32[16,16,128]{2,1,0:T(8,128)}), f32[16,16,128]{2,1,0:T(8,128)S(1)}, u32[]{:S(2)}, u32[]{:S(2)}) async-start(f32[16,16,128]{2,1,0:T(8,128)} %shard_map.111), calls=%async_computation.2 | async-start | bytes 262144 | tf_op jit(solution)/shard_map/all_to_all | solution.py:395
  74.8 1.5 %collective-permute-start.14 = (bf16[4,17,8,128]{3,2,1,0:T(8,128)(2,1)S(1)}, bf16[4,17,8,128]{3,2,1,0:T(8,128)(2,1)S(1)}, u32[]{:S(2)}, u32[]{:S(2)}) collective-permute-start(bf16[4,17,8,128]{3,2,1,0:T(8,128)(2,1)S(1)} %get-tuple-element.33), channel_id=1, source_target_pairs={{0,8},{8,16},{16,24},{24,0},{32,40},{40,48},{48,56},{56,32},{64,72... | collective-permute-start | bytes 417800 | tf_op jit(solution)/shard_map/ppermute | solution.py:460
  77.2 2.3 %collective-permute-start.16 = (bf16[4,17,8,128]{3,2,1,0:T(8,128)(2,1)S(1)}, bf16[4,17,8,128]{3,2,1,0:T(8,128)(2,1)S(1)}, u32[]{:S(2)}, u32[]{:S(2)}) collective-permute-start(bf16[4,17,8,128]{3,2,1,0:T(8,128)(2,1)S(1)} %get-tuple-element.35), channel_id=1, source_target_pairs={{0,24},{8,0},{16,8},{24,16},{32,56},{40,32},{48,40},{56,48},{64,88... | collective-permute-start | bytes 417800 | tf_op jit(solution)/shard_map/ppermute | solution.py:460
  79.5 2.3 %collective-permute-done.14.refs_1_ = bf16[4,17,8,128]{3,2,1,0:T(8,128)(2,1)S(1)} collective-permute-done((bf16[4,17,8,128]{3,2,1,0:T(8,128)(2,1)S(1)}, bf16[4,17,8,128]{3,2,1,0:T(8,128)(2,1)S(1)}, u32[]{:S(2)}, u32[]{:S(2)}) %collective-permute-start.14) | collective-permute-done | bytes 139296 | tf_op jit(solution)/shard_map/ppermute | solution.py:460
  81.8 2.4 %collective-permute-done.15.refs_2_ = bf16[4,17,8,128]{3,2,1,0:T(8,128)(2,1)S(1)} collective-permute-done((bf16[4,17,8,128]{3,2,1,0:T(8,128)(2,1)S(1)}, bf16[4,17,8,128]{3,2,1,0:T(8,128)(2,1)S(1)}, u32[]{:S(2)}, u32[]{:S(2)}) %collective-permute-start.15) | collective-permute-done | bytes 139296 | tf_op jit(solution)/shard_map/ppermute | solution.py:460
  86.0 1.5 %collective-permute-start.17 = (bf16[17,8,128]{2,1,0:T(8,128)(2,1)S(1)}, bf16[17,8,128]{2,1,0:T(8,128)(2,1)S(1)}, u32[]{:S(2)}, u32[]{:S(2)}) collective-permute-start(bf16[17,8,128]{2,1,0:T(8,128)(2,1)S(1)} %get-tuple-element.37), channel_id=1, source_target_pairs={{0,32},{8,40},{16,48},{24,56},{32,64},{40,72},{48,80},{56,88},{64,... | collective-permute-start | bytes 104456 | tf_op jit(solution)/shard_map/ppermute | solution.py:468
  87.5 2.1 %collective-permute-start.18 = (bf16[17,8,128]{2,1,0:T(8,128)(2,1)S(1)}, bf16[17,8,128]{2,1,0:T(8,128)(2,1)S(1)}, u32[]{:S(2)}, u32[]{:S(2)}) collective-permute-start(bf16[17,8,128]{2,1,0:T(8,128)(2,1)S(1)} %get-tuple-element.38), channel_id=1, source_target_pairs={{0,64},{8,72},{16,80},{24,88},{32,96},{40,104},{48,112},{56,120},{... | collective-permute-start | bytes 104456 | tf_op jit(solution)/shard_map/ppermute | solution.py:468
  89.6 1.6 %collective-permute-start.19 = (bf16[17,8,128]{2,1,0:T(8,128)(2,1)S(1)}, bf16[17,8,128]{2,1,0:T(8,128)(2,1)S(1)}, u32[]{:S(2)}, u32[]{:S(2)}) collective-permute-start(bf16[17,8,128]{2,1,0:T(8,128)(2,1)S(1)} %get-tuple-element.39), channel_id=1, source_target_pairs={{0,96},{8,104},{16,112},{24,120},{32,0},{40,8},{48,16},{56,24},{64... | collective-permute-start | bytes 104456 | tf_op jit(solution)/shard_map/ppermute | solution.py:468
  91.2 1.0 %collective-permute-done.17.refs_1_ = bf16[17,8,128]{2,1,0:T(8,128)(2,1)S(1)} collective-permute-done((bf16[17,8,128]{2,1,0:T(8,128)(2,1)S(1)}, bf16[17,8,128]{2,1,0:T(8,128)(2,1)S(1)}, u32[]{:S(2)}, u32[]{:S(2)}) %collective-permute-start.17) | collective-permute-done | bytes 34848 | tf_op jit(solution)/shard_map/ppermute | solution.py:468
  (43 shorter events, 9.0 us)
Async XLA Ops:
  1.8 6.2 %collective-permute-start.6 = (bf16[384,512]{1,0:T(8,128)(2,1)S(1)}, bf16[384,512]{1,0:T(8,128)(2,1)S(1)}, u32[]{:S(2)}, u32[]{:S(2)}) collective-permute-start(bf16[384,512]{1,0:T(8,128)(2,1)S(1)} %bitcast.7), channel_id=1, source_target_pairs={{0,1},{1,0},{2,3},{3,2},{4,5},{5,4},{6,7},{7,6},{8,9},{9,8},{10,11... | collective-permute-start | bytes 1179656 | tf_op jit(solution)/shard_map/ppermute | solution.py:392
  1.9 12.3 %collective-permute-start.3 = (bf16[384,512]{1,0:T(8,128)(2,1)S(1)}, bf16[384,512]{1,0:T(8,128)(2,1)S(1)}, u32[]{:S(2)}, u32[]{:S(2)}) collective-permute-start(bf16[384,512]{1,0:T(8,128)(2,1)S(1)} %bitcast.11), channel_id=1, source_target_pairs={{0,6},{1,7},{2,0},{3,1},{4,2},{5,3},{6,4},{7,5},{8,14},{9,15},{10,... | collective-permute-start | bytes 1179656 | tf_op jit(solution)/shard_map/ppermute | solution.py:389
  4.7 13.2 %collective-permute-start = (bf16[384,512]{1,0:T(8,128)(2,1)S(1)}, bf16[384,512]{1,0:T(8,128)(2,1)S(1)}, u32[]{:S(2)}, u32[]{:S(2)}) collective-permute-start(bf16[384,512]{1,0:T(8,128)(2,1)S(1)} %bitcast.8), channel_id=1, source_target_pairs={{0,2},{1,3},{2,4},{3,5},{4,6},{5,7},{6,0},{7,1},{8,10},{9,11},{10,... | collective-permute-start | bytes 1179656 | tf_op jit(solution)/shard_map/ppermute | solution.py:389
  4.7 13.2 %collective-permute-start.7 = (bf16[384,512]{1,0:T(8,128)(2,1)S(1)}, bf16[384,512]{1,0:T(8,128)(2,1)S(1)}, u32[]{:S(2)}, u32[]{:S(2)}) collective-permute-start(bf16[384,512]{1,0:T(8,128)(2,1)S(1)} %bitcast.12), channel_id=1, source_target_pairs={{0,1},{1,0},{2,3},{3,2},{4,5},{5,4},{6,7},{7,6},{8,9},{9,8},{10,11... | collective-permute-start | bytes 1179656 | tf_op jit(solution)/shard_map/ppermute | solution.py:392
  4.8 17.8 %collective-permute-start.9 = (bf16[384,512]{1,0:T(8,128)(2,1)S(1)}, bf16[384,512]{1,0:T(8,128)(2,1)S(1)}, u32[]{:S(2)}, u32[]{:S(2)}) collective-permute-start(bf16[384,512]{1,0:T(8,128)(2,1)S(1)} %bitcast.9), channel_id=1, source_target_pairs={{0,6},{1,7},{2,0},{3,1},{4,2},{5,3},{6,4},{7,5},{8,14},{9,15},{10,... | collective-permute-start | bytes 1179656 | tf_op jit(solution)/shard_map/ppermute | solution.py:389
  7.9 18.5 %collective-permute-start.11 = (bf16[384,512]{1,0:T(8,128)(2,1)S(1)}, bf16[384,512]{1,0:T(8,128)(2,1)}, u32[]{:S(2)}, u32[]{:S(2)}) collective-permute-start(bf16[384,512]{1,0:T(8,128)(2,1)S(1)} %bitcast.13), channel_id=1, source_target_pairs={{0,2},{1,3},{2,4},{3,5},{4,6},{5,7},{6,0},{7,1},{8,10},{9,11},{10,... | collective-permute-start | bytes 1179656 | tf_op jit(solution)/shard_map/ppermute | solution.py:389
  14.2 12.2 %collective-permute-start.13 = (bf16[384,512]{1,0:T(8,128)(2,1)S(1)}, bf16[384,512]{1,0:T(8,128)(2,1)S(1)}, u32[]{:S(2)}, u32[]{:S(2)}) collective-permute-start(bf16[384,512]{1,0:T(8,128)(2,1)S(1)} %collective-permute-done.3.refs_6_), channel_id=1, source_target_pairs={{0,1},{1,0},{2,3},{3,2},{4,5},{5,4},{6,7},{7,6},{8,9},{9,8},{10,11... | collective-permute-start | bytes 1179656 | tf_op jit(solution)/shard_map/ppermute | solution.py:392
  17.9 21.1 %collective-permute-start.1 = (bf16[384,512]{1,0:T(8,128)(2,1)S(1)}, bf16[384,512]{1,0:T(8,128)(2,1)}, u32[]{:S(2)}, u32[]{:S(2)}) collective-permute-start(bf16[384,512]{1,0:T(8,128)(2,1)S(1)} %collective-permute-done.refs_0_), channel_id=1, source_target_pairs={{0,2},{1,3},{2,4},{3,5},{4,6},{5,7},{6,0},{7,1},{8,10},{9,11},{10,... | collective-permute-start | bytes 1179656 | tf_op jit(solution)/shard_map/ppermute | solution.py:389
  17.9 21.2 %collective-permute-start.4 = (bf16[384,512]{1,0:T(8,128)(2,1)S(1)}, bf16[384,512]{1,0:T(8,128)(2,1)}, u32[]{:S(2)}, u32[]{:S(2)}) collective-permute-start(bf16[384,512]{1,0:T(8,128)(2,1)S(1)} %collective-permute-done.3.refs_6_), channel_id=1, source_target_pairs={{0,6},{1,7},{2,0},{3,1},{4,2},{5,3},{6,4},{7,5},{8,14},{9,15},{10,... | collective-permute-start | bytes 1179656 | tf_op jit(solution)/shard_map/ppermute | solution.py:389
  22.6 20.5 %collective-permute-start.8 = (bf16[384,512]{1,0:T(8,128)(2,1)S(1)}, bf16[384,512]{1,0:T(8,128)(2,1)}, u32[]{:S(2)}, u32[]{:S(2)}) collective-permute-start(bf16[384,512]{1,0:T(8,128)(2,1)S(1)} %collective-permute-done.refs_0_), channel_id=1, source_target_pairs={{0,1},{1,0},{2,3},{3,2},{4,5},{5,4},{6,7},{7,6},{8,9},{9,8},{10,11... | collective-permute-start | bytes 1179656 | tf_op jit(solution)/shard_map/ppermute | solution.py:392
  26.4 16.7 %collective-permute-start.10 = (bf16[384,512]{1,0:T(8,128)(2,1)S(1)}, bf16[384,512]{1,0:T(8,128)(2,1)}, u32[]{:S(2)}, u32[]{:S(2)}) collective-permute-start(bf16[384,512]{1,0:T(8,128)(2,1)S(1)} %collective-permute-done.9.refs_2_), channel_id=1, source_target_pairs={{0,1},{1,0},{2,3},{3,2},{4,5},{5,4},{6,7},{7,6},{8,9},{9,8},{10,11... | collective-permute-start | bytes 1179656 | tf_op jit(solution)/shard_map/ppermute | solution.py:392
  27.2 15.9 %collective-permute-start.12 = (bf16[384,512]{1,0:T(8,128)(2,1)}, bf16[384,512]{1,0:T(8,128)(2,1)}, u32[]{:S(2)}, u32[]{:S(2)}) collective-permute-start(bf16[384,512]{1,0:T(8,128)(2,1)} %collective-permute-done.11.refs_4_), channel_id=1, source_target_pairs={{0,1},{1,0},{2,3},{3,2},{4,5},{5,4},{6,7},{7,6},{8,9},{9,8},{10,11... | collective-permute-start | bytes 1179656 | tf_op jit(solution)/shard_map/ppermute | solution.py:392
  30.0 23.9 %all-to-all-start.1 = ((f32[16,16,512]{2,1,0:T(8,128)}), f32[16,16,512]{2,1,0:T(8,128)S(1)}, u32[]{:S(2)}, u32[]{:S(2)}) async-start(f32[16,16,512]{2,1,0:T(8,128)} %shard_map.109), calls=%async_computation.1 | async-start | bytes 1048576 | tf_op jit(solution)/shard_map/all_to_all | solution.py:395
  39.1 8.9 %collective-permute-start.2 = (bf16[384,512]{1,0:T(8,128)(2,1)}, bf16[384,512]{1,0:T(8,128)(2,1)S(1)}, u32[]{:S(2)}, u32[]{:S(2)}) collective-permute-start(bf16[384,512]{1,0:T(8,128)(2,1)} %collective-permute-done.1.refs_0_), channel_id=1, source_target_pairs={{0,1},{1,0},{2,3},{3,2},{4,5},{5,4},{6,7},{7,6},{8,9},{9,8},{10,11... | collective-permute-start | bytes 1179656 | tf_op jit(solution)/shard_map/ppermute | solution.py:392
  39.2 8.8 %collective-permute-start.5 = (bf16[384,512]{1,0:T(8,128)(2,1)}, bf16[384,512]{1,0:T(8,128)(2,1)S(1)}, u32[]{:S(2)}, u32[]{:S(2)}) collective-permute-start(bf16[384,512]{1,0:T(8,128)(2,1)} %collective-permute-done.4.refs_2_), channel_id=1, source_target_pairs={{0,1},{1,0},{2,3},{3,2},{4,5},{5,4},{6,7},{7,6},{8,9},{9,8},{10,11... | collective-permute-start | bytes 1179656 | tf_op jit(solution)/shard_map/ppermute | solution.py:392
  48.0 46.4 %copy-start.3 = (f32[128]{0:T(128)S(1)}, f32[128]{0:T(128)}, u32[]{:S(2)}) copy-start(f32[128]{0:T(128)} %param.17) | copy-start | bytes 1540
  53.9 15.2 %all-to-all-start = ((f32[16,16,128]{2,1,0:T(8,128)}), f32[16,16,128]{2,1,0:T(8,128)S(1)}, u32[]{:S(2)}, u32[]{:S(2)}) async-start(f32[16,16,128]{2,1,0:T(8,128)} %get-tuple-element.40), calls=%async_computation | async-start | bytes 262144 | tf_op jit(solution)/shard_map/all_to_all | solution.py:395
  70.0 24.4 %all-to-all-start.2 = ((f32[16,16,128]{2,1,0:T(8,128)}), f32[16,16,128]{2,1,0:T(8,128)S(1)}, u32[]{:S(2)}, u32[]{:S(2)}) async-start(f32[16,16,128]{2,1,0:T(8,128)} %shard_map.111), calls=%async_computation.2 | async-start | bytes 262144 | tf_op jit(solution)/shard_map/all_to_all | solution.py:395
  74.8 7.0 %collective-permute-start.14 = (bf16[4,17,8,128]{3,2,1,0:T(8,128)(2,1)S(1)}, bf16[4,17,8,128]{3,2,1,0:T(8,128)(2,1)S(1)}, u32[]{:S(2)}, u32[]{:S(2)}) collective-permute-start(bf16[4,17,8,128]{3,2,1,0:T(8,128)(2,1)S(1)} %get-tuple-element.33), channel_id=1, source_target_pairs={{0,8},{8,16},{16,24},{24,0},{32,40},{40,48},{48,56},{56,32},{64,72... | collective-permute-start | bytes 417800 | tf_op jit(solution)/shard_map/ppermute | solution.py:460
  76.3 7.9 %collective-permute-start.15 = (bf16[4,17,8,128]{3,2,1,0:T(8,128)(2,1)S(1)}, bf16[4,17,8,128]{3,2,1,0:T(8,128)(2,1)S(1)}, u32[]{:S(2)}, u32[]{:S(2)}) collective-permute-start(bf16[4,17,8,128]{3,2,1,0:T(8,128)(2,1)S(1)} %get-tuple-element.34), channel_id=1, source_target_pairs={{0,16},{8,24},{16,0},{24,8},{32,48},{40,56},{48,32},{56,40},{64,80... | collective-permute-start | bytes 417800 | tf_op jit(solution)/shard_map/ppermute | solution.py:460
  77.2 7.9 %collective-permute-start.16 = (bf16[4,17,8,128]{3,2,1,0:T(8,128)(2,1)S(1)}, bf16[4,17,8,128]{3,2,1,0:T(8,128)(2,1)S(1)}, u32[]{:S(2)}, u32[]{:S(2)}) collective-permute-start(bf16[4,17,8,128]{3,2,1,0:T(8,128)(2,1)S(1)} %get-tuple-element.35), channel_id=1, source_target_pairs={{0,24},{8,0},{16,8},{24,16},{32,56},{40,32},{48,40},{56,48},{64,88... | collective-permute-start | bytes 417800 | tf_op jit(solution)/shard_map/ppermute | solution.py:460
  86.0 6.1 %collective-permute-start.17 = (bf16[17,8,128]{2,1,0:T(8,128)(2,1)S(1)}, bf16[17,8,128]{2,1,0:T(8,128)(2,1)S(1)}, u32[]{:S(2)}, u32[]{:S(2)}) collective-permute-start(bf16[17,8,128]{2,1,0:T(8,128)(2,1)S(1)} %get-tuple-element.37), channel_id=1, source_target_pairs={{0,32},{8,40},{16,48},{24,56},{32,64},{40,72},{48,80},{56,88},{64,... | collective-permute-start | bytes 104456 | tf_op jit(solution)/shard_map/ppermute | solution.py:468
  87.5 5.1 %collective-permute-start.18 = (bf16[17,8,128]{2,1,0:T(8,128)(2,1)S(1)}, bf16[17,8,128]{2,1,0:T(8,128)(2,1)S(1)}, u32[]{:S(2)}, u32[]{:S(2)}) collective-permute-start(bf16[17,8,128]{2,1,0:T(8,128)(2,1)S(1)} %get-tuple-element.38), channel_id=1, source_target_pairs={{0,64},{8,72},{16,80},{24,88},{32,96},{40,104},{48,112},{56,120},{... | collective-permute-start | bytes 104456 | tf_op jit(solution)/shard_map/ppermute | solution.py:468
  89.6 3.9 %collective-permute-start.19 = (bf16[17,8,128]{2,1,0:T(8,128)(2,1)S(1)}, bf16[17,8,128]{2,1,0:T(8,128)(2,1)S(1)}, u32[]{:S(2)}, u32[]{:S(2)}) collective-permute-start(bf16[17,8,128]{2,1,0:T(8,128)(2,1)S(1)} %get-tuple-element.39), channel_id=1, source_target_pairs={{0,96},{8,104},{16,112},{24,120},{32,0},{40,8},{48,16},{56,24},{64... | collective-permute-start | bytes 104456 | tf_op jit(solution)/shard_map/ppermute | solution.py:468
  (4 other events, 14.5 us)

commit v6 on v5

--- a/solution.py
+++ b/solution.py
@@ -146,12 +146,51 @@
     return [pltpu.with_memory_space_constraint(w, pltpu.VMEM) for w in weights], [f, v]
 
 
-def state_kernel(*refs, plan, head_dim):
+def gates(forget, slack):
+    return slack / (1.0 + jnp.exp(forget.astype(F32)))
+
+
+def total_kernel(*refs, plan):
     count = sum(map(len, plan))
     pieces, (wf_ref, wv_ref, f_in, v_in, *refs) = refs[:count], refs[count:]
-    slack_ref, damp_ref, *outs, total_ref, state_ref, f_acc, v_acc, parts_ref = refs
+    slack_ref, damp_ref, f_out, v_out, total_ref, f_acc, v_acc = refs
     add_products(pieces, plan, (wf_ref, wv_ref), (f_in, v_in), (f_acc, v_acc))
-    far, rows = parts_ref.shape[1], parts_ref.shape[3]
+    seqs, heads, length = damp_ref.shape
+    head_dim = total_ref.shape[2]
+    totals = []
+    for s in range(seqs):
+        here = pl.ds(s * length, length)
+        forget = f_acc[here, :].astype(BF)
+        f_out[here, :] = forget
+        v_out[here, :] = v_acc[here, :].astype(BF)
+        decay = jnp.sum(jnp.log(1.0 - gates(forget, slack_ref[...])), axis=0, keepdims=True)
+        damping = jnp.sum(damp_ref[s], axis=1, keepdims=True)
+        for h in range(heads):
+            totals.append(decay[:, h * head_dim : (h + 1) * head_dim] + damping[h : h + 1, :])
+    totals = jnp.concatenate(totals)
+    for p in range(total_ref.shape[0]):
+        total_ref[p] = totals
+
+
+def log_totals(pieces, plan, weights, sums, slack, damp, parts):
+    seqs, heads, _ = damp.shape
+    return in_vmem(
+        functools.partial(total_kernel, plan=plan),
+        [jax.ShapeDtypeStruct(s.shape, BF) for s in sums]
+        + [jax.ShapeDtypeStruct((parts, seqs * heads, weights[0].shape[1] // heads), F32)],
+        *pieces,
+        *weights,
+        *sums,
+        slack,
+        damp,
+        scratch=[pltpu.VMEM(s.shape, F32) for s in sums],
+        flops=12 * len(pieces) * pieces[0].size * weights[0].shape[1],
+    )
+
+
+def state_kernel(forget_ref, value_ref, slack_ref, damp_ref, *refs):
+    *outs, state_ref, parts_ref = refs
+    far, rows, head_dim = parts_ref.shape[1], *parts_ref.shape[3:]
     seqs, heads, length = damp_ref.shape
     channels = heads * head_dim
     tall = length + 8
@@ -166,9 +205,8 @@
     totals = []
     for s in range(seqs):
         here = pl.ds(s * length, length)
-        forget = f_acc[here, :].astype(BF).astype(F32)
-        values = v_acc[here, :].astype(BF)
-        gate = slack_ref[...] / (1.0 + jnp.exp(forget))
+        values = value_ref[here, :]
+        gate = gates(forget_ref[here, :], slack_ref[...])
         high, middle, _ = three_terms(jnp.log(1.0 - gate))
         damping = lax.dot_general(
             later,
@@ -195,10 +233,7 @@
             for y in range(NEAR):
                 parts_ref[y, :, s * heads + h] = blocks[:, y]
     pairs = seqs * heads
-    totals = jnp.concatenate(totals)
-    for p in range(total_ref.shape[0]):
-        total_ref[p] = totals
-    terms = [t.astype(F32) for t in three_terms(totals)]
+    terms = [t.astype(F32) for t in three_terms(jnp.concatenate(totals))]
     packed = jnp.concatenate([*terms, jnp.zeros((head_dim - 3 * pairs, head_dim), F32)])
     blocks = packed.T.astype(BF).reshape(far, NEAR, rows, head_dim)
     for y in range(NEAR):
@@ -208,27 +243,23 @@
         out[...] = parts_ref[lax.rem(near + step, NEAR)]
 
 
-def states(pieces, plan, weights, sums, slack, damp, parts):
+def states(forget, values, slack, damp, parts):
     seqs, heads, _ = damp.shape
-    head_dim = weights[0].shape[1] // heads
+    head_dim = forget.shape[1] // heads
     pairs = seqs * heads
     shape = (parts // NEAR, pairs + 1, head_dim // parts, head_dim)
-    *outs, totals, state = in_vmem(
-        functools.partial(state_kernel, plan=plan, head_dim=head_dim),
+    *outs, state = in_vmem(
+        state_kernel,
         [jax.ShapeDtypeStruct(shape, BF)] * NEAR
-        + [
-            jax.ShapeDtypeStruct((parts, pairs, head_dim), F32),
-            jax.ShapeDtypeStruct((pairs, head_dim, head_dim), BF),
-        ],
-        *pieces,
-        *weights,
-        *sums,
+        + [jax.ShapeDtypeStruct((pairs, head_dim, head_dim), BF)],
+        forget,
+        values,
         slack,
         damp,
-        scratch=[pltpu.VMEM(s.shape, F32) for s in sums] + [pltpu.VMEM((NEAR, *shape), BF)],
-        flops=12 * len(pieces) * pieces[0].size * weights[0].shape[1],
-    )
-    return outs, totals, state
+        scratch=[pltpu.VMEM((NEAR, *shape), BF)],
+        flops=4 * forget.size * head_dim,
+    )
+    return outs, state
 
 
 def unpacked(tile, pairs):
@@ -438,18 +469,21 @@
     weights, sums = load_and_project(
         [own_a, other_a, own_b, other_b], (both(0), both(0)), (forget_weight, value_weight)
     )
-    pieces = [right_a, other_right_a, left_a, other_left_a]
-    pieces += [right_b, other_right_b, left_b, other_left_b]
-    sums = project(pieces, (both(1) + both(-1), both(1) + both(-1)), weights, sums)
-    parts, totals, state = states(
+    pieces = [right_a, other_right_a, left_b, other_left_b]
+    sums = project(pieces, (both(1), both(-1)), weights, sums)
+    pieces = [left_a, other_left_a, right_b, other_right_b]
+    sums = project(pieces, (both(-1), both(1)), weights, sums)
+    damp = additional_damping_exponent.transpose(0, 2, 1)
+    forget, values, totals = log_totals(
         [far_a, other_far_a, far_b, other_far_b],
         (both(2), both(2)),
         weights,
         sums,
         slack,
-        additional_damping_exponent.transpose(0, 2, 1),
+        damp,
         sp_count,
     )
+    parts, state = states(forget, values, slack, damp, sp_count)
 
     planes = sp_count // NEAR
 

time: 95.7 us -> 93.7 us (0.979)
  the two profiles are of different devices: /device:TPU:8 before, /device:TPU:2 now
where the time goes in v6:
time: 93.7 us; the launch traced here: 93 us
  starting transfers between devices  40.1 us (43%)
  waiting for transfers between devices  26.8 us (29%)
  Pallas kernels  22.2 us (24%)
  local copies, waits for them, and re-layouts  3.16 us (3%)
    all_to_all x3, starting transfers between devices, exchange(): return lax.all_to_all(x, 'sp', 0, 0, tiled=True)  18.7 us
    pallas_call x10, Pallas kernels, in_vmem(): pl.pallas_call(kernel, in_specs=in_specs or [VMEM] * len(arrays), out_spe...  17.5 us
    ppermute x6, waiting for transfers between devices, shifted(): return lax.ppermute(x, 'tp', pairs)  12.4 us
    ppermute x6, starting transfers between devices, shifted(): return lax.ppermute(x, 'tp', pairs)  8.8 us
    all_to_all x3, waiting for transfers between devices, exchange(): return lax.all_to_all(x, 'sp', 0, 0, tiled=True)  7.04 us
    ppermute x3, starting transfers between devices, along_y(): return lax.ppermute(parts[step], 'sp', pairs)  5.95 us
    ppermute x3, starting transfers between devices, along_z(): return lax.ppermute(parts[step], 'sp', pairs)  5.29 us
    ppermute x3, waiting for transfers between devices, along_y(): return lax.ppermute(parts[step], 'sp', pairs)  5.1 us
  transfers between devices with their start and end apart: 23, of which 10 were waited for; matrix products, arithmetic and copies ran while one was open for 1% of the time, Pallas kernels for 21%

profile of v6, /device:TPU:2, one launch (start us, length us, event | category | flops | bytes accessed | tf_op | source)
XLA Modules:
  0.0 93.0 jit_solution(887160429058726612)
XLA Ops:
  1.9 1.6 %collective-permute-start = (bf16[384,512]{1,0:T(8,128)(2,1)S(1)}, bf16[384,512]{1,0:T(8,128)(2,1)S(1)}, u32[]{:S(2)}, u32[]{:S(2)}) collective-permute-start(bf16[384,512]{1,0:T(8,128)(2,1)S(1)} %bitcast.8), channel_id=1, source_target_pairs={{0,2},{1,3},{2,4},{3,5},{4,6},{5,7},{6,0},{7,1},{8,10},{9,11},{10,... | collective-permute-start | bytes 1179656 | tf_op jit(solution)/shard_map/ppermute | solution.py:420
  5.6 2.0 %collective-permute-start.8 = (bf16[384,512]{1,0:T(8,128)(2,1)S(1)}, bf16[384,512]{1,0:T(8,128)(2,1)S(1)}, u32[]{:S(2)}, u32[]{:S(2)}) collective-permute-start(bf16[384,512]{1,0:T(8,128)(2,1)S(1)} %bitcast.9), channel_id=1, source_target_pairs={{0,6},{1,7},{2,0},{3,1},{4,2},{5,3},{6,4},{7,5},{8,14},{9,15},{10,... | collective-permute-start | bytes 1179656 | tf_op jit(solution)/shard_map/ppermute | solution.py:420
  7.6 6.6 %collective-permute-done.refs_0_ = bf16[384,512]{1,0:T(8,128)(2,1)S(1)} collective-permute-done((bf16[384,512]{1,0:T(8,128)(2,1)S(1)}, bf16[384,512]{1,0:T(8,128)(2,1)S(1)}, u32[]{:S(2)}, u32[]{:S(2)}) %collective-permute-start) | collective-permute-done | bytes 393248 | tf_op jit(solution)/shard_map/ppermute | solution.py:420
  16.2 2.0 %collective-permute-start.4 = (bf16[384,512]{1,0:T(8,128)(2,1)S(1)}, bf16[384,512]{1,0:T(8,128)(2,1)}, u32[]{:S(2)}, u32[]{:S(2)}) collective-permute-start(bf16[384,512]{1,0:T(8,128)(2,1)S(1)} %collective-permute-done.3.refs_2_), channel_id=1, source_target_pairs={{0,6},{1,7},{2,0},{3,1},{4,2},{5,3},{6,4},{7,5},{8,14},{9,15},{10,... | collective-permute-start | bytes 1179656 | tf_op jit(solution)/shard_map/ppermute | solution.py:420
  18.2 4.4 %collective-permute-done.10.refs_2_ = bf16[384,512]{1,0:T(8,128)(2,1)S(1)} collective-permute-done((bf16[384,512]{1,0:T(8,128)(2,1)S(1)}, bf16[384,512]{1,0:T(8,128)(2,1)S(1)}, u32[]{:S(2)}, u32[]{:S(2)}) %collective-permute-start.10) | collective-permute-done | bytes 393248 | tf_op jit(solution)/shard_map/ppermute | solution.py:420
  22.6 1.4 %collective-permute-done.8.refs_0_ = bf16[384,512]{1,0:T(8,128)(2,1)S(1)} collective-permute-done((bf16[384,512]{1,0:T(8,128)(2,1)S(1)}, bf16[384,512]{1,0:T(8,128)(2,1)S(1)}, u32[]{:S(2)}, u32[]{:S(2)}) %collective-permute-start.8) | collective-permute-done | bytes 393248 | tf_op jit(solution)/shard_map/ppermute | solution.py:420
  25.3 2.3 %shard_map.111 = f32[16,16,512]{2,1,0:T(8,128)} custom-call(bf16[4,256]{1,0:T(4,128)(2,1)} %x_ref.1, bf16[256,512]{1,0:T(8,128)(2,1)} %q_hbm.1, bf16[256,512]{1,0:T(8,128)(2,1)} %g_hbm.1, bf16[4096,512]{1,0:T(8,128)(2,1)} %f_hbm.1, bf16[4096,512]{1,0:T(8,128)(2,1)} %v_hbm.1), custom_call_target="tpu_custom_call" | custom-call | tf_op jit(solution)/shard_map/pallas_call | solution.py:28
  27.6 8.6 %all-to-all-start.1 = ((f32[16,16,512]{2,1,0:T(8,128)}), f32[16,16,512]{2,1,0:T(8,128)S(1)}, u32[]{:S(2)}, u32[]{:S(2)}) async-start(f32[16,16,512]{2,1,0:T(8,128)} %shard_map.111), calls=%async_computation.1 | async-start | bytes 1048576 | tf_op jit(solution)/shard_map/all_to_all | solution.py:426
  37.8 3.5 %load.1 = (bf16[4096,512]{1,0:T(8,128)(2,1)S(1)}, bf16[4096,512]{1,0:T(8,128)(2,1)S(1)}, f32[768,512]{1,0:T(8,128)S(1)}, f32[768,512]{1,0:T(8,128)S(1)}) custom-call(bf16[384,512]{1,0:T(8,128)(2,1)S(1)} %bitcast.10, bf16[384,512]{1,0:T(8,128)(2,1)S(1)} %collective-permute-done.6.refs_1_, bf16[384,512]{1,0:T(8,128)(2,1)S(1)} %bitcast.14, ...), custom_call_target="tpu_custom_call" | custom-call | tf_op jit(solution)/shard_map/load/pallas_call | solution.py:137
  41.4 2.8 %shard_map.105 = (f32[768,512]{1,0:T(8,128)S(1)}, f32[768,512]{1,0:T(8,128)S(1)}) custom-call(bf16[384,512]{1,0:T(8,128)(2,1)S(1)} %collective-permute-done.refs_0_, bf16[384,512]{1,0:T(8,128)(2,1)S(1)} %copy-done.3, bf16[384,512]{1,0:T(8,128)(2,1)S(1)} %collective-permute-done.3.refs_2_, bf16[384,512]{1,0:T(8,128)(2,1)} %collective-permute-done.13.refs_3_, ...), custom_call_target="tpu_custom_call" | custom-call | flops 1610612736 | tf_op jit(solution)/shard_map/pallas_call | solution.py:28
  44.2 2.9 %shard_map.106 = (f32[768,512]{1,0:T(8,128)S(1)}, f32[768,512]{1,0:T(8,128)S(1)}) custom-call(bf16[384,512]{1,0:T(8,128)(2,1)S(1)} %collective-permute-done.8.refs_0_, bf16[384,512]{1,0:T(8,128)(2,1)} %collective-permute-done.9.refs_1_, bf16[384,512]{1,0:T(8,128)(2,1)S(1)} %collective-permute-done.10.refs_2_, ...), custom_call_target="tpu_custom_call" | custom-call | flops 1610612736 | tf_op jit(solution)/shard_map/pallas_call | solution.py:28
  47.2 3.6 %shard_map.107 = (bf16[768,512]{1,0:T(8,128)(2,1)S(1)}, bf16[768,512]{1,0:T(8,128)(2,1)S(1)}, f32[16,16,128]{2,1,0:T(8,128)}) custom-call(bf16[384,512]{1,0:T(8,128)(2,1)} %collective-permute-done.1.refs_0_, bf16[384,512]{1,0:T(8,128)(2,1)S(1)} %collective-permute-done.2.refs_1_, bf16[384,512]{1,0:T(8,128)(2,1)} %collective-permute-done.4.refs_2_, ...), custom_call_target="tpu_custom_call" | custom-call | flops 4831838208 | tf_op jit(solution)/shard_map/pallas_call | solution.py:28
  51.8 6.5 %all-to-all-start = ((f32[16,16,128]{2,1,0:T(8,128)}), f32[16,16,128]{2,1,0:T(8,128)S(1)}, u32[]{:S(2)}, u32[]{:S(2)}) async-start(f32[16,16,128]{2,1,0:T(8,128)} %get-tuple-element.48), calls=%async_computation | async-start | bytes 262144 | tf_op jit(solution)/shard_map/all_to_all | solution.py:426
  58.4 2.9 %shard_map.108 = (bf16[4,17,8,128]{3,2,1,0:T(8,128)(2,1)S(1)}, bf16[4,17,8,128]{3,2,1,0:T(8,128)(2,1)S(1)}, bf16[4,17,8,128]{3,2,1,0:T(8,128)(2,1)S(1)}, bf16[4,...) custom-call(bf16[768,512]{1,0:T(8,128)(2,1)S(1)} %get-tuple-element.38.forget_ref, ...), custom_call_target="tpu_custom_call" | custom-call | flops 201326592 | tf_op jit(solution)/shard_map/pallas_call | solution.py:28
  61.3 6.1 %all-to-all-done.totals_ref = f32[16,16,128]{2,1,0:T(8,128)S(1)} async-done(((f32[16,16,128]{2,1,0:T(8,128)}), f32[16,16,128]{2,1,0:T(8,128)S(1)}, u32[]{:S(2)}, u32[]{:S(2)}) %all-to-all-start) | async-done | bytes 131104 | tf_op jit(solution)/shard_map/all_to_all | solution.py:426
  68.3 3.5 %all-to-all-start.2 = ((f32[16,16,128]{2,1,0:T(8,128)}), f32[16,16,128]{2,1,0:T(8,128)S(1)}, u32[]{:S(2)}, u32[]{:S(2)}) async-start(f32[16,16,128]{2,1,0:T(8,128)} %shard_map.113), calls=%async_computation.2 | async-start | bytes 262144 | tf_op jit(solution)/shard_map/all_to_all | solution.py:426
  71.8 1.8 %collective-permute-start.14 = (bf16[4,17,8,128]{3,2,1,0:T(8,128)(2,1)S(1)}, bf16[4,17,8,128]{3,2,1,0:T(8,128)(2,1)S(1)}, u32[]{:S(2)}, u32[]{:S(2)}) collective-permute-start(bf16[4,17,8,128]{3,2,1,0:T(8,128)(2,1)S(1)} %get-tuple-element.41), channel_id=1, source_target_pairs={{0,8},{8,16},{16,24},{24,0},{32,40},{40,48},{48,56},{56,32},{64,72... | collective-permute-start | bytes 417800 | tf_op jit(solution)/shard_map/ppermute | solution.py:494
  73.6 2.7 %collective-permute-start.15 = (bf16[4,17,8,128]{3,2,1,0:T(8,128)(2,1)S(1)}, bf16[4,17,8,128]{3,2,1,0:T(8,128)(2,1)S(1)}, u32[]{:S(2)}, u32[]{:S(2)}) collective-permute-start(bf16[4,17,8,128]{3,2,1,0:T(8,128)(2,1)S(1)} %get-tuple-element.42), channel_id=1, source_target_pairs={{0,16},{8,24},{16,0},{24,8},{32,48},{40,56},{48,32},{56,40},{64,80... | collective-permute-start | bytes 417800 | tf_op jit(solution)/shard_map/ppermute | solution.py:494
  76.3 1.5 %collective-permute-start.16 = (bf16[4,17,8,128]{3,2,1,0:T(8,128)(2,1)S(1)}, bf16[4,17,8,128]{3,2,1,0:T(8,128)(2,1)S(1)}, u32[]{:S(2)}, u32[]{:S(2)}) collective-permute-start(bf16[4,17,8,128]{3,2,1,0:T(8,128)(2,1)S(1)} %get-tuple-element.43), channel_id=1, source_target_pairs={{0,24},{8,0},{16,8},{24,16},{32,56},{40,32},{48,40},{56,48},{64,88... | collective-permute-start | bytes 417800 | tf_op jit(solution)/shard_map/ppermute | solution.py:494
  77.8 2.3 %collective-permute-done.14.refs_1_ = bf16[4,17,8,128]{3,2,1,0:T(8,128)(2,1)S(1)} collective-permute-done((bf16[4,17,8,128]{3,2,1,0:T(8,128)(2,1)S(1)}, bf16[4,17,8,128]{3,2,1,0:T(8,128)(2,1)S(1)}, u32[]{:S(2)}, u32[]{:S(2)}) %collective-permute-start.14) | collective-permute-done | bytes 139296 | tf_op jit(solution)/shard_map/ppermute | solution.py:494
  80.0 2.8 %collective-permute-done.15.refs_2_ = bf16[4,17,8,128]{3,2,1,0:T(8,128)(2,1)S(1)} collective-permute-done((bf16[4,17,8,128]{3,2,1,0:T(8,128)(2,1)S(1)}, bf16[4,17,8,128]{3,2,1,0:T(8,128)(2,1)S(1)}, u32[]{:S(2)}, u32[]{:S(2)}) %collective-permute-start.15) | collective-permute-done | bytes 139296 | tf_op jit(solution)/shard_map/ppermute | solution.py:494
  83.8 1.5 %collective-permute-start.17 = (bf16[17,8,128]{2,1,0:T(8,128)(2,1)S(1)}, bf16[17,8,128]{2,1,0:T(8,128)(2,1)S(1)}, u32[]{:S(2)}, u32[]{:S(2)}) collective-permute-start(bf16[17,8,128]{2,1,0:T(8,128)(2,1)S(1)} %get-tuple-element.45), channel_id=1, source_target_pairs={{0,32},{8,40},{16,48},{24,56},{32,64},{40,72},{48,80},{56,88},{64,... | collective-permute-start | bytes 104456 | tf_op jit(solution)/shard_map/ppermute | solution.py:502
  85.3 2.1 %collective-permute-start.18 = (bf16[17,8,128]{2,1,0:T(8,128)(2,1)S(1)}, bf16[17,8,128]{2,1,0:T(8,128)(2,1)S(1)}, u32[]{:S(2)}, u32[]{:S(2)}) collective-permute-start(bf16[17,8,128]{2,1,0:T(8,128)(2,1)S(1)} %get-tuple-element.46), channel_id=1, source_target_pairs={{0,64},{8,72},{16,80},{24,88},{32,96},{40,104},{48,112},{56,120},{... | collective-permute-start | bytes 104456 | tf_op jit(solution)/shard_map/ppermute | solution.py:502
  87.4 1.7 %collective-permute-start.19 = (bf16[17,8,128]{2,1,0:T(8,128)(2,1)S(1)}, bf16[17,8,128]{2,1,0:T(8,128)(2,1)S(1)}, u32[]{:S(2)}, u32[]{:S(2)}) collective-permute-start(bf16[17,8,128]{2,1,0:T(8,128)(2,1)S(1)} %get-tuple-element.47), channel_id=1, source_target_pairs={{0,96},{8,104},{16,112},{24,120},{32,0},{40,8},{48,16},{56,24},{64... | collective-permute-start | bytes 104456 | tf_op jit(solution)/shard_map/ppermute | solution.py:502
  (49 shorter events, 15.2 us)
Async XLA Ops:
  1.8 3.8 %collective-permute-start.6 = (bf16[384,512]{1,0:T(8,128)(2,1)S(1)}, bf16[384,512]{1,0:T(8,128)(2,1)S(1)}, u32[]{:S(2)}, u32[]{:S(2)}) collective-permute-start(bf16[384,512]{1,0:T(8,128)(2,1)S(1)} %bitcast.7), channel_id=1, source_target_pairs={{0,1},{1,0},{2,3},{3,2},{4,5},{5,4},{6,7},{7,6},{8,9},{9,8},{10,11... | collective-permute-start | bytes 1179656 | tf_op jit(solution)/shard_map/ppermute | solution.py:423
  1.9 12.3 %collective-permute-start = (bf16[384,512]{1,0:T(8,128)(2,1)S(1)}, bf16[384,512]{1,0:T(8,128)(2,1)S(1)}, u32[]{:S(2)}, u32[]{:S(2)}) collective-permute-start(bf16[384,512]{1,0:T(8,128)(2,1)S(1)} %bitcast.8), channel_id=1, source_target_pairs={{0,2},{1,3},{2,4},{3,5},{4,6},{5,7},{6,0},{7,1},{8,10},{9,11},{10,... | collective-permute-start | bytes 1179656 | tf_op jit(solution)/shard_map/ppermute | solution.py:420
  3.4 10.7 %collective-permute-start.7 = (bf16[384,512]{1,0:T(8,128)(2,1)S(1)}, bf16[384,512]{1,0:T(8,128)(2,1)S(1)}, u32[]{:S(2)}, u32[]{:S(2)}) collective-permute-start(bf16[384,512]{1,0:T(8,128)(2,1)S(1)} %bitcast.11), channel_id=1, source_target_pairs={{0,1},{1,0},{2,3},{3,2},{4,5},{5,4},{6,7},{7,6},{8,9},{9,8},{10,11... | collective-permute-start | bytes 1179656 | tf_op jit(solution)/shard_map/ppermute | solution.py:423
  3.6 12.6 %collective-permute-start.3 = (bf16[384,512]{1,0:T(8,128)(2,1)S(1)}, bf16[384,512]{1,0:T(8,128)(2,1)S(1)}, u32[]{:S(2)}, u32[]{:S(2)}) collective-permute-start(bf16[384,512]{1,0:T(8,128)(2,1)S(1)} %bitcast.12), channel_id=1, source_target_pairs={{0,6},{1,7},{2,0},{3,1},{4,2},{5,3},{6,4},{7,5},{8,14},{9,15},{10,... | collective-permute-start | bytes 1179656 | tf_op jit(solution)/shard_map/ppermute | solution.py:420
  4.6 18.0 %collective-permute-start.10 = (bf16[384,512]{1,0:T(8,128)(2,1)S(1)}, bf16[384,512]{1,0:T(8,128)(2,1)S(1)}, u32[]{:S(2)}, u32[]{:S(2)}) collective-permute-start(bf16[384,512]{1,0:T(8,128)(2,1)S(1)} %bitcast.13), channel_id=1, source_target_pairs={{0,2},{1,3},{2,4},{3,5},{4,6},{5,7},{6,0},{7,1},{8,10},{9,11},{10,... | collective-permute-start | bytes 1179656 | tf_op jit(solution)/shard_map/ppermute | solution.py:420
  5.6 18.4 %collective-permute-start.8 = (bf16[384,512]{1,0:T(8,128)(2,1)S(1)}, bf16[384,512]{1,0:T(8,128)(2,1)S(1)}, u32[]{:S(2)}, u32[]{:S(2)}) collective-permute-start(bf16[384,512]{1,0:T(8,128)(2,1)S(1)} %bitcast.9), channel_id=1, source_target_pairs={{0,6},{1,7},{2,0},{3,1},{4,2},{5,3},{6,4},{7,5},{8,14},{9,15},{10,... | collective-permute-start | bytes 1179656 | tf_op jit(solution)/shard_map/ppermute | solution.py:420
  14.2 9.8 %collective-permute-start.12 = (bf16[384,512]{1,0:T(8,128)(2,1)S(1)}, bf16[384,512]{1,0:T(8,128)(2,1)S(1)}, u32[]{:S(2)}, u32[]{:S(2)}) collective-permute-start(bf16[384,512]{1,0:T(8,128)(2,1)S(1)} %collective-permute-done.refs_0_), channel_id=1, source_target_pairs={{0,1},{1,0},{2,3},{3,2},{4,5},{5,4},{6,7},{7,6},{8,9},{9,8},{10,11... | collective-permute-start | bytes 1179656 | tf_op jit(solution)/shard_map/ppermute | solution.py:423
  14.9 21.3 %collective-permute-start.1 = (bf16[384,512]{1,0:T(8,128)(2,1)S(1)}, bf16[384,512]{1,0:T(8,128)(2,1)}, u32[]{:S(2)}, u32[]{:S(2)}) collective-permute-start(bf16[384,512]{1,0:T(8,128)(2,1)S(1)} %collective-permute-done.refs_0_), channel_id=1, source_target_pairs={{0,2},{1,3},{2,4},{3,5},{4,6},{5,7},{6,0},{7,1},{8,10},{9,11},{10,... | collective-permute-start | bytes 1179656 | tf_op jit(solution)/shard_map/ppermute | solution.py:420
  16.2 20.1 %collective-permute-start.4 = (bf16[384,512]{1,0:T(8,128)(2,1)S(1)}, bf16[384,512]{1,0:T(8,128)(2,1)}, u32[]{:S(2)}, u32[]{:S(2)}) collective-permute-start(bf16[384,512]{1,0:T(8,128)(2,1)S(1)} %collective-permute-done.3.refs_2_), channel_id=1, source_target_pairs={{0,6},{1,7},{2,0},{3,1},{4,2},{5,3},{6,4},{7,5},{8,14},{9,15},{10,... | collective-permute-start | bytes 1179656 | tf_op jit(solution)/shard_map/ppermute | solution.py:420
  22.6 18.8 %collective-permute-start.13 = (bf16[384,512]{1,0:T(8,128)(2,1)S(1)}, bf16[384,512]{1,0:T(8,128)(2,1)}, u32[]{:S(2)}, u32[]{:S(2)}) collective-permute-start(bf16[384,512]{1,0:T(8,128)(2,1)S(1)} %collective-permute-done.3.refs_2_), channel_id=1, source_target_pairs={{0,1},{1,0},{2,3},{3,2},{4,5},{5,4},{6,7},{7,6},{8,9},{9,8},{10,11... | collective-permute-start | bytes 1179656 | tf_op jit(solution)/shard_map/ppermute | solution.py:423
  24.0 20.2 %collective-permute-start.11 = (bf16[384,512]{1,0:T(8,128)(2,1)S(1)}, bf16[384,512]{1,0:T(8,128)(2,1)}, u32[]{:S(2)}, u32[]{:S(2)}) collective-permute-start(bf16[384,512]{1,0:T(8,128)(2,1)S(1)} %collective-permute-done.10.refs_2_), channel_id=1, source_target_pairs={{0,1},{1,0},{2,3},{3,2},{4,5},{5,4},{6,7},{7,6},{8,9},{9,8},{10,11... | collective-permute-start | bytes 1179656 | tf_op jit(solution)/shard_map/ppermute | solution.py:423
  24.7 19.4 %collective-permute-start.9 = (bf16[384,512]{1,0:T(8,128)(2,1)S(1)}, bf16[384,512]{1,0:T(8,128)(2,1)}, u32[]{:S(2)}, u32[]{:S(2)}) collective-permute-start(bf16[384,512]{1,0:T(8,128)(2,1)S(1)} %collective-permute-done.8.refs_0_), channel_id=1, source_target_pairs={{0,1},{1,0},{2,3},{3,2},{4,5},{5,4},{6,7},{7,6},{8,9},{9,8},{10,11... | collective-permute-start | bytes 1179656 | tf_op jit(solution)/shard_map/ppermute | solution.py:423
  27.6 24.2 %all-to-all-start.1 = ((f32[16,16,512]{2,1,0:T(8,128)}), f32[16,16,512]{2,1,0:T(8,128)S(1)}, u32[]{:S(2)}, u32[]{:S(2)}) async-start(f32[16,16,512]{2,1,0:T(8,128)} %shard_map.111), calls=%async_computation.1 | async-start | bytes 1048576 | tf_op jit(solution)/shard_map/all_to_all | solution.py:426
  36.2 10.9 %collective-permute-start.2 = (bf16[384,512]{1,0:T(8,128)(2,1)}, bf16[384,512]{1,0:T(8,128)(2,1)S(1)}, u32[]{:S(2)}, u32[]{:S(2)}) collective-permute-start(bf16[384,512]{1,0:T(8,128)(2,1)} %collective-permute-done.1.refs_0_), channel_id=1, source_target_pairs={{0,1},{1,0},{2,3},{3,2},{4,5},{5,4},{6,7},{7,6},{8,9},{9,8},{10,11... | collective-permute-start | bytes 1179656 | tf_op jit(solution)/shard_map/ppermute | solution.py:423
  36.3 10.8 %collective-permute-start.5 = (bf16[384,512]{1,0:T(8,128)(2,1)}, bf16[384,512]{1,0:T(8,128)(2,1)S(1)}, u32[]{:S(2)}, u32[]{:S(2)}) collective-permute-start(bf16[384,512]{1,0:T(8,128)(2,1)} %collective-permute-done.4.refs_2_), channel_id=1, source_target_pairs={{0,1},{1,0},{2,3},{3,2},{4,5},{5,4},{6,7},{7,6},{8,9},{9,8},{10,11... | collective-permute-start | bytes 1179656 | tf_op jit(solution)/shard_map/ppermute | solution.py:423
  51.8 15.6 %all-to-all-start = ((f32[16,16,128]{2,1,0:T(8,128)}), f32[16,16,128]{2,1,0:T(8,128)S(1)}, u32[]{:S(2)}, u32[]{:S(2)}) async-start(f32[16,16,128]{2,1,0:T(8,128)} %get-tuple-element.48), calls=%async_computation | async-start | bytes 262144 | tf_op jit(solution)/shard_map/all_to_all | solution.py:426
  58.4 33.9 %copy-start.6 = (f32[128]{0:T(128)S(1)}, f32[128]{0:T(128)}, u32[]{:S(2)}) copy-start(f32[128]{0:T(128)} %param.17) | copy-start | bytes 1540
  68.3 23.9 %all-to-all-start.2 = ((f32[16,16,128]{2,1,0:T(8,128)}), f32[16,16,128]{2,1,0:T(8,128)S(1)}, u32[]{:S(2)}, u32[]{:S(2)}) async-start(f32[16,16,128]{2,1,0:T(8,128)} %shard_map.113), calls=%async_computation.2 | async-start | bytes 262144 | tf_op jit(solution)/shard_map/all_to_all | solution.py:426
  71.8 8.2 %collective-permute-start.14 = (bf16[4,17,8,128]{3,2,1,0:T(8,128)(2,1)S(1)}, bf16[4,17,8,128]{3,2,1,0:T(8,128)(2,1)S(1)}, u32[]{:S(2)}, u32[]{:S(2)}) collective-permute-start(bf16[4,17,8,128]{3,2,1,0:T(8,128)(2,1)S(1)} %get-tuple-element.41), channel_id=1, source_target_pairs={{0,8},{8,16},{16,24},{24,0},{32,40},{40,48},{48,56},{56,32},{64,72... | collective-permute-start | bytes 417800 | tf_op jit(solution)/shard_map/ppermute | solution.py:494
  73.6 9.2 %collective-permute-start.15 = (bf16[4,17,8,128]{3,2,1,0:T(8,128)(2,1)S(1)}, bf16[4,17,8,128]{3,2,1,0:T(8,128)(2,1)S(1)}, u32[]{:S(2)}, u32[]{:S(2)}) collective-permute-start(bf16[4,17,8,128]{3,2,1,0:T(8,128)(2,1)S(1)} %get-tuple-element.42), channel_id=1, source_target_pairs={{0,16},{8,24},{16,0},{24,8},{32,48},{40,56},{48,32},{56,40},{64,80... | collective-permute-start | bytes 417800 | tf_op jit(solution)/shard_map/ppermute | solution.py:494
  76.3 6.6 %collective-permute-start.16 = (bf16[4,17,8,128]{3,2,1,0:T(8,128)(2,1)S(1)}, bf16[4,17,8,128]{3,2,1,0:T(8,128)(2,1)S(1)}, u32[]{:S(2)}, u32[]{:S(2)}) collective-permute-start(bf16[4,17,8,128]{3,2,1,0:T(8,128)(2,1)S(1)} %get-tuple-element.43), channel_id=1, source_target_pairs={{0,24},{8,0},{16,8},{24,16},{32,56},{40,32},{48,40},{56,48},{64,88... | collective-permute-start | bytes 417800 | tf_op jit(solution)/shard_map/ppermute | solution.py:494
  83.8 5.8 %collective-permute-start.17 = (bf16[17,8,128]{2,1,0:T(8,128)(2,1)S(1)}, bf16[17,8,128]{2,1,0:T(8,128)(2,1)S(1)}, u32[]{:S(2)}, u32[]{:S(2)}) collective-permute-start(bf16[17,8,128]{2,1,0:T(8,128)(2,1)S(1)} %get-tuple-element.45), channel_id=1, source_target_pairs={{0,32},{8,40},{16,48},{24,56},{32,64},{40,72},{48,80},{56,88},{64,... | collective-permute-start | bytes 104456 | tf_op jit(solution)/shard_map/ppermute | solution.py:502
  85.3 4.8 %collective-permute-start.18 = (bf16[17,8,128]{2,1,0:T(8,128)(2,1)S(1)}, bf16[17,8,128]{2,1,0:T(8,128)(2,1)S(1)}, u32[]{:S(2)}, u32[]{:S(2)}) collective-permute-start(bf16[17,8,128]{2,1,0:T(8,128)(2,1)S(1)} %get-tuple-element.46), channel_id=1, source_target_pairs={{0,64},{8,72},{16,80},{24,88},{32,96},{40,104},{48,112},{56,120},{... | collective-permute-start | bytes 104456 | tf_op jit(solution)/shard_map/ppermute | solution.py:502
  87.4 3.9 %collective-permute-start.19 = (bf16[17,8,128]{2,1,0:T(8,128)(2,1)S(1)}, bf16[17,8,128]{2,1,0:T(8,128)(2,1)S(1)}, u32[]{:S(2)}, u32[]{:S(2)}) collective-permute-start(bf16[17,8,128]{2,1,0:T(8,128)(2,1)S(1)} %get-tuple-element.47), channel_id=1, source_target_pairs={{0,96},{8,104},{16,112},{24,120},{32,0},{40,8},{48,16},{56,24},{64... | collective-permute-start | bytes 104456 | tf_op jit(solution)/shard_map/ppermute | solution.py:502
  (6 other events, 12.0 us)

commit v7 on v6

--- a/solution.py
+++ b/solution.py
@@ -109,40 +109,37 @@
     )
 
 
-def load_kernel(*refs, plan):
-    count = sum(map(len, plan))
-    pieces, (wf_hbm, wv_hbm, wf_ref, wv_ref, *outs, sems) = refs[:count], refs[count:]
+def load_kernel(own_hbm, other_hbm, wf_hbm, wv_hbm, *refs, plan):
+    wf_ref, wv_ref, *outs, own_ref, other_ref, sems = refs
     chips = lax.axis_size("tp") // 2
     depth = wf_ref.shape[0] // chips
     chip = lax.axis_index("tp") // 2
-    copies = []
+    pairs = [(own_hbm, own_ref), (other_hbm, other_ref)]
     for step in range(chips):
         here = pl.ds(pl.multiple_of(lax.rem(chip + step, chips) * depth, depth), depth)
-        for n, (source, target) in enumerate(((wf_hbm, wf_ref), (wv_hbm, wv_ref))):
-            copies.append(
-                pltpu.make_async_copy(source.at[here], target.at[here], sems.at[2 * step + n])
-            )
+        pairs += [(wf_hbm.at[here], wf_ref.at[here]), (wv_hbm.at[here], wv_ref.at[here])]
+    copies = [pltpu.make_async_copy(*pair, sems.at[n]) for n, pair in enumerate(pairs)]
     for copy in copies:
         copy.start()
-    for copy in copies[:2]:
+    for copy in copies[:4]:
         copy.wait()
-    add_products(pieces, plan, (wf_ref, wv_ref), (), outs)
-    for copy in copies[2:]:
+    add_products((own_ref, other_ref), plan, (wf_ref, wv_ref), (), outs)
+    for copy in copies[4:]:
         copy.wait()
 
 
-def load_and_project(pieces, plan, weights):
-    rows = len(plan) * pieces[0].shape[0]
-    out = jax.ShapeDtypeStruct((rows, weights[0].shape[1]), F32)
+def load_and_project(own, other, plan, weights):
+    out = jax.ShapeDtypeStruct((own.shape[0], weights[0].shape[1]), F32)
     *weights, f, v = pl.pallas_call(
         functools.partial(load_kernel, plan=plan),
-        in_specs=[VMEM] * len(pieces) + [pl.BlockSpec(memory_space=pltpu.HBM)] * 2,
+        in_specs=[pl.BlockSpec(memory_space=pltpu.HBM)] * 4,
         out_specs=[VMEM] * 4,
         out_shape=[pltpu.VMEM(w.shape, BF) for w in weights] + [out] * 2,
-        scratch_shapes=[pltpu.SemaphoreType.DMA((lax.axis_size("tp"),))],
+        scratch_shapes=[pltpu.VMEM(own.shape, BF)] * 2
+        + [pltpu.SemaphoreType.DMA((lax.axis_size("tp") + 2,))],
         compiler_params=pltpu.CompilerParams(vmem_limit_bytes=12 << 20),
         name="load",
-    )(*pieces, *(pltpu.with_memory_space_constraint(w, pltpu.HBM) for w in weights))
+    )(*(pltpu.with_memory_space_constraint(x, pltpu.HBM) for x in (own, other, *weights)))
     return [pltpu.with_memory_space_constraint(w, pltpu.VMEM) for w in weights], [f, v]
 
 
@@ -426,10 +423,11 @@
         return lax.all_to_all(x, "sp", 0, 0, tiled=True)
 
     rows = seqs // 2 * length
+    own = tokens.reshape(seqs * length, width)
+    other = sibling(own)
     own_a, own_b = (x.reshape(rows, width) for x in split(tokens, 2))
     right_a, left_a = shifted(own_a, 1), shifted(own_a, -1)
     right_b, left_b = shifted(own_b, 1), shifted(own_b, -1)
-    other_a, other_b = sibling(own_a), sibling(own_b)
 
     partial = in_vmem(
         new_token_kernel,
@@ -467,7 +465,7 @@
         return ((by, False), (by, True))
 
     weights, sums = load_and_project(
-        [own_a, other_a, own_b, other_b], (both(0), both(0)), (forget_weight, value_weight)
+        own, other, (both(0),), (forget_weight, value_weight)
     )
     pieces = [right_a, other_right_a, left_b, other_left_b]
     sums = project(pieces, (both(1), both(-1)), weights, sums)

time: 93.7 us -> 92.5 us (0.987)
  waiting for transfers between devices: 26.8 us -> 29.9 us
  local copies, waits for them, and re-layouts: 3.16 us -> 1.02 us
  starting transfers between devices: 40.1 us -> 38.3 us
    all_to_all x3, starting transfers between devices: 18.7 us -> 15.3 us  [exchange(): return lax.all_to_all(x, 'sp', 0, 0, tiled=True)]
    unnamed x15 -> x9, local copies, waits for them, and re-layouts: 3.16 us -> 1.02 us
    all_to_all x3, waiting for transfers between devices: 7.04 us -> 8.75 us  [exchange(): return lax.all_to_all(x, 'sp', 0, 0, tiled=True)]
    ppermute x6, waiting for transfers between devices: 12.4 us -> 13.8 us  [shifted(): return lax.ppermute(x, 'tp', pairs)]
    ppermute x6, starting transfers between devices: 8.8 us -> 10.1 us  [shifted(): return lax.ppermute(x, 'tp', pairs)]
    pallas_call x10, Pallas kernels: 17.5 us -> 16.4 us  [in_vmem(): pl.pallas_call(kernel, in_specs=in_specs or [VMEM] * len(arrays), out_spe...]
  transfers between devices with their start and end apart: 23 -> 22, of which waited for: 10 -> 10; matrix products, arithmetic and copies ran while one was open for 1% -> 1% of each run, Pallas kernels for 21% -> 22%
where the time goes in v7:
time: 92.5 us; the launch traced here: 91.6 us
  starting transfers between devices  38.3 us (41%)
  waiting for transfers between devices  29.9 us (32%)
  Pallas kernels  21.5 us (23%)
  local copies, waits for them, and re-layouts  1.02 us (1%)
    pallas_call x10, Pallas kernels, in_vmem(): pl.pallas_call(kernel, in_specs=in_specs or [VMEM] * len(arrays), out_spe...  16.4 us
    all_to_all x3, starting transfers between devices, exchange(): return lax.all_to_all(x, 'sp', 0, 0, tiled=True)  15.3 us
    ppermute x6, waiting for transfers between devices, shifted(): return lax.ppermute(x, 'tp', pairs)  13.8 us
    ppermute x6, starting transfers between devices, shifted(): return lax.ppermute(x, 'tp', pairs)  10.1 us
    all_to_all x3, waiting for transfers between devices, exchange(): return lax.all_to_all(x, 'sp', 0, 0, tiled=True)  8.75 us
    ppermute x3, starting transfers between devices, along_y(): return lax.ppermute(parts[step], 'sp', pairs)  5.95 us
    ppermute x3, starting transfers between devices, along_z(): return lax.ppermute(parts[step], 'sp', pairs)  5.29 us
    ppermute x3, waiting for transfers between devices, along_y(): return lax.ppermute(parts[step], 'sp', pairs)  5.1 us
  transfers between devices with their start and end apart: 22, of which 10 were waited for; matrix products, arithmetic and copies ran while one was open for 1% of the time, Pallas kernels for 22%

profile of v7, /device:TPU:2, one launch (start us, length us, event | category | flops | bytes accessed | tf_op | source)
XLA Modules:
  0.0 91.6 jit_solution(14790732578960491764)
XLA Ops:
  1.9 1.6 %collective-permute-start = (bf16[384,512]{1,0:T(8,128)(2,1)S(1)}, bf16[384,512]{1,0:T(8,128)(2,1)S(1)}, u32[]{:S(2)}, u32[]{:S(2)}) collective-permute-start(bf16[384,512]{1,0:T(8,128)(2,1)S(1)} %bitcast.14), channel_id=1, source_target_pairs={{0,2},{1,3},{2,4},{3,5},{4,6},{5,7},{6,0},{7,1},{8,10},{9,11},{10,... | collective-permute-start | bytes 1179656 | tf_op jit(solution)/shard_map/ppermute | solution.py:417
  5.5 2.0 %collective-permute-start.7 = (bf16[384,512]{1,0:T(8,128)(2,1)S(1)}, bf16[384,512]{1,0:T(8,128)(2,1)S(1)}, u32[]{:S(2)}, u32[]{:S(2)}) collective-permute-start(bf16[384,512]{1,0:T(8,128)(2,1)S(1)} %bitcast.15), channel_id=1, source_target_pairs={{0,6},{1,7},{2,0},{3,1},{4,2},{5,3},{6,4},{7,5},{8,14},{9,15},{10,... | collective-permute-start | bytes 1179656 | tf_op jit(solution)/shard_map/ppermute | solution.py:417
  7.4 6.7 %collective-permute-done.refs_0_ = bf16[384,512]{1,0:T(8,128)(2,1)S(1)} collective-permute-done((bf16[384,512]{1,0:T(8,128)(2,1)S(1)}, bf16[384,512]{1,0:T(8,128)(2,1)S(1)}, u32[]{:S(2)}, u32[]{:S(2)}) %collective-permute-start) | collective-permute-done | bytes 393248 | tf_op jit(solution)/shard_map/ppermute | solution.py:417
  16.8 5.8 %collective-permute-done.9.refs_2_ = bf16[384,512]{1,0:T(8,128)(2,1)S(1)} collective-permute-done((bf16[384,512]{1,0:T(8,128)(2,1)S(1)}, bf16[384,512]{1,0:T(8,128)(2,1)S(1)}, u32[]{:S(2)}, u32[]{:S(2)}) %collective-permute-start.9) | collective-permute-done | bytes 393248 | tf_op jit(solution)/shard_map/ppermute | solution.py:417
  22.6 3.2 %collective-permute-start.4 = (bf16[384,512]{1,0:T(8,128)(2,1)S(1)}, bf16[384,512]{1,0:T(8,128)(2,1)}, u32[]{:S(2)}, u32[]{:S(2)}) collective-permute-start(bf16[384,512]{1,0:T(8,128)(2,1)S(1)} %collective-permute-done.3.refs_2_), channel_id=1, source_target_pairs={{0,6},{1,7},{2,0},{3,1},{4,2},{5,3},{6,4},{7,5},{8,14},{9,15},{10,... | collective-permute-start | bytes 1179656 | tf_op jit(solution)/shard_map/ppermute | solution.py:417
  27.2 2.3 %shard_map.111 = f32[16,16,512]{2,1,0:T(8,128)} custom-call(bf16[4,256]{1,0:T(4,128)(2,1)} %x_ref.1, bf16[256,512]{1,0:T(8,128)(2,1)} %q_hbm.1, bf16[256,512]{1,0:T(8,128)(2,1)} %g_hbm.1, bf16[4096,512]{1,0:T(8,128)(2,1)} %f_hbm.1, bf16[4096,512]{1,0:T(8,128)(2,1)} %v_hbm.1), custom_call_target="tpu_custom_call" | custom-call | tf_op jit(solution)/shard_map/pallas_call | solution.py:28
  29.6 6.9 %all-to-all-start.1 = ((f32[16,16,512]{2,1,0:T(8,128)}), f32[16,16,512]{2,1,0:T(8,128)S(1)}, u32[]{:S(2)}, u32[]{:S(2)}) async-start(f32[16,16,512]{2,1,0:T(8,128)} %shard_map.111), calls=%async_computation.1 | async-start | bytes 1048576 | tf_op jit(solution)/shard_map/all_to_all | solution.py:423
  37.1 3.9 %load.1 = (bf16[4096,512]{1,0:T(8,128)(2,1)S(1)}, bf16[4096,512]{1,0:T(8,128)(2,1)S(1)}, f32[768,512]{1,0:T(8,128)S(1)}, f32[768,512]{1,0:T(8,128)S(1)}) custom-call(bf16[768,512]{1,0:T(8,128)(2,1)} %bitcast.19, bf16[768,512]{1,0:T(8,128)(2,1)} %copy-done.3, bf16[4096,512]{1,0:T(8,128)(2,1)} %f_hbm.1, bf16[4096,512]{1,0:T(8,128)(2,1)} %v_hbm.1), custom_call_target="tpu_custom_call" | custom-call | tf_op jit(solution)/shard_map/load/pallas_call | solution.py:133
  41.1 2.8 %shard_map.105 = (f32[768,512]{1,0:T(8,128)S(1)}, f32[768,512]{1,0:T(8,128)S(1)}) custom-call(bf16[384,512]{1,0:T(8,128)(2,1)S(1)} %collective-permute-done.refs_0_, bf16[384,512]{1,0:T(8,128)(2,1)S(1)} %collective-permute-done.11.refs_1_, bf16[384,512]{1,0:T(8,128)(2,1)S(1)} %collective-permute-done.3.refs_2_, ...), custom_call_target="tpu_custom_call" | custom-call | flops 1610612736 | tf_op jit(solution)/shard_map/pallas_call | solution.py:28
  43.9 1.8 %shard_map.106 = (f32[768,512]{1,0:T(8,128)S(1)}, f32[768,512]{1,0:T(8,128)S(1)}) custom-call(bf16[384,512]{1,0:T(8,128)(2,1)S(1)} %collective-permute-done.7.refs_0_, bf16[384,512]{1,0:T(8,128)(2,1)S(1)} %collective-permute-done.8.refs_1_, bf16[384,512]{1,0:T(8,128)(2,1)S(1)} %collective-permute-done.9.refs_2_, ...), custom_call_target="tpu_custom_call" | custom-call | flops 1610612736 | tf_op jit(solution)/shard_map/pallas_call | solution.py:28
  45.8 3.6 %shard_map.107 = (bf16[768,512]{1,0:T(8,128)(2,1)S(1)}, bf16[768,512]{1,0:T(8,128)(2,1)S(1)}, f32[16,16,128]{2,1,0:T(8,128)}) custom-call(bf16[384,512]{1,0:T(8,128)(2,1)} %collective-permute-done.1.refs_0_, bf16[384,512]{1,0:T(8,128)(2,1)S(1)} %collective-permute-done.2.refs_1_, bf16[384,512]{1,0:T(8,128)(2,1)} %collective-permute-done.4.refs_2_, ...), custom_call_target="tpu_custom_call" | custom-call | flops 4831838208 | tf_op jit(solution)/shard_map/pallas_call | solution.py:28
  49.4 2.7 %all-to-all-done.1.got_ref = f32[16,16,512]{2,1,0:T(8,128)S(1)} async-done(((f32[16,16,512]{2,1,0:T(8,128)}), f32[16,16,512]{2,1,0:T(8,128)S(1)}, u32[]{:S(2)}, u32[]{:S(2)}) %all-to-all-start.1) | async-done | bytes 524320 | tf_op jit(solution)/shard_map/all_to_all | solution.py:423
  52.1 4.8 %all-to-all-start = ((f32[16,16,128]{2,1,0:T(8,128)}), f32[16,16,128]{2,1,0:T(8,128)S(1)}, u32[]{:S(2)}, u32[]{:S(2)}) async-start(f32[16,16,128]{2,1,0:T(8,128)} %get-tuple-element.48), calls=%async_computation | async-start | bytes 262144 | tf_op jit(solution)/shard_map/all_to_all | solution.py:423
  57.0 2.9 %shard_map.108 = (bf16[4,17,8,128]{3,2,1,0:T(8,128)(2,1)S(1)}, bf16[4,17,8,128]{3,2,1,0:T(8,128)(2,1)S(1)}, bf16[4,17,8,128]{3,2,1,0:T(8,128)(2,1)S(1)}, bf16[4,...) custom-call(bf16[768,512]{1,0:T(8,128)(2,1)S(1)} %get-tuple-element.38.forget_ref, ...), custom_call_target="tpu_custom_call" | custom-call | flops 201326592 | tf_op jit(solution)/shard_map/pallas_call | solution.py:28
  59.9 6.0 %all-to-all-done.totals_ref = f32[16,16,128]{2,1,0:T(8,128)S(1)} async-done(((f32[16,16,128]{2,1,0:T(8,128)}), f32[16,16,128]{2,1,0:T(8,128)S(1)}, u32[]{:S(2)}, u32[]{:S(2)}) %all-to-all-start) | async-done | bytes 131104 | tf_op jit(solution)/shard_map/all_to_all | solution.py:423
  66.9 3.5 %all-to-all-start.2 = ((f32[16,16,128]{2,1,0:T(8,128)}), f32[16,16,128]{2,1,0:T(8,128)S(1)}, u32[]{:S(2)}, u32[]{:S(2)}) async-start(f32[16,16,128]{2,1,0:T(8,128)} %shard_map.113), calls=%async_computation.2 | async-start | bytes 262144 | tf_op jit(solution)/shard_map/all_to_all | solution.py:423
  70.4 1.8 %collective-permute-start.13 = (bf16[4,17,8,128]{3,2,1,0:T(8,128)(2,1)S(1)}, bf16[4,17,8,128]{3,2,1,0:T(8,128)(2,1)S(1)}, u32[]{:S(2)}, u32[]{:S(2)}) collective-permute-start(bf16[4,17,8,128]{3,2,1,0:T(8,128)(2,1)S(1)} %get-tuple-element.41), channel_id=1, source_target_pairs={{0,8},{8,16},{16,24},{24,0},{32,40},{40,48},{48,56},{56,32},{64,72... | collective-permute-start | bytes 417800 | tf_op jit(solution)/shard_map/ppermute | solution.py:492
  72.2 2.7 %collective-permute-start.14 = (bf16[4,17,8,128]{3,2,1,0:T(8,128)(2,1)S(1)}, bf16[4,17,8,128]{3,2,1,0:T(8,128)(2,1)S(1)}, u32[]{:S(2)}, u32[]{:S(2)}) collective-permute-start(bf16[4,17,8,128]{3,2,1,0:T(8,128)(2,1)S(1)} %get-tuple-element.42), channel_id=1, source_target_pairs={{0,16},{8,24},{16,0},{24,8},{32,48},{40,56},{48,32},{56,40},{64,80... | collective-permute-start | bytes 417800 | tf_op jit(solution)/shard_map/ppermute | solution.py:492
  74.9 1.5 %collective-permute-start.15 = (bf16[4,17,8,128]{3,2,1,0:T(8,128)(2,1)S(1)}, bf16[4,17,8,128]{3,2,1,0:T(8,128)(2,1)S(1)}, u32[]{:S(2)}, u32[]{:S(2)}) collective-permute-start(bf16[4,17,8,128]{3,2,1,0:T(8,128)(2,1)S(1)} %get-tuple-element.43), channel_id=1, source_target_pairs={{0,24},{8,0},{16,8},{24,16},{32,56},{40,32},{48,40},{56,48},{64,88... | collective-permute-start | bytes 417800 | tf_op jit(solution)/shard_map/ppermute | solution.py:492
  76.3 2.3 %collective-permute-done.13.refs_1_ = bf16[4,17,8,128]{3,2,1,0:T(8,128)(2,1)S(1)} collective-permute-done((bf16[4,17,8,128]{3,2,1,0:T(8,128)(2,1)S(1)}, bf16[4,17,8,128]{3,2,1,0:T(8,128)(2,1)S(1)}, u32[]{:S(2)}, u32[]{:S(2)}) %collective-permute-start.13) | collective-permute-done | bytes 139296 | tf_op jit(solution)/shard_map/ppermute | solution.py:492
  78.6 2.8 %collective-permute-done.14.refs_2_ = bf16[4,17,8,128]{3,2,1,0:T(8,128)(2,1)S(1)} collective-permute-done((bf16[4,17,8,128]{3,2,1,0:T(8,128)(2,1)S(1)}, bf16[4,17,8,128]{3,2,1,0:T(8,128)(2,1)S(1)}, u32[]{:S(2)}, u32[]{:S(2)}) %collective-permute-start.14) | collective-permute-done | bytes 139296 | tf_op jit(solution)/shard_map/ppermute | solution.py:492
  82.4 1.5 %collective-permute-start.16 = (bf16[17,8,128]{2,1,0:T(8,128)(2,1)S(1)}, bf16[17,8,128]{2,1,0:T(8,128)(2,1)S(1)}, u32[]{:S(2)}, u32[]{:S(2)}) collective-permute-start(bf16[17,8,128]{2,1,0:T(8,128)(2,1)S(1)} %get-tuple-element.45), channel_id=1, source_target_pairs={{0,32},{8,40},{16,48},{24,56},{32,64},{40,72},{48,80},{56,88},{64,... | collective-permute-start | bytes 104456 | tf_op jit(solution)/shard_map/ppermute | solution.py:500
  83.8 2.1 %collective-permute-start.17 = (bf16[17,8,128]{2,1,0:T(8,128)(2,1)S(1)}, bf16[17,8,128]{2,1,0:T(8,128)(2,1)S(1)}, u32[]{:S(2)}, u32[]{:S(2)}) collective-permute-start(bf16[17,8,128]{2,1,0:T(8,128)(2,1)S(1)} %get-tuple-element.46), channel_id=1, source_target_pairs={{0,64},{8,72},{16,80},{24,88},{32,96},{40,104},{48,112},{56,120},{... | collective-permute-start | bytes 104456 | tf_op jit(solution)/shard_map/ppermute | solution.py:500
  86.0 1.7 %collective-permute-start.18 = (bf16[17,8,128]{2,1,0:T(8,128)(2,1)S(1)}, bf16[17,8,128]{2,1,0:T(8,128)(2,1)S(1)}, u32[]{:S(2)}, u32[]{:S(2)}) collective-permute-start(bf16[17,8,128]{2,1,0:T(8,128)(2,1)S(1)} %get-tuple-element.47), channel_id=1, source_target_pairs={{0,96},{8,104},{16,112},{24,120},{32,0},{40,8},{48,16},{56,24},{64... | collective-permute-start | bytes 104456 | tf_op jit(solution)/shard_map/ppermute | solution.py:500
  (41 shorter events, 13.7 us)
Async XLA Ops:
  0.6 25.2 %collective-permute-start.6 = (bf16[768,512]{1,0:T(8,128)(2,1)}, bf16[768,512]{1,0:T(8,128)(2,1)S(1)}, u32[]{:S(2)}, u32[]{:S(2)}) collective-permute-start(bf16[768,512]{1,0:T(8,128)(2,1)} %bitcast.18), channel_id=1, source_target_pairs={{0,1},{1,0},{2,3},{3,2},{4,5},{5,4},{6,7},{7,6},{8,9},{9,8},{10,11... | collective-permute-start | bytes 2359304 | tf_op jit(solution)/shard_map/ppermute | solution.py:420
  1.9 12.3 %collective-permute-start = (bf16[384,512]{1,0:T(8,128)(2,1)S(1)}, bf16[384,512]{1,0:T(8,128)(2,1)S(1)}, u32[]{:S(2)}, u32[]{:S(2)}) collective-permute-start(bf16[384,512]{1,0:T(8,128)(2,1)S(1)} %bitcast.14), channel_id=1, source_target_pairs={{0,2},{1,3},{2,4},{3,5},{4,6},{5,7},{6,0},{7,1},{8,10},{9,11},{10,... | collective-permute-start | bytes 1179656 | tf_op jit(solution)/shard_map/ppermute | solution.py:417
  3.4 12.0 %collective-permute-start.3 = (bf16[384,512]{1,0:T(8,128)(2,1)S(1)}, bf16[384,512]{1,0:T(8,128)(2,1)S(1)}, u32[]{:S(2)}, u32[]{:S(2)}) collective-permute-start(bf16[384,512]{1,0:T(8,128)(2,1)S(1)} %bitcast.16), channel_id=1, source_target_pairs={{0,6},{1,7},{2,0},{3,1},{4,2},{5,3},{6,4},{7,5},{8,14},{9,15},{10,... | collective-permute-start | bytes 1179656 | tf_op jit(solution)/shard_map/ppermute | solution.py:417
  4.3 18.3 %collective-permute-start.9 = (bf16[384,512]{1,0:T(8,128)(2,1)S(1)}, bf16[384,512]{1,0:T(8,128)(2,1)S(1)}, u32[]{:S(2)}, u32[]{:S(2)}) collective-permute-start(bf16[384,512]{1,0:T(8,128)(2,1)S(1)} %bitcast.17), channel_id=1, source_target_pairs={{0,2},{1,3},{2,4},{3,5},{4,6},{5,7},{6,0},{7,1},{8,10},{9,11},{10,... | collective-permute-start | bytes 1179656 | tf_op jit(solution)/shard_map/ppermute | solution.py:417
  5.5 20.4 %collective-permute-start.7 = (bf16[384,512]{1,0:T(8,128)(2,1)S(1)}, bf16[384,512]{1,0:T(8,128)(2,1)S(1)}, u32[]{:S(2)}, u32[]{:S(2)}) collective-permute-start(bf16[384,512]{1,0:T(8,128)(2,1)S(1)} %bitcast.15), channel_id=1, source_target_pairs={{0,6},{1,7},{2,0},{3,1},{4,2},{5,3},{6,4},{7,5},{8,14},{9,15},{10,... | collective-permute-start | bytes 1179656 | tf_op jit(solution)/shard_map/ppermute | solution.py:417
  14.2 12.2 %collective-permute-start.11 = (bf16[384,512]{1,0:T(8,128)(2,1)S(1)}, bf16[384,512]{1,0:T(8,128)(2,1)S(1)}, u32[]{:S(2)}, u32[]{:S(2)}) collective-permute-start(bf16[384,512]{1,0:T(8,128)(2,1)S(1)} %collective-permute-done.refs_0_), channel_id=1, source_target_pairs={{0,1},{1,0},{2,3},{3,2},{4,5},{5,4},{6,7},{7,6},{8,9},{9,8},{10,11... | collective-permute-start | bytes 1179656 | tf_op jit(solution)/shard_map/ppermute | solution.py:420
  15.4 21.1 %collective-permute-start.1 = (bf16[384,512]{1,0:T(8,128)(2,1)S(1)}, bf16[384,512]{1,0:T(8,128)(2,1)}, u32[]{:S(2)}, u32[]{:S(2)}) collective-permute-start(bf16[384,512]{1,0:T(8,128)(2,1)S(1)} %collective-permute-done.refs_0_), channel_id=1, source_target_pairs={{0,2},{1,3},{2,4},{3,5},{4,6},{5,7},{6,0},{7,1},{8,10},{9,11},{10,... | collective-permute-start | bytes 1179656 | tf_op jit(solution)/shard_map/ppermute | solution.py:417
  22.6 14.0 %collective-permute-start.4 = (bf16[384,512]{1,0:T(8,128)(2,1)S(1)}, bf16[384,512]{1,0:T(8,128)(2,1)}, u32[]{:S(2)}, u32[]{:S(2)}) collective-permute-start(bf16[384,512]{1,0:T(8,128)(2,1)S(1)} %collective-permute-done.3.refs_2_), channel_id=1, source_target_pairs={{0,6},{1,7},{2,0},{3,1},{4,2},{5,3},{6,4},{7,5},{8,14},{9,15},{10,... | collective-permute-start | bytes 1179656 | tf_op jit(solution)/shard_map/ppermute | solution.py:417
  25.8 15.2 %collective-permute-start.12 = (bf16[384,512]{1,0:T(8,128)(2,1)S(1)}, bf16[384,512]{1,0:T(8,128)(2,1)}, u32[]{:S(2)}, u32[]{:S(2)}) collective-permute-start(bf16[384,512]{1,0:T(8,128)(2,1)S(1)} %collective-permute-done.3.refs_2_), channel_id=1, source_target_pairs={{0,1},{1,0},{2,3},{3,2},{4,5},{5,4},{6,7},{7,6},{8,9},{9,8},{10,11... | collective-permute-start | bytes 1179656 | tf_op jit(solution)/shard_map/ppermute | solution.py:420
  25.8 18.0 %collective-permute-start.10 = (bf16[384,512]{1,0:T(8,128)(2,1)S(1)}, bf16[384,512]{1,0:T(8,128)(2,1)S(1)}, u32[]{:S(2)}, u32[]{:S(2)}) collective-permute-start(bf16[384,512]{1,0:T(8,128)(2,1)S(1)} %collective-permute-done.9.refs_2_), channel_id=1, source_target_pairs={{0,1},{1,0},{2,3},{3,2},{4,5},{5,4},{6,7},{7,6},{8,9},{9,8},{10,11... | collective-permute-start | bytes 1179656 | tf_op jit(solution)/shard_map/ppermute | solution.py:420
  26.7 17.2 %collective-permute-start.8 = (bf16[384,512]{1,0:T(8,128)(2,1)S(1)}, bf16[384,512]{1,0:T(8,128)(2,1)S(1)}, u32[]{:S(2)}, u32[]{:S(2)}) collective-permute-start(bf16[384,512]{1,0:T(8,128)(2,1)S(1)} %collective-permute-done.7.refs_0_), channel_id=1, source_target_pairs={{0,1},{1,0},{2,3},{3,2},{4,5},{5,4},{6,7},{7,6},{8,9},{9,8},{10,11... | collective-permute-start | bytes 1179656 | tf_op jit(solution)/shard_map/ppermute | solution.py:420
  29.6 22.5 %all-to-all-start.1 = ((f32[16,16,512]{2,1,0:T(8,128)}), f32[16,16,512]{2,1,0:T(8,128)S(1)}, u32[]{:S(2)}, u32[]{:S(2)}) async-start(f32[16,16,512]{2,1,0:T(8,128)} %shard_map.111), calls=%async_computation.1 | async-start | bytes 1048576 | tf_op jit(solution)/shard_map/all_to_all | solution.py:423
  36.5 9.2 %collective-permute-start.2 = (bf16[384,512]{1,0:T(8,128)(2,1)}, bf16[384,512]{1,0:T(8,128)(2,1)S(1)}, u32[]{:S(2)}, u32[]{:S(2)}) collective-permute-start(bf16[384,512]{1,0:T(8,128)(2,1)} %collective-permute-done.1.refs_0_), channel_id=1, source_target_pairs={{0,1},{1,0},{2,3},{3,2},{4,5},{5,4},{6,7},{7,6},{8,9},{9,8},{10,11... | collective-permute-start | bytes 1179656 | tf_op jit(solution)/shard_map/ppermute | solution.py:420
  36.6 9.1 %collective-permute-start.5 = (bf16[384,512]{1,0:T(8,128)(2,1)}, bf16[384,512]{1,0:T(8,128)(2,1)S(1)}, u32[]{:S(2)}, u32[]{:S(2)}) collective-permute-start(bf16[384,512]{1,0:T(8,128)(2,1)} %collective-permute-done.4.refs_2_), channel_id=1, source_target_pairs={{0,1},{1,0},{2,3},{3,2},{4,5},{5,4},{6,7},{7,6},{8,9},{9,8},{10,11... | collective-permute-start | bytes 1179656 | tf_op jit(solution)/shard_map/ppermute | solution.py:420
  43.9 1.9 %copy-start = (f32[4,192,4]{1,2,0:T(4,128)S(1)}, f32[4,192,4]{1,2,0:T(4,128)}, u32[]{:S(2)}) copy-start(f32[4,192,4]{1,2,0:T(4,128)} %param.16) | copy-start | bytes 36868
  52.1 13.8 %all-to-all-start = ((f32[16,16,128]{2,1,0:T(8,128)}), f32[16,16,128]{2,1,0:T(8,128)S(1)}, u32[]{:S(2)}, u32[]{:S(2)}) async-start(f32[16,16,128]{2,1,0:T(8,128)} %get-tuple-element.48), calls=%async_computation | async-start | bytes 262144 | tf_op jit(solution)/shard_map/all_to_all | solution.py:423
  56.9 33.8 %copy-start.2 = (f32[128]{0:T(128)S(1)}, f32[128]{0:T(128)}, u32[]{:S(2)}) copy-start(f32[128]{0:T(128)} %param.17) | copy-start | bytes 1540
  66.9 23.9 %all-to-all-start.2 = ((f32[16,16,128]{2,1,0:T(8,128)}), f32[16,16,128]{2,1,0:T(8,128)S(1)}, u32[]{:S(2)}, u32[]{:S(2)}) async-start(f32[16,16,128]{2,1,0:T(8,128)} %shard_map.113), calls=%async_computation.2 | async-start | bytes 262144 | tf_op jit(solution)/shard_map/all_to_all | solution.py:423
  70.4 8.2 %collective-permute-start.13 = (bf16[4,17,8,128]{3,2,1,0:T(8,128)(2,1)S(1)}, bf16[4,17,8,128]{3,2,1,0:T(8,128)(2,1)S(1)}, u32[]{:S(2)}, u32[]{:S(2)}) collective-permute-start(bf16[4,17,8,128]{3,2,1,0:T(8,128)(2,1)S(1)} %get-tuple-element.41), channel_id=1, source_target_pairs={{0,8},{8,16},{16,24},{24,0},{32,40},{40,48},{48,56},{56,32},{64,72... | collective-permute-start | bytes 417800 | tf_op jit(solution)/shard_map/ppermute | solution.py:492
  72.2 9.2 %collective-permute-start.14 = (bf16[4,17,8,128]{3,2,1,0:T(8,128)(2,1)S(1)}, bf16[4,17,8,128]{3,2,1,0:T(8,128)(2,1)S(1)}, u32[]{:S(2)}, u32[]{:S(2)}) collective-permute-start(bf16[4,17,8,128]{3,2,1,0:T(8,128)(2,1)S(1)} %get-tuple-element.42), channel_id=1, source_target_pairs={{0,16},{8,24},{16,0},{24,8},{32,48},{40,56},{48,32},{56,40},{64,80... | collective-permute-start | bytes 417800 | tf_op jit(solution)/shard_map/ppermute | solution.py:492
  74.9 6.6 %collective-permute-start.15 = (bf16[4,17,8,128]{3,2,1,0:T(8,128)(2,1)S(1)}, bf16[4,17,8,128]{3,2,1,0:T(8,128)(2,1)S(1)}, u32[]{:S(2)}, u32[]{:S(2)}) collective-permute-start(bf16[4,17,8,128]{3,2,1,0:T(8,128)(2,1)S(1)} %get-tuple-element.43), channel_id=1, source_target_pairs={{0,24},{8,0},{16,8},{24,16},{32,56},{40,32},{48,40},{56,48},{64,88... | collective-permute-start | bytes 417800 | tf_op jit(solution)/shard_map/ppermute | solution.py:492
  82.4 5.8 %collective-permute-start.16 = (bf16[17,8,128]{2,1,0:T(8,128)(2,1)S(1)}, bf16[17,8,128]{2,1,0:T(8,128)(2,1)S(1)}, u32[]{:S(2)}, u32[]{:S(2)}) collective-permute-start(bf16[17,8,128]{2,1,0:T(8,128)(2,1)S(1)} %get-tuple-element.45), channel_id=1, source_target_pairs={{0,32},{8,40},{16,48},{24,56},{32,64},{40,72},{48,80},{56,88},{64,... | collective-permute-start | bytes 104456 | tf_op jit(solution)/shard_map/ppermute | solution.py:500
  83.8 4.8 %collective-permute-start.17 = (bf16[17,8,128]{2,1,0:T(8,128)(2,1)S(1)}, bf16[17,8,128]{2,1,0:T(8,128)(2,1)S(1)}, u32[]{:S(2)}, u32[]{:S(2)}) collective-permute-start(bf16[17,8,128]{2,1,0:T(8,128)(2,1)S(1)} %get-tuple-element.46), channel_id=1, source_target_pairs={{0,64},{8,72},{16,80},{24,88},{32,96},{40,104},{48,112},{56,120},{... | collective-permute-start | bytes 104456 | tf_op jit(solution)/shard_map/ppermute | solution.py:500
  86.0 3.9 %collective-permute-start.18 = (bf16[17,8,128]{2,1,0:T(8,128)(2,1)S(1)}, bf16[17,8,128]{2,1,0:T(8,128)(2,1)S(1)}, u32[]{:S(2)}, u32[]{:S(2)}) collective-permute-start(bf16[17,8,128]{2,1,0:T(8,128)(2,1)S(1)} %get-tuple-element.47), channel_id=1, source_target_pairs={{0,96},{8,104},{16,112},{24,120},{32,0},{40,8},{48,16},{56,24},{64... | collective-permute-start | bytes 104456 | tf_op jit(solution)/shard_map/ppermute | solution.py:500
  (2 other events, 2.7 us)

commit v8 on v7

--- a/solution.py
+++ b/solution.py
@@ -237,7 +237,7 @@
         parts_ref[y, :, pairs] = blocks[:, y]
     near = lax.rem(lax.axis_index("sp"), NEAR)
     for step, out in enumerate(outs):
-        out[...] = parts_ref[lax.rem(near + step, NEAR)]
+        out[...] = parts_ref[near ^ step]
 
 
 def states(forget, values, slack, damp, parts):
@@ -265,9 +265,9 @@
     return tile + pltpu.roll(tile, lanes - pairs, 1) + pltpu.roll(tile, lanes - 2 * pairs, 1)
 
 
-def joined(tiles, place, count):
+def joined(tiles, place):
     pairs = tiles[0].shape[0] - 1
-    places = [lax.rem(place + count - step, count) for step in range(count)]
+    places = [place ^ step for step in range(len(tiles))]
     totals = [unpacked(tile[pairs], pairs) for tile in tiles]
     sums = [None] * pairs
     for here, tile in zip(places, tiles):
@@ -286,7 +286,7 @@
     me = lax.axis_index("sp")
     lane = lax.broadcasted_iota(jnp.int32, (rows, lanes), 1)
     for z in range(far):
-        sums, total = joined([t.at[z] for t in tiles], lax.rem(me, NEAR), NEAR)
+        sums, total = joined([t.at[z] for t in tiles], lax.rem(me, NEAR))
         for j in range(pairs):
             parts_ref[z, j] = sums[j].astype(BF)
         high, middle, low = (t.astype(F32) for t in three_terms(total))
@@ -294,7 +294,7 @@
         packed = jnp.where(lane < pairs, high, packed)
         parts_ref[z, pairs] = jnp.where(lane < 3 * pairs, packed, 0.0).astype(BF)
     for step, out in enumerate(outs):
-        out[...] = parts_ref[lax.rem(me // NEAR + step, far)]
+        out[...] = parts_ref[(me // NEAR) ^ step]
 
 
 def join_near(tiles):
@@ -309,7 +309,7 @@
 
 def far_kernel(*refs):
     tiles, cache_ref = refs[:-1], refs[-1]
-    sums, _ = joined(tiles, lax.axis_index("sp") // NEAR, len(tiles))
+    sums, _ = joined(tiles, lax.axis_index("sp") // NEAR)
     for j, part in enumerate(sums):
         cache_ref[j] = part.astype(BF)
 
@@ -471,10 +471,11 @@
     sums = project(pieces, (both(1), both(-1)), weights, sums)
     pieces = [left_a, other_left_a, right_b, other_right_b]
     sums = project(pieces, (both(-1), both(1)), weights, sums)
+    sums = project([far_a, far_b], (((2, False),), ((2, False),)), weights, sums)
     damp = additional_damping_exponent.transpose(0, 2, 1)
     forget, values, totals = log_totals(
-        [far_a, other_far_a, far_b, other_far_b],
-        (both(2), both(2)),
+        [other_far_a, other_far_b],
+        (((2, True),), ((2, True),)),
         weights,
         sums,
         slack,
@@ -487,13 +488,13 @@
 
     def along_y(step):
         pairs = [
-            (z * NEAR + y, z * NEAR + (y + step) % NEAR) for z in range(planes) for y in range(NEAR)
+            (z * NEAR + y, z * NEAR + (y ^ step)) for z in range(planes) for y in range(NEAR)
         ]
         return lax.ppermute(parts[step], "sp", pairs)
 
     def along_z(step):
         pairs = [
-            (z * NEAR + y, (z + step) % planes * NEAR + y)
+            (z * NEAR + y, (z ^ step) * NEAR + y)
             for z in range(planes)
             for y in range(NEAR)
         ]

time: 92.5 us -> 93.5 us (1.011)
  waiting for transfers between devices: 29.9 us -> 35.1 us
  starting transfers between devices: 38.3 us -> 35.8 us
    ppermute x3, waiting for transfers between devices: 2.22 us -> 4.9 us  [along_z(): return lax.ppermute(parts[step], 'sp', pairs)]
    ppermute x3, waiting for transfers between devices: 5.1 us -> 7.21 us  [along_y(): return lax.ppermute(parts[step], 'sp', pairs)]
    ppermute x3, starting transfers between devices: 5.95 us -> 4.79 us  [along_y(): return lax.ppermute(parts[step], 'sp', pairs)]
    pallas_call x10 -> x11, Pallas kernels: 16.4 us -> 15.7 us  [in_vmem(): pl.pallas_call(kernel, in_specs=in_specs or [VMEM] * len(arrays), out_spe...]
  transfers between devices with their start and end apart: 22 -> 22, of which waited for: 10 -> 10; matrix products, arithmetic and copies ran while one was open for 1% -> 1% of each run, Pallas kernels for 22% -> 20%
where the time goes in v8:
time: 93.5 us; the launch traced here: 93.1 us
  starting transfers between devices  35.8 us (38%)
  waiting for transfers between devices  35.1 us (38%)
  Pallas kernels  20.8 us (22%)
    pallas_call x11, Pallas kernels, in_vmem(): pl.pallas_call(kernel, in_specs=in_specs or [VMEM] * len(arrays), out_spe...  15.7 us
    all_to_all x3, starting transfers between devices, exchange(): return lax.all_to_all(x, 'sp', 0, 0, tiled=True)  15.2 us
    ppermute x6, waiting for transfers between devices, shifted(): return lax.ppermute(x, 'tp', pairs)  13.8 us
    ppermute x6, starting transfers between devices, shifted(): return lax.ppermute(x, 'tp', pairs)  10.1 us
    all_to_all x3, waiting for transfers between devices, exchange(): return lax.all_to_all(x, 'sp', 0, 0, tiled=True)  9.14 us
    ppermute x3, waiting for transfers between devices, along_y(): return lax.ppermute(parts[step], 'sp', pairs)  7.21 us
    ppermute x3, waiting for transfers between devices, along_z(): return lax.ppermute(parts[step], 'sp', pairs)  4.9 us
    ppermute x3, starting transfers between devices, along_y(): return lax.ppermute(parts[step], 'sp', pairs)  4.79 us
  transfers between devices with their start and end apart: 22, of which 10 were waited for; matrix products, arithmetic and copies ran while one was open for 1% of the time, Pallas kernels for 20%

profile of v8, /device:TPU:2, one launch (start us, length us, event | category | flops | bytes accessed | tf_op | source)
XLA Modules:
  0.0 93.1 jit_solution(11043171354244111194)
XLA Ops:
  1.9 1.6 %collective-permute-start = (bf16[384,512]{1,0:T(8,128)(2,1)S(1)}, bf16[384,512]{1,0:T(8,128)(2,1)S(1)}, u32[]{:S(2)}, u32[]{:S(2)}) collective-permute-start(bf16[384,512]{1,0:T(8,128)(2,1)S(1)} %bitcast.14), channel_id=1, source_target_pairs={{0,2},{1,3},{2,4},{3,5},{4,6},{5,7},{6,0},{7,1},{8,10},{9,11},{10,... | collective-permute-start | bytes 1179656 | tf_op jit(solution)/shard_map/ppermute | solution.py:417
  5.5 2.0 %collective-permute-start.7 = (bf16[384,512]{1,0:T(8,128)(2,1)S(1)}, bf16[384,512]{1,0:T(8,128)(2,1)S(1)}, u32[]{:S(2)}, u32[]{:S(2)}) collective-permute-start(bf16[384,512]{1,0:T(8,128)(2,1)S(1)} %bitcast.15), channel_id=1, source_target_pairs={{0,6},{1,7},{2,0},{3,1},{4,2},{5,3},{6,4},{7,5},{8,14},{9,15},{10,... | collective-permute-start | bytes 1179656 | tf_op jit(solution)/shard_map/ppermute | solution.py:417
  7.4 6.7 %collective-permute-done.refs_0_ = bf16[384,512]{1,0:T(8,128)(2,1)S(1)} collective-permute-done((bf16[384,512]{1,0:T(8,128)(2,1)S(1)}, bf16[384,512]{1,0:T(8,128)(2,1)S(1)}, u32[]{:S(2)}, u32[]{:S(2)}) %collective-permute-start) | collective-permute-done | bytes 393248 | tf_op jit(solution)/shard_map/ppermute | solution.py:417
  16.8 5.8 %collective-permute-done.9.refs_2_ = bf16[384,512]{1,0:T(8,128)(2,1)S(1)} collective-permute-done((bf16[384,512]{1,0:T(8,128)(2,1)S(1)}, bf16[384,512]{1,0:T(8,128)(2,1)S(1)}, u32[]{:S(2)}, u32[]{:S(2)}) %collective-permute-start.9) | collective-permute-done | bytes 393248 | tf_op jit(solution)/shard_map/ppermute | solution.py:417
  22.6 3.2 %collective-permute-start.4 = (bf16[384,512]{1,0:T(8,128)(2,1)S(1)}, bf16[384,512]{1,0:T(8,128)(2,1)S(1)}, u32[]{:S(2)}, u32[]{:S(2)}) collective-permute-start(bf16[384,512]{1,0:T(8,128)(2,1)S(1)} %collective-permute-done.3.refs_2_), channel_id=1, source_target_pairs={{0,6},{1,7},{2,0},{3,1},{4,2},{5,3},{6,4},{7,5},{8,14},{9,15},{10,... | collective-permute-start | bytes 1179656 | tf_op jit(solution)/shard_map/ppermute | solution.py:417
  25.8 2.3 %shard_map.112 = f32[16,16,512]{2,1,0:T(8,128)} custom-call(bf16[4,256]{1,0:T(4,128)(2,1)} %x_ref.1, bf16[256,512]{1,0:T(8,128)(2,1)} %q_hbm.1, bf16[256,512]{1,0:T(8,128)(2,1)} %g_hbm.1, bf16[4096,512]{1,0:T(8,128)(2,1)} %f_hbm.1, bf16[4096,512]{1,0:T(8,128)(2,1)} %v_hbm.1), custom_call_target="tpu_custom_call" | custom-call | tf_op jit(solution)/shard_map/pallas_call | solution.py:28
  28.2 6.9 %all-to-all-start.1 = ((f32[16,16,512]{2,1,0:T(8,128)}), f32[16,16,512]{2,1,0:T(8,128)S(1)}, u32[]{:S(2)}, u32[]{:S(2)}) async-start(f32[16,16,512]{2,1,0:T(8,128)} %shard_map.112), calls=%async_computation.1 | async-start | bytes 1048576 | tf_op jit(solution)/shard_map/all_to_all | solution.py:423
  36.2 3.9 %load.1 = (bf16[4096,512]{1,0:T(8,128)(2,1)S(1)}, bf16[4096,512]{1,0:T(8,128)(2,1)S(1)}, f32[768,512]{1,0:T(8,128)S(1)}, f32[768,512]{1,0:T(8,128)S(1)}) custom-call(bf16[768,512]{1,0:T(8,128)(2,1)} %bitcast.19, bf16[768,512]{1,0:T(8,128)(2,1)} %collective-permute-done.6.other_hbm, bf16[4096,512]{1,0:T(8,128)(2,1)} %f_hbm.1, bf16[4096,512]{1,0:T(8,128)(2,1)} %v_hbm.1), custom_call_target="tpu_custom_call" | custom-call | tf_op jit(solution)/shard_map/load/pallas_call | solution.py:133
  40.2 2.8 %shard_map.105 = (f32[768,512]{1,0:T(8,128)S(1)}, f32[768,512]{1,0:T(8,128)S(1)}) custom-call(bf16[384,512]{1,0:T(8,128)(2,1)S(1)} %collective-permute-done.refs_0_, bf16[384,512]{1,0:T(8,128)(2,1)S(1)} %collective-permute-done.11.refs_1_, bf16[384,512]{1,0:T(8,128)(2,1)S(1)} %collective-permute-done.3.refs_2_, ...), custom_call_target="tpu_custom_call" | custom-call | flops 1610612736 | tf_op jit(solution)/shard_map/pallas_call | solution.py:28
  43.0 1.8 %shard_map.106 = (f32[768,512]{1,0:T(8,128)S(1)}, f32[768,512]{1,0:T(8,128)S(1)}) custom-call(bf16[384,512]{1,0:T(8,128)(2,1)S(1)} %collective-permute-done.7.refs_0_, bf16[384,512]{1,0:T(8,128)(2,1)S(1)} %collective-permute-done.8.refs_1_, bf16[384,512]{1,0:T(8,128)(2,1)S(1)} %collective-permute-done.9.refs_2_, ...), custom_call_target="tpu_custom_call" | custom-call | flops 1610612736 | tf_op jit(solution)/shard_map/pallas_call | solution.py:28
  45.9 1.9 %shard_map.108 = (bf16[768,512]{1,0:T(8,128)(2,1)S(1)}, bf16[768,512]{1,0:T(8,128)(2,1)S(1)}, f32[16,16,128]{2,1,0:T(8,128)}) custom-call(bf16[384,512]{1,0:T(8,128)(2,1)S(1)} %collective-permute-done.2.refs_0_, bf16[384,512]{1,0:T(8,128)(2,1)S(1)} %collective-permute-done.5.refs_1_, bf16[4096,512]{1,0:T(8,128)(2,1)S(1)} %get-tuple-element.32.refs_4_.refs_2_, ...), custom_call_target="tpu_custom_call" | custom-call | flops 2415919104 | tf_op jit(solution)/shard_map/pallas_call | solution.py:28
  47.8 3.2 %all-to-all-done.1.got_ref = f32[16,16,512]{2,1,0:T(8,128)S(1)} async-done(((f32[16,16,512]{2,1,0:T(8,128)}), f32[16,16,512]{2,1,0:T(8,128)S(1)}, u32[]{:S(2)}, u32[]{:S(2)}) %all-to-all-start.1) | async-done | bytes 524320 | tf_op jit(solution)/shard_map/all_to_all | solution.py:423
  51.0 4.7 %all-to-all-start = ((f32[16,16,128]{2,1,0:T(8,128)}), f32[16,16,128]{2,1,0:T(8,128)S(1)}, u32[]{:S(2)}, u32[]{:S(2)}) async-start(f32[16,16,128]{2,1,0:T(8,128)} %get-tuple-element.52), calls=%async_computation | async-start | bytes 262144 | tf_op jit(solution)/shard_map/all_to_all | solution.py:423
  55.7 2.9 %shard_map.109 = (bf16[4,17,8,128]{3,2,1,0:T(8,128)(2,1)S(1)}, bf16[4,17,8,128]{3,2,1,0:T(8,128)(2,1)S(1)}, bf16[4,17,8,128]{3,2,1,0:T(8,128)(2,1)S(1)}, bf16[4,...) custom-call(bf16[768,512]{1,0:T(8,128)(2,1)S(1)} %get-tuple-element.42.forget_ref, ...), custom_call_target="tpu_custom_call" | custom-call | flops 201326592 | tf_op jit(solution)/shard_map/pallas_call | solution.py:28
  58.6 6.0 %all-to-all-done.totals_ref = f32[16,16,128]{2,1,0:T(8,128)S(1)} async-done(((f32[16,16,128]{2,1,0:T(8,128)}), f32[16,16,128]{2,1,0:T(8,128)S(1)}, u32[]{:S(2)}, u32[]{:S(2)}) %all-to-all-start) | async-done | bytes 131104 | tf_op jit(solution)/shard_map/all_to_all | solution.py:423
  65.6 3.5 %all-to-all-start.2 = ((f32[16,16,128]{2,1,0:T(8,128)}), f32[16,16,128]{2,1,0:T(8,128)S(1)}, u32[]{:S(2)}, u32[]{:S(2)}) async-start(f32[16,16,128]{2,1,0:T(8,128)} %shard_map.114), calls=%async_computation.2 | async-start | bytes 262144 | tf_op jit(solution)/shard_map/all_to_all | solution.py:423
  69.1 1.8 %collective-permute-start.13 = (bf16[4,17,8,128]{3,2,1,0:T(8,128)(2,1)S(1)}, bf16[4,17,8,128]{3,2,1,0:T(8,128)(2,1)S(1)}, u32[]{:S(2)}, u32[]{:S(2)}) collective-permute-start(bf16[4,17,8,128]{3,2,1,0:T(8,128)(2,1)S(1)} %get-tuple-element.45), channel_id=1, source_target_pairs={{0,8},{8,0},{16,24},{24,16},{32,40},{40,32},{48,56},{56,48},{64,72... | collective-permute-start | bytes 417800 | tf_op jit(solution)/shard_map/ppermute | solution.py:493
  70.9 2.7 %collective-permute-start.14 = (bf16[4,17,8,128]{3,2,1,0:T(8,128)(2,1)S(1)}, bf16[4,17,8,128]{3,2,1,0:T(8,128)(2,1)S(1)}, u32[]{:S(2)}, u32[]{:S(2)}) collective-permute-start(bf16[4,17,8,128]{3,2,1,0:T(8,128)(2,1)S(1)} %get-tuple-element.46), channel_id=1, source_target_pairs={{0,16},{8,24},{16,0},{24,8},{32,48},{40,56},{48,32},{56,40},{64,80... | collective-permute-start | bytes 417800 | tf_op jit(solution)/shard_map/ppermute | solution.py:493
  73.9 2.4 %collective-permute-done.13.refs_1_ = bf16[4,17,8,128]{3,2,1,0:T(8,128)(2,1)S(1)} collective-permute-done((bf16[4,17,8,128]{3,2,1,0:T(8,128)(2,1)S(1)}, bf16[4,17,8,128]{3,2,1,0:T(8,128)(2,1)S(1)}, u32[]{:S(2)}, u32[]{:S(2)}) %collective-permute-start.13) | collective-permute-done | bytes 139296 | tf_op jit(solution)/shard_map/ppermute | solution.py:493
  76.3 3.3 %collective-permute-done.14.refs_2_ = bf16[4,17,8,128]{3,2,1,0:T(8,128)(2,1)S(1)} collective-permute-done((bf16[4,17,8,128]{3,2,1,0:T(8,128)(2,1)S(1)}, bf16[4,17,8,128]{3,2,1,0:T(8,128)(2,1)S(1)}, u32[]{:S(2)}, u32[]{:S(2)}) %collective-permute-start.14) | collective-permute-done | bytes 139296 | tf_op jit(solution)/shard_map/ppermute | solution.py:493
  79.6 1.5 %collective-permute-done.15.refs_3_ = bf16[4,17,8,128]{3,2,1,0:T(8,128)(2,1)S(1)} collective-permute-done((bf16[4,17,8,128]{3,2,1,0:T(8,128)(2,1)S(1)}, bf16[4,17,8,128]{3,2,1,0:T(8,128)(2,1)S(1)}, u32[]{:S(2)}, u32[]{:S(2)}) %collective-permute-start.15) | collective-permute-done | bytes 139296 | tf_op jit(solution)/shard_map/ppermute | solution.py:493
  83.5 2.2 %collective-permute-start.17 = (bf16[17,8,128]{2,1,0:T(8,128)(2,1)S(1)}, bf16[17,8,128]{2,1,0:T(8,128)(2,1)S(1)}, u32[]{:S(2)}, u32[]{:S(2)}) collective-permute-start(bf16[17,8,128]{2,1,0:T(8,128)(2,1)S(1)} %get-tuple-element.50), channel_id=1, source_target_pairs={{0,64},{8,72},{16,80},{24,88},{32,96},{40,104},{48,112},{56,120},{... | collective-permute-start | bytes 104456 | tf_op jit(solution)/shard_map/ppermute | solution.py:501
  86.5 2.2 %collective-permute-done.17.refs_2_ = bf16[17,8,128]{2,1,0:T(8,128)(2,1)S(1)} collective-permute-done((bf16[17,8,128]{2,1,0:T(8,128)(2,1)S(1)}, bf16[17,8,128]{2,1,0:T(8,128)(2,1)S(1)}, u32[]{:S(2)}, u32[]{:S(2)}) %collective-permute-start.17) | collective-permute-done | bytes 34848 | tf_op jit(solution)/shard_map/ppermute | solution.py:501
  88.7 2.7 %collective-permute-done.18.refs_3_ = bf16[17,8,128]{2,1,0:T(8,128)(2,1)S(1)} collective-permute-done((bf16[17,8,128]{2,1,0:T(8,128)(2,1)S(1)}, bf16[17,8,128]{2,1,0:T(8,128)(2,1)S(1)}, u32[]{:S(2)}, u32[]{:S(2)}) %collective-permute-start.18) | collective-permute-done | bytes 34848 | tf_op jit(solution)/shard_map/ppermute | solution.py:501
  (40 shorter events, 14.3 us)
Async XLA Ops:
  0.6 34.5 %collective-permute-start.6 = (bf16[768,512]{1,0:T(8,128)(2,1)}, bf16[768,512]{1,0:T(8,128)(2,1)}, u32[]{:S(2)}, u32[]{:S(2)}) collective-permute-start(bf16[768,512]{1,0:T(8,128)(2,1)} %bitcast.18), channel_id=1, source_target_pairs={{0,1},{1,0},{2,3},{3,2},{4,5},{5,4},{6,7},{7,6},{8,9},{9,8},{10,11... | collective-permute-start | bytes 2359304 | tf_op jit(solution)/shard_map/ppermute | solution.py:420
  1.9 12.3 %collective-permute-start = (bf16[384,512]{1,0:T(8,128)(2,1)S(1)}, bf16[384,512]{1,0:T(8,128)(2,1)S(1)}, u32[]{:S(2)}, u32[]{:S(2)}) collective-permute-start(bf16[384,512]{1,0:T(8,128)(2,1)S(1)} %bitcast.14), channel_id=1, source_target_pairs={{0,2},{1,3},{2,4},{3,5},{4,6},{5,7},{6,0},{7,1},{8,10},{9,11},{10,... | collective-permute-start | bytes 1179656 | tf_op jit(solution)/shard_map/ppermute | solution.py:417
  3.4 12.0 %collective-permute-start.3 = (bf16[384,512]{1,0:T(8,128)(2,1)S(1)}, bf16[384,512]{1,0:T(8,128)(2,1)S(1)}, u32[]{:S(2)}, u32[]{:S(2)}) collective-permute-start(bf16[384,512]{1,0:T(8,128)(2,1)S(1)} %bitcast.16), channel_id=1, source_target_pairs={{0,6},{1,7},{2,0},{3,1},{4,2},{5,3},{6,4},{7,5},{8,14},{9,15},{10,... | collective-permute-start | bytes 1179656 | tf_op jit(solution)/shard_map/ppermute | solution.py:417
  4.3 18.3 %collective-permute-start.9 = (bf16[384,512]{1,0:T(8,128)(2,1)S(1)}, bf16[384,512]{1,0:T(8,128)(2,1)S(1)}, u32[]{:S(2)}, u32[]{:S(2)}) collective-permute-start(bf16[384,512]{1,0:T(8,128)(2,1)S(1)} %bitcast.17), channel_id=1, source_target_pairs={{0,2},{1,3},{2,4},{3,5},{4,6},{5,7},{6,0},{7,1},{8,10},{9,11},{10,... | collective-permute-start | bytes 1179656 | tf_op jit(solution)/shard_map/ppermute | solution.py:417
  5.5 20.4 %collective-permute-start.7 = (bf16[384,512]{1,0:T(8,128)(2,1)S(1)}, bf16[384,512]{1,0:T(8,128)(2,1)S(1)}, u32[]{:S(2)}, u32[]{:S(2)}) collective-permute-start(bf16[384,512]{1,0:T(8,128)(2,1)S(1)} %bitcast.15), channel_id=1, source_target_pairs={{0,6},{1,7},{2,0},{3,1},{4,2},{5,3},{6,4},{7,5},{8,14},{9,15},{10,... | collective-permute-start | bytes 1179656 | tf_op jit(solution)/shard_map/ppermute | solution.py:417
  14.2 21.3 %collective-permute-start.11 = (bf16[384,512]{1,0:T(8,128)(2,1)S(1)}, bf16[384,512]{1,0:T(8,128)(2,1)S(1)}, u32[]{:S(2)}, u32[]{:S(2)}) collective-permute-start(bf16[384,512]{1,0:T(8,128)(2,1)S(1)} %collective-permute-done.refs_0_), channel_id=1, source_target_pairs={{0,1},{1,0},{2,3},{3,2},{4,5},{5,4},{6,7},{7,6},{8,9},{9,8},{10,11... | collective-permute-start | bytes 1179656 | tf_op jit(solution)/shard_map/ppermute | solution.py:420
  15.4 20.3 %collective-permute-start.1 = (bf16[384,512]{1,0:T(8,128)(2,1)S(1)}, bf16[384,512]{1,0:T(8,128)(2,1)S(1)}, u32[]{:S(2)}, u32[]{:S(2)}) collective-permute-start(bf16[384,512]{1,0:T(8,128)(2,1)S(1)} %collective-permute-done.refs_0_), channel_id=1, source_target_pairs={{0,2},{1,3},{2,4},{3,5},{4,6},{5,7},{6,0},{7,1},{8,10},{9,11},{10,... | collective-permute-start | bytes 1179656 | tf_op jit(solution)/shard_map/ppermute | solution.py:417
  22.6 13.4 %collective-permute-start.4 = (bf16[384,512]{1,0:T(8,128)(2,1)S(1)}, bf16[384,512]{1,0:T(8,128)(2,1)S(1)}, u32[]{:S(2)}, u32[]{:S(2)}) collective-permute-start(bf16[384,512]{1,0:T(8,128)(2,1)S(1)} %collective-permute-done.3.refs_2_), channel_id=1, source_target_pairs={{0,6},{1,7},{2,0},{3,1},{4,2},{5,3},{6,4},{7,5},{8,14},{9,15},{10,... | collective-permute-start | bytes 1179656 | tf_op jit(solution)/shard_map/ppermute | solution.py:417
  25.8 14.4 %collective-permute-start.12 = (bf16[384,512]{1,0:T(8,128)(2,1)S(1)}, bf16[384,512]{1,0:T(8,128)(2,1)}, u32[]{:S(2)}, u32[]{:S(2)}) collective-permute-start(bf16[384,512]{1,0:T(8,128)(2,1)S(1)} %collective-permute-done.3.refs_2_), channel_id=1, source_target_pairs={{0,1},{1,0},{2,3},{3,2},{4,5},{5,4},{6,7},{7,6},{8,9},{9,8},{10,11... | collective-permute-start | bytes 1179656 | tf_op jit(solution)/shard_map/ppermute | solution.py:420
  28.2 22.8 %all-to-all-start.1 = ((f32[16,16,512]{2,1,0:T(8,128)}), f32[16,16,512]{2,1,0:T(8,128)S(1)}, u32[]{:S(2)}, u32[]{:S(2)}) async-start(f32[16,16,512]{2,1,0:T(8,128)} %shard_map.112), calls=%async_computation.1 | async-start | bytes 1048576 | tf_op jit(solution)/shard_map/all_to_all | solution.py:423
  35.1 7.9 %collective-permute-start.10 = (bf16[384,512]{1,0:T(8,128)(2,1)S(1)}, bf16[384,512]{1,0:T(8,128)(2,1)S(1)}, u32[]{:S(2)}, u32[]{:S(2)}) collective-permute-start(bf16[384,512]{1,0:T(8,128)(2,1)S(1)} %collective-permute-done.9.refs_2_), channel_id=1, source_target_pairs={{0,1},{1,0},{2,3},{3,2},{4,5},{5,4},{6,7},{7,6},{8,9},{9,8},{10,11... | collective-permute-start | bytes 1179656 | tf_op jit(solution)/shard_map/ppermute | solution.py:420
  35.4 7.6 %collective-permute-start.8 = (bf16[384,512]{1,0:T(8,128)(2,1)S(1)}, bf16[384,512]{1,0:T(8,128)(2,1)S(1)}, u32[]{:S(2)}, u32[]{:S(2)}) collective-permute-start(bf16[384,512]{1,0:T(8,128)(2,1)S(1)} %collective-permute-done.7.refs_0_), channel_id=1, source_target_pairs={{0,1},{1,0},{2,3},{3,2},{4,5},{5,4},{6,7},{7,6},{8,9},{9,8},{10,11... | collective-permute-start | bytes 1179656 | tf_op jit(solution)/shard_map/ppermute | solution.py:420
  35.7 10.1 %collective-permute-start.2 = (bf16[384,512]{1,0:T(8,128)(2,1)S(1)}, bf16[384,512]{1,0:T(8,128)(2,1)S(1)}, u32[]{:S(2)}, u32[]{:S(2)}) collective-permute-start(bf16[384,512]{1,0:T(8,128)(2,1)S(1)} %collective-permute-done.1.refs_0_), channel_id=1, source_target_pairs={{0,1},{1,0},{2,3},{3,2},{4,5},{5,4},{6,7},{7,6},{8,9},{9,8},{10,11... | collective-permute-start | bytes 1179656 | tf_op jit(solution)/shard_map/ppermute | solution.py:420
  35.9 9.9 %collective-permute-start.5 = (bf16[384,512]{1,0:T(8,128)(2,1)S(1)}, bf16[384,512]{1,0:T(8,128)(2,1)S(1)}, u32[]{:S(2)}, u32[]{:S(2)}) collective-permute-start(bf16[384,512]{1,0:T(8,128)(2,1)S(1)} %collective-permute-done.4.refs_1_), channel_id=1, source_target_pairs={{0,1},{1,0},{2,3},{3,2},{4,5},{5,4},{6,7},{7,6},{8,9},{9,8},{10,11... | collective-permute-start | bytes 1179656 | tf_op jit(solution)/shard_map/ppermute | solution.py:420
  44.8 1.0 %copy-start = (f32[4,192,4]{1,2,0:T(4,128)S(1)}, f32[4,192,4]{1,2,0:T(4,128)}, u32[]{:S(2)}) copy-start(f32[4,192,4]{1,2,0:T(4,128)} %param.16) | copy-start | bytes 36868
  51.0 13.6 %all-to-all-start = ((f32[16,16,128]{2,1,0:T(8,128)}), f32[16,16,128]{2,1,0:T(8,128)S(1)}, u32[]{:S(2)}, u32[]{:S(2)}) async-start(f32[16,16,128]{2,1,0:T(8,128)} %get-tuple-element.52), calls=%async_computation | async-start | bytes 262144 | tf_op jit(solution)/shard_map/all_to_all | solution.py:423
  55.7 36.6 %copy-start.2 = (f32[128]{0:T(128)S(1)}, f32[128]{0:T(128)}, u32[]{:S(2)}) copy-start(f32[128]{0:T(128)} %param.17) | copy-start | bytes 1540
  65.6 26.7 %all-to-all-start.2 = ((f32[16,16,128]{2,1,0:T(8,128)}), f32[16,16,128]{2,1,0:T(8,128)S(1)}, u32[]{:S(2)}, u32[]{:S(2)}) async-start(f32[16,16,128]{2,1,0:T(8,128)} %shard_map.114), calls=%async_computation.2 | async-start | bytes 262144 | tf_op jit(solution)/shard_map/all_to_all | solution.py:423
  69.1 7.2 %collective-permute-start.13 = (bf16[4,17,8,128]{3,2,1,0:T(8,128)(2,1)S(1)}, bf16[4,17,8,128]{3,2,1,0:T(8,128)(2,1)S(1)}, u32[]{:S(2)}, u32[]{:S(2)}) collective-permute-start(bf16[4,17,8,128]{3,2,1,0:T(8,128)(2,1)S(1)} %get-tuple-element.45), channel_id=1, source_target_pairs={{0,8},{8,0},{16,24},{24,16},{32,40},{40,32},{48,56},{56,48},{64,72... | collective-permute-start | bytes 417800 | tf_op jit(solution)/shard_map/ppermute | solution.py:493
  70.9 8.7 %collective-permute-start.14 = (bf16[4,17,8,128]{3,2,1,0:T(8,128)(2,1)S(1)}, bf16[4,17,8,128]{3,2,1,0:T(8,128)(2,1)S(1)}, u32[]{:S(2)}, u32[]{:S(2)}) collective-permute-start(bf16[4,17,8,128]{3,2,1,0:T(8,128)(2,1)S(1)} %get-tuple-element.46), channel_id=1, source_target_pairs={{0,16},{8,24},{16,0},{24,8},{32,48},{40,56},{48,32},{56,40},{64,80... | collective-permute-start | bytes 417800 | tf_op jit(solution)/shard_map/ppermute | solution.py:493
  73.6 7.5 %collective-permute-start.15 = (bf16[4,17,8,128]{3,2,1,0:T(8,128)(2,1)S(1)}, bf16[4,17,8,128]{3,2,1,0:T(8,128)(2,1)S(1)}, u32[]{:S(2)}, u32[]{:S(2)}) collective-permute-start(bf16[4,17,8,128]{3,2,1,0:T(8,128)(2,1)S(1)} %get-tuple-element.47), channel_id=1, source_target_pairs={{0,24},{8,16},{16,8},{24,0},{32,56},{40,48},{48,40},{56,32},{64,88... | collective-permute-start | bytes 417800 | tf_op jit(solution)/shard_map/ppermute | solution.py:493
  82.0 4.5 %collective-permute-start.16 = (bf16[17,8,128]{2,1,0:T(8,128)(2,1)S(1)}, bf16[17,8,128]{2,1,0:T(8,128)(2,1)S(1)}, u32[]{:S(2)}, u32[]{:S(2)}) collective-permute-start(bf16[17,8,128]{2,1,0:T(8,128)(2,1)S(1)} %get-tuple-element.49), channel_id=1, source_target_pairs={{0,32},{8,40},{16,48},{24,56},{32,0},{40,8},{48,16},{56,24},{64,96... | collective-permute-start | bytes 104456 | tf_op jit(solution)/shard_map/ppermute | solution.py:501
  83.5 5.2 %collective-permute-start.17 = (bf16[17,8,128]{2,1,0:T(8,128)(2,1)S(1)}, bf16[17,8,128]{2,1,0:T(8,128)(2,1)S(1)}, u32[]{:S(2)}, u32[]{:S(2)}) collective-permute-start(bf16[17,8,128]{2,1,0:T(8,128)(2,1)S(1)} %get-tuple-element.50), channel_id=1, source_target_pairs={{0,64},{8,72},{16,80},{24,88},{32,96},{40,104},{48,112},{56,120},{... | collective-permute-start | bytes 104456 | tf_op jit(solution)/shard_map/ppermute | solution.py:501
  85.7 5.7 %collective-permute-start.18 = (bf16[17,8,128]{2,1,0:T(8,128)(2,1)S(1)}, bf16[17,8,128]{2,1,0:T(8,128)(2,1)S(1)}, u32[]{:S(2)}, u32[]{:S(2)}) collective-permute-start(bf16[17,8,128]{2,1,0:T(8,128)(2,1)S(1)} %get-tuple-element.51), channel_id=1, source_target_pairs={{0,96},{8,104},{16,112},{24,120},{32,64},{40,72},{48,80},{56,88},{... | collective-permute-start | bytes 104456 | tf_op jit(solution)/shard_map/ppermute | solution.py:501
  (1 other events, 1.0 us)

commit v9 on v8

--- a/solution.py
+++ b/solution.py
@@ -307,18 +307,6 @@
     )
 
 
-def far_kernel(*refs):
-    tiles, cache_ref = refs[:-1], refs[-1]
-    sums, _ = joined(tiles, lax.axis_index("sp") // NEAR)
-    for j, part in enumerate(sums):
-        cache_ref[j] = part.astype(BF)
-
-
-def join_far(tiles):
-    tile_count, rows, lanes = tiles[0].shape
-    return in_vmem(far_kernel, pltpu.VMEM((tile_count - 1, rows, lanes), BF), *tiles)
-
-
 def read_kernel(totals_ref, state_ref, query_ref, keys_ref, out_ref):
     me = lax.axis_index("sp")
     after = sum(
@@ -340,7 +328,13 @@
     return in_vmem(read_kernel, jax.ShapeDtypeStruct(totals.shape, F32), totals, state, query, keys)
 
 
-def finish_kernel(got_ref, query_ref, keys_ref, value_ref, norm_ref, gate_ref, out_ref):
+def finish_kernel(
+    got_ref, query_ref, keys_ref, value_ref, norm_ref, gate_ref, *refs
+):
+    *tiles, cache_ref, out_ref = refs
+    sums, _ = joined(tiles, lax.axis_index("sp") // NEAR)
+    for j, part in enumerate(sums):
+        cache_ref[j] = part.astype(BF)
     heads = out_ref.shape[1] // got_ref.shape[2]
     head_dim = got_ref.shape[2]
     shared = jnp.sum(query_ref[...] * keys_ref[...], axis=1, keepdims=True)
@@ -503,20 +497,23 @@
     parts = [parts[0], *(along_y(step) for step in range(1, NEAR))]
     parts = join_near(parts)
     parts = [parts[0], *(along_z(step) for step in range(1, planes))]
-    cache = join_far(parts)
 
     totals = exchange(totals)
     read = read_parts(totals, state, query_new, keys_new)
     got = exchange(read)
-    first_read = in_vmem(
+    cache, first_read = in_vmem(
         finish_kernel,
-        jax.ShapeDtypeStruct((seqs, channels), BF),
+        [
+            jax.ShapeDtypeStruct((pairs, row_count, head_dim), BF),
+            jax.ShapeDtypeStruct((seqs, channels), BF),
+        ],
         got,
         query_new,
         keys_new,
         value_new,
         read_norm_scale.reshape(1, head_dim),
         gate_new,
+        *parts,
     )
     return cache.reshape(seqs, heads, row_count, head_dim), first_read
 

time: 93.5 us -> 92.7 us (level)
    pallas_call x11 -> x10, Pallas kernels: 15.7 us -> 15.6 us  [in_vmem(): pl.pallas_call(kernel, in_specs=in_specs or [VMEM] * len(arrays), out_spe...]
  transfers between devices with their start and end apart: 22 -> 22, of which waited for: 10 -> 10; matrix products, arithmetic and copies ran while one was open for 1% -> 0% of each run, Pallas kernels for 20% -> 20%
where the time goes in v9:
time: 92.7 us; the launch traced here: 92.3 us
  starting transfers between devices  35.8 us (39%)
  waiting for transfers between devices  35.1 us (38%)
  Pallas kernels  20.6 us (22%)
    pallas_call x10, Pallas kernels, in_vmem(): pl.pallas_call(kernel, in_specs=in_specs or [VMEM] * len(arrays), out_spe...  15.6 us
    all_to_all x3, starting transfers between devices, exchange(): return lax.all_to_all(x, 'sp', 0, 0, tiled=True)  15.2 us
    ppermute x6, waiting for transfers between devices, shifted(): return lax.ppermute(x, 'tp', pairs)  13.8 us
    ppermute x6, starting transfers between devices, shifted(): return lax.ppermute(x, 'tp', pairs)  10.1 us
    all_to_all x3, waiting for transfers between devices, exchange(): return lax.all_to_all(x, 'sp', 0, 0, tiled=True)  9.14 us
    ppermute x3, waiting for transfers between devices, along_y(): return lax.ppermute(parts[step], 'sp', pairs)  7.2 us
    ppermute x3, waiting for transfers between devices, along_z(): return lax.ppermute(parts[step], 'sp', pairs)  4.9 us
    ppermute x3, starting transfers between devices, along_y(): return lax.ppermute(parts[step], 'sp', pairs)  4.79 us
  transfers between devices with their start and end apart: 22, of which 10 were waited for; matrix products, arithmetic and copies ran while one was open for 0% of the time, Pallas kernels for 20%

profile of v9, /device:TPU:2, one launch (start us, length us, event | category | flops | bytes accessed | tf_op | source)
XLA Modules:
  0.0 92.3 jit_solution(3539337908736070563)
XLA Ops:
  1.9 1.6 %collective-permute-start = (bf16[384,512]{1,0:T(8,128)(2,1)S(1)}, bf16[384,512]{1,0:T(8,128)(2,1)S(1)}, u32[]{:S(2)}, u32[]{:S(2)}) collective-permute-start(bf16[384,512]{1,0:T(8,128)(2,1)S(1)} %bitcast.13), channel_id=1, source_target_pairs={{0,2},{1,3},{2,4},{3,5},{4,6},{5,7},{6,0},{7,1},{8,10},{9,11},{10,... | collective-permute-start | bytes 1179656 | tf_op jit(solution)/shard_map/ppermute | solution.py:411
  5.5 2.0 %collective-permute-start.7 = (bf16[384,512]{1,0:T(8,128)(2,1)S(1)}, bf16[384,512]{1,0:T(8,128)(2,1)S(1)}, u32[]{:S(2)}, u32[]{:S(2)}) collective-permute-start(bf16[384,512]{1,0:T(8,128)(2,1)S(1)} %bitcast.14), channel_id=1, source_target_pairs={{0,6},{1,7},{2,0},{3,1},{4,2},{5,3},{6,4},{7,5},{8,14},{9,15},{10,... | collective-permute-start | bytes 1179656 | tf_op jit(solution)/shard_map/ppermute | solution.py:411
  7.4 6.7 %collective-permute-done.refs_0_ = bf16[384,512]{1,0:T(8,128)(2,1)S(1)} collective-permute-done((bf16[384,512]{1,0:T(8,128)(2,1)S(1)}, bf16[384,512]{1,0:T(8,128)(2,1)S(1)}, u32[]{:S(2)}, u32[]{:S(2)}) %collective-permute-start) | collective-permute-done | bytes 393248 | tf_op jit(solution)/shard_map/ppermute | solution.py:411
  16.8 5.8 %collective-permute-done.9.refs_2_ = bf16[384,512]{1,0:T(8,128)(2,1)S(1)} collective-permute-done((bf16[384,512]{1,0:T(8,128)(2,1)S(1)}, bf16[384,512]{1,0:T(8,128)(2,1)S(1)}, u32[]{:S(2)}, u32[]{:S(2)}) %collective-permute-start.9) | collective-permute-done | bytes 393248 | tf_op jit(solution)/shard_map/ppermute | solution.py:411
  22.6 3.2 %collective-permute-start.4 = (bf16[384,512]{1,0:T(8,128)(2,1)S(1)}, bf16[384,512]{1,0:T(8,128)(2,1)S(1)}, u32[]{:S(2)}, u32[]{:S(2)}) collective-permute-start(bf16[384,512]{1,0:T(8,128)(2,1)S(1)} %collective-permute-done.3.refs_2_), channel_id=1, source_target_pairs={{0,6},{1,7},{2,0},{3,1},{4,2},{5,3},{6,4},{7,5},{8,14},{9,15},{10,... | collective-permute-start | bytes 1179656 | tf_op jit(solution)/shard_map/ppermute | solution.py:411
  25.8 2.3 %shard_map.110 = f32[16,16,512]{2,1,0:T(8,128)} custom-call(bf16[4,256]{1,0:T(4,128)(2,1)} %x_ref.1, bf16[256,512]{1,0:T(8,128)(2,1)} %q_hbm.1, bf16[256,512]{1,0:T(8,128)(2,1)} %g_hbm.1, bf16[4096,512]{1,0:T(8,128)(2,1)} %f_hbm.1, bf16[4096,512]{1,0:T(8,128)(2,1)} %v_hbm.1), custom_call_target="tpu_custom_call" | custom-call | tf_op jit(solution)/shard_map/pallas_call | solution.py:28
  28.1 6.9 %all-to-all-start.1 = ((f32[16,16,512]{2,1,0:T(8,128)}), f32[16,16,512]{2,1,0:T(8,128)S(1)}, u32[]{:S(2)}, u32[]{:S(2)}) async-start(f32[16,16,512]{2,1,0:T(8,128)} %shard_map.110), calls=%async_computation.1 | async-start | bytes 1048576 | tf_op jit(solution)/shard_map/all_to_all | solution.py:417
  36.2 3.9 %load.1 = (bf16[4096,512]{1,0:T(8,128)(2,1)S(1)}, bf16[4096,512]{1,0:T(8,128)(2,1)S(1)}, f32[768,512]{1,0:T(8,128)S(1)}, f32[768,512]{1,0:T(8,128)S(1)}) custom-call(bf16[768,512]{1,0:T(8,128)(2,1)} %bitcast.18, bf16[768,512]{1,0:T(8,128)(2,1)} %collective-permute-done.6.other_hbm, bf16[4096,512]{1,0:T(8,128)(2,1)} %f_hbm.1, bf16[4096,512]{1,0:T(8,128)(2,1)} %v_hbm.1), custom_call_target="tpu_custom_call" | custom-call | tf_op jit(solution)/shard_map/load/pallas_call | solution.py:133
  40.2 2.8 %shard_map.105 = (f32[768,512]{1,0:T(8,128)S(1)}, f32[768,512]{1,0:T(8,128)S(1)}) custom-call(bf16[384,512]{1,0:T(8,128)(2,1)S(1)} %collective-permute-done.refs_0_, bf16[384,512]{1,0:T(8,128)(2,1)S(1)} %collective-permute-done.11.refs_1_, bf16[384,512]{1,0:T(8,128)(2,1)S(1)} %collective-permute-done.3.refs_2_, ...), custom_call_target="tpu_custom_call" | custom-call | flops 1610612736 | tf_op jit(solution)/shard_map/pallas_call | solution.py:28
  43.0 1.8 %shard_map.106 = (f32[768,512]{1,0:T(8,128)S(1)}, f32[768,512]{1,0:T(8,128)S(1)}) custom-call(bf16[384,512]{1,0:T(8,128)(2,1)S(1)} %collective-permute-done.7.refs_0_, bf16[384,512]{1,0:T(8,128)(2,1)S(1)} %collective-permute-done.8.refs_1_, bf16[384,512]{1,0:T(8,128)(2,1)S(1)} %collective-permute-done.9.refs_2_, ...), custom_call_target="tpu_custom_call" | custom-call | flops 1610612736 | tf_op jit(solution)/shard_map/pallas_call | solution.py:28
  45.9 1.9 %shard_map.108 = (bf16[768,512]{1,0:T(8,128)(2,1)S(1)}, bf16[768,512]{1,0:T(8,128)(2,1)S(1)}, f32[16,16,128]{2,1,0:T(8,128)}) custom-call(bf16[384,512]{1,0:T(8,128)(2,1)S(1)} %collective-permute-done.2.refs_0_, bf16[384,512]{1,0:T(8,128)(2,1)S(1)} %collective-permute-done.5.refs_1_, bf16[4096,512]{1,0:T(8,128)(2,1)S(1)} %get-tuple-element.34.refs_4_.refs_2_, ...), custom_call_target="tpu_custom_call" | custom-call | flops 2415919104 | tf_op jit(solution)/shard_map/pallas_call | solution.py:28
  47.8 3.2 %all-to-all-done.1.got_ref = f32[16,16,512]{2,1,0:T(8,128)S(1)} async-done(((f32[16,16,512]{2,1,0:T(8,128)}), f32[16,16,512]{2,1,0:T(8,128)S(1)}, u32[]{:S(2)}, u32[]{:S(2)}) %all-to-all-start.1) | async-done | bytes 524320 | tf_op jit(solution)/shard_map/all_to_all | solution.py:417
  50.9 4.7 %all-to-all-start = ((f32[16,16,128]{2,1,0:T(8,128)}), f32[16,16,128]{2,1,0:T(8,128)S(1)}, u32[]{:S(2)}, u32[]{:S(2)}) async-start(f32[16,16,128]{2,1,0:T(8,128)} %get-tuple-element.44), calls=%async_computation | async-start | bytes 262144 | tf_op jit(solution)/shard_map/all_to_all | solution.py:417
  55.7 2.9 %shard_map.109 = (bf16[4,17,8,128]{3,2,1,0:T(8,128)(2,1)S(1)}, bf16[4,17,8,128]{3,2,1,0:T(8,128)(2,1)S(1)}, bf16[4,17,8,128]{3,2,1,0:T(8,128)(2,1)S(1)}, bf16[4,...) custom-call(bf16[768,512]{1,0:T(8,128)(2,1)S(1)} %get-tuple-element.45.forget_ref, ...), custom_call_target="tpu_custom_call" | custom-call | flops 201326592 | tf_op jit(solution)/shard_map/pallas_call | solution.py:28
  58.6 6.0 %all-to-all-done.totals_ref = f32[16,16,128]{2,1,0:T(8,128)S(1)} async-done(((f32[16,16,128]{2,1,0:T(8,128)}), f32[16,16,128]{2,1,0:T(8,128)S(1)}, u32[]{:S(2)}, u32[]{:S(2)}) %all-to-all-start) | async-done | bytes 131104 | tf_op jit(solution)/shard_map/all_to_all | solution.py:417
  65.5 3.5 %all-to-all-start.2 = ((f32[16,16,128]{2,1,0:T(8,128)}), f32[16,16,128]{2,1,0:T(8,128)S(1)}, u32[]{:S(2)}, u32[]{:S(2)}) async-start(f32[16,16,128]{2,1,0:T(8,128)} %shard_map.112), calls=%async_computation.2 | async-start | bytes 262144 | tf_op jit(solution)/shard_map/all_to_all | solution.py:417
  69.1 1.8 %collective-permute-start.13 = (bf16[4,17,8,128]{3,2,1,0:T(8,128)(2,1)S(1)}, bf16[4,17,8,128]{3,2,1,0:T(8,128)(2,1)S(1)}, u32[]{:S(2)}, u32[]{:S(2)}) collective-permute-start(bf16[4,17,8,128]{3,2,1,0:T(8,128)(2,1)S(1)} %get-tuple-element.53), channel_id=1, source_target_pairs={{0,8},{8,0},{16,24},{24,16},{32,40},{40,32},{48,56},{56,48},{64,72... | collective-permute-start | bytes 417800 | tf_op jit(solution)/shard_map/ppermute | solution.py:487
  70.9 2.7 %collective-permute-start.14 = (bf16[4,17,8,128]{3,2,1,0:T(8,128)(2,1)S(1)}, bf16[4,17,8,128]{3,2,1,0:T(8,128)(2,1)S(1)}, u32[]{:S(2)}, u32[]{:S(2)}) collective-permute-start(bf16[4,17,8,128]{3,2,1,0:T(8,128)(2,1)S(1)} %get-tuple-element.54), channel_id=1, source_target_pairs={{0,16},{8,24},{16,0},{24,8},{32,48},{40,56},{48,32},{56,40},{64,80... | collective-permute-start | bytes 417800 | tf_op jit(solution)/shard_map/ppermute | solution.py:487
  73.8 2.4 %collective-permute-done.13.refs_1_ = bf16[4,17,8,128]{3,2,1,0:T(8,128)(2,1)S(1)} collective-permute-done((bf16[4,17,8,128]{3,2,1,0:T(8,128)(2,1)S(1)}, bf16[4,17,8,128]{3,2,1,0:T(8,128)(2,1)S(1)}, u32[]{:S(2)}, u32[]{:S(2)}) %collective-permute-start.13) | collective-permute-done | bytes 139296 | tf_op jit(solution)/shard_map/ppermute | solution.py:487
  76.3 3.3 %collective-permute-done.14.refs_2_ = bf16[4,17,8,128]{3,2,1,0:T(8,128)(2,1)S(1)} collective-permute-done((bf16[4,17,8,128]{3,2,1,0:T(8,128)(2,1)S(1)}, bf16[4,17,8,128]{3,2,1,0:T(8,128)(2,1)S(1)}, u32[]{:S(2)}, u32[]{:S(2)}) %collective-permute-start.14) | collective-permute-done | bytes 139296 | tf_op jit(solution)/shard_map/ppermute | solution.py:487
  79.6 1.5 %collective-permute-done.15.refs_3_ = bf16[4,17,8,128]{3,2,1,0:T(8,128)(2,1)S(1)} collective-permute-done((bf16[4,17,8,128]{3,2,1,0:T(8,128)(2,1)S(1)}, bf16[4,17,8,128]{3,2,1,0:T(8,128)(2,1)S(1)}, u32[]{:S(2)}, u32[]{:S(2)}) %collective-permute-start.15) | collective-permute-done | bytes 139296 | tf_op jit(solution)/shard_map/ppermute | solution.py:487
  83.5 2.2 %collective-permute-start.17 = (bf16[17,8,128]{2,1,0:T(8,128)(2,1)S(1)}, bf16[17,8,128]{2,1,0:T(8,128)(2,1)S(1)}, u32[]{:S(2)}, u32[]{:S(2)}) collective-permute-start(bf16[17,8,128]{2,1,0:T(8,128)(2,1)S(1)} %get-tuple-element.58), channel_id=1, source_target_pairs={{0,64},{8,72},{16,80},{24,88},{32,96},{40,104},{48,112},{56,120},{... | collective-permute-start | bytes 104456 | tf_op jit(solution)/shard_map/ppermute | solution.py:495
  86.5 2.2 %collective-permute-done.17.refs_2_ = bf16[17,8,128]{2,1,0:T(8,128)(2,1)S(1)} collective-permute-done((bf16[17,8,128]{2,1,0:T(8,128)(2,1)S(1)}, bf16[17,8,128]{2,1,0:T(8,128)(2,1)S(1)}, u32[]{:S(2)}, u32[]{:S(2)}) %collective-permute-start.17) | collective-permute-done | bytes 34848 | tf_op jit(solution)/shard_map/ppermute | solution.py:495
  88.7 2.7 %collective-permute-done.18.refs_3_ = bf16[17,8,128]{2,1,0:T(8,128)(2,1)S(1)} collective-permute-done((bf16[17,8,128]{2,1,0:T(8,128)(2,1)S(1)}, bf16[17,8,128]{2,1,0:T(8,128)(2,1)S(1)}, u32[]{:S(2)}, u32[]{:S(2)}) %collective-permute-start.18) | collective-permute-done | bytes 34848 | tf_op jit(solution)/shard_map/ppermute | solution.py:495
  (38 shorter events, 13.5 us)
Async XLA Ops:
  0.6 34.5 %collective-permute-start.6 = (bf16[768,512]{1,0:T(8,128)(2,1)}, bf16[768,512]{1,0:T(8,128)(2,1)}, u32[]{:S(2)}, u32[]{:S(2)}) collective-permute-start(bf16[768,512]{1,0:T(8,128)(2,1)} %bitcast.17), channel_id=1, source_target_pairs={{0,1},{1,0},{2,3},{3,2},{4,5},{5,4},{6,7},{7,6},{8,9},{9,8},{10,11... | collective-permute-start | bytes 2359304 | tf_op jit(solution)/shard_map/ppermute | solution.py:414
  1.9 12.3 %collective-permute-start = (bf16[384,512]{1,0:T(8,128)(2,1)S(1)}, bf16[384,512]{1,0:T(8,128)(2,1)S(1)}, u32[]{:S(2)}, u32[]{:S(2)}) collective-permute-start(bf16[384,512]{1,0:T(8,128)(2,1)S(1)} %bitcast.13), channel_id=1, source_target_pairs={{0,2},{1,3},{2,4},{3,5},{4,6},{5,7},{6,0},{7,1},{8,10},{9,11},{10,... | collective-permute-start | bytes 1179656 | tf_op jit(solution)/shard_map/ppermute | solution.py:411
  3.4 12.0 %collective-permute-start.3 = (bf16[384,512]{1,0:T(8,128)(2,1)S(1)}, bf16[384,512]{1,0:T(8,128)(2,1)S(1)}, u32[]{:S(2)}, u32[]{:S(2)}) collective-permute-start(bf16[384,512]{1,0:T(8,128)(2,1)S(1)} %bitcast.15), channel_id=1, source_target_pairs={{0,6},{1,7},{2,0},{3,1},{4,2},{5,3},{6,4},{7,5},{8,14},{9,15},{10,... | collective-permute-start | bytes 1179656 | tf_op jit(solution)/shard_map/ppermute | solution.py:411
  4.3 18.3 %collective-permute-start.9 = (bf16[384,512]{1,0:T(8,128)(2,1)S(1)}, bf16[384,512]{1,0:T(8,128)(2,1)S(1)}, u32[]{:S(2)}, u32[]{:S(2)}) collective-permute-start(bf16[384,512]{1,0:T(8,128)(2,1)S(1)} %bitcast.16), channel_id=1, source_target_pairs={{0,2},{1,3},{2,4},{3,5},{4,6},{5,7},{6,0},{7,1},{8,10},{9,11},{10,... | collective-permute-start | bytes 1179656 | tf_op jit(solution)/shard_map/ppermute | solution.py:411
  5.5 20.4 %collective-permute-start.7 = (bf16[384,512]{1,0:T(8,128)(2,1)S(1)}, bf16[384,512]{1,0:T(8,128)(2,1)S(1)}, u32[]{:S(2)}, u32[]{:S(2)}) collective-permute-start(bf16[384,512]{1,0:T(8,128)(2,1)S(1)} %bitcast.14), channel_id=1, source_target_pairs={{0,6},{1,7},{2,0},{3,1},{4,2},{5,3},{6,4},{7,5},{8,14},{9,15},{10,... | collective-permute-start | bytes 1179656 | tf_op jit(solution)/shard_map/ppermute | solution.py:411
  14.2 21.2 %collective-permute-start.11 = (bf16[384,512]{1,0:T(8,128)(2,1)S(1)}, bf16[384,512]{1,0:T(8,128)(2,1)S(1)}, u32[]{:S(2)}, u32[]{:S(2)}) collective-permute-start(bf16[384,512]{1,0:T(8,128)(2,1)S(1)} %collective-permute-done.refs_0_), channel_id=1, source_target_pairs={{0,1},{1,0},{2,3},{3,2},{4,5},{5,4},{6,7},{7,6},{8,9},{9,8},{10,11... | collective-permute-start | bytes 1179656 | tf_op jit(solution)/shard_map/ppermute | solution.py:414
  15.4 20.3 %collective-permute-start.1 = (bf16[384,512]{1,0:T(8,128)(2,1)S(1)}, bf16[384,512]{1,0:T(8,128)(2,1)S(1)}, u32[]{:S(2)}, u32[]{:S(2)}) collective-permute-start(bf16[384,512]{1,0:T(8,128)(2,1)S(1)} %collective-permute-done.refs_0_), channel_id=1, source_target_pairs={{0,2},{1,3},{2,4},{3,5},{4,6},{5,7},{6,0},{7,1},{8,10},{9,11},{10,... | collective-permute-start | bytes 1179656 | tf_op jit(solution)/shard_map/ppermute | solution.py:411
  22.6 13.3 %collective-permute-start.4 = (bf16[384,512]{1,0:T(8,128)(2,1)S(1)}, bf16[384,512]{1,0:T(8,128)(2,1)S(1)}, u32[]{:S(2)}, u32[]{:S(2)}) collective-permute-start(bf16[384,512]{1,0:T(8,128)(2,1)S(1)} %collective-permute-done.3.refs_2_), channel_id=1, source_target_pairs={{0,6},{1,7},{2,0},{3,1},{4,2},{5,3},{6,4},{7,5},{8,14},{9,15},{10,... | collective-permute-start | bytes 1179656 | tf_op jit(solution)/shard_map/ppermute | solution.py:411
  25.8 14.3 %collective-permute-start.12 = (bf16[384,512]{1,0:T(8,128)(2,1)S(1)}, bf16[384,512]{1,0:T(8,128)(2,1)}, u32[]{:S(2)}, u32[]{:S(2)}) collective-permute-start(bf16[384,512]{1,0:T(8,128)(2,1)S(1)} %collective-permute-done.3.refs_2_), channel_id=1, source_target_pairs={{0,1},{1,0},{2,3},{3,2},{4,5},{5,4},{6,7},{7,6},{8,9},{9,8},{10,11... | collective-permute-start | bytes 1179656 | tf_op jit(solution)/shard_map/ppermute | solution.py:414
  28.1 22.8 %all-to-all-start.1 = ((f32[16,16,512]{2,1,0:T(8,128)}), f32[16,16,512]{2,1,0:T(8,128)S(1)}, u32[]{:S(2)}, u32[]{:S(2)}) async-start(f32[16,16,512]{2,1,0:T(8,128)} %shard_map.110), calls=%async_computation.1 | async-start | bytes 1048576 | tf_op jit(solution)/shard_map/all_to_all | solution.py:417
  35.1 7.9 %collective-permute-start.10 = (bf16[384,512]{1,0:T(8,128)(2,1)S(1)}, bf16[384,512]{1,0:T(8,128)(2,1)S(1)}, u32[]{:S(2)}, u32[]{:S(2)}) collective-permute-start(bf16[384,512]{1,0:T(8,128)(2,1)S(1)} %collective-permute-done.9.refs_2_), channel_id=1, source_target_pairs={{0,1},{1,0},{2,3},{3,2},{4,5},{5,4},{6,7},{7,6},{8,9},{9,8},{10,11... | collective-permute-start | bytes 1179656 | tf_op jit(solution)/shard_map/ppermute | solution.py:414
  35.4 7.6 %collective-permute-start.8 = (bf16[384,512]{1,0:T(8,128)(2,1)S(1)}, bf16[384,512]{1,0:T(8,128)(2,1)S(1)}, u32[]{:S(2)}, u32[]{:S(2)}) collective-permute-start(bf16[384,512]{1,0:T(8,128)(2,1)S(1)} %collective-permute-done.7.refs_0_), channel_id=1, source_target_pairs={{0,1},{1,0},{2,3},{3,2},{4,5},{5,4},{6,7},{7,6},{8,9},{9,8},{10,11... | collective-permute-start | bytes 1179656 | tf_op jit(solution)/shard_map/ppermute | solution.py:414
  35.7 10.1 %collective-permute-start.2 = (bf16[384,512]{1,0:T(8,128)(2,1)S(1)}, bf16[384,512]{1,0:T(8,128)(2,1)S(1)}, u32[]{:S(2)}, u32[]{:S(2)}) collective-permute-start(bf16[384,512]{1,0:T(8,128)(2,1)S(1)} %collective-permute-done.1.refs_0_), channel_id=1, source_target_pairs={{0,1},{1,0},{2,3},{3,2},{4,5},{5,4},{6,7},{7,6},{8,9},{9,8},{10,11... | collective-permute-start | bytes 1179656 | tf_op jit(solution)/shard_map/ppermute | solution.py:414
  35.9 9.9 %collective-permute-start.5 = (bf16[384,512]{1,0:T(8,128)(2,1)S(1)}, bf16[384,512]{1,0:T(8,128)(2,1)S(1)}, u32[]{:S(2)}, u32[]{:S(2)}) collective-permute-start(bf16[384,512]{1,0:T(8,128)(2,1)S(1)} %collective-permute-done.4.refs_1_), channel_id=1, source_target_pairs={{0,1},{1,0},{2,3},{3,2},{4,5},{5,4},{6,7},{7,6},{8,9},{9,8},{10,11... | collective-permute-start | bytes 1179656 | tf_op jit(solution)/shard_map/ppermute | solution.py:414
  44.8 1.0 %copy-start = (f32[4,192,4]{1,2,0:T(4,128)S(1)}, f32[4,192,4]{1,2,0:T(4,128)}, u32[]{:S(2)}) copy-start(f32[4,192,4]{1,2,0:T(4,128)} %param.16) | copy-start | bytes 36868
  50.9 13.6 %all-to-all-start = ((f32[16,16,128]{2,1,0:T(8,128)}), f32[16,16,128]{2,1,0:T(8,128)S(1)}, u32[]{:S(2)}, u32[]{:S(2)}) async-start(f32[16,16,128]{2,1,0:T(8,128)} %get-tuple-element.44), calls=%async_computation | async-start | bytes 262144 | tf_op jit(solution)/shard_map/all_to_all | solution.py:417
  55.7 35.7 %copy-start.2 = (f32[128]{0:T(128)S(1)}, f32[128]{0:T(128)}, u32[]{:S(2)}) copy-start(f32[128]{0:T(128)} %param.17) | copy-start | bytes 1540
  65.5 25.8 %all-to-all-start.2 = ((f32[16,16,128]{2,1,0:T(8,128)}), f32[16,16,128]{2,1,0:T(8,128)S(1)}, u32[]{:S(2)}, u32[]{:S(2)}) async-start(f32[16,16,128]{2,1,0:T(8,128)} %shard_map.112), calls=%async_computation.2 | async-start | bytes 262144 | tf_op jit(solution)/shard_map/all_to_all | solution.py:417
  69.1 7.2 %collective-permute-start.13 = (bf16[4,17,8,128]{3,2,1,0:T(8,128)(2,1)S(1)}, bf16[4,17,8,128]{3,2,1,0:T(8,128)(2,1)S(1)}, u32[]{:S(2)}, u32[]{:S(2)}) collective-permute-start(bf16[4,17,8,128]{3,2,1,0:T(8,128)(2,1)S(1)} %get-tuple-element.53), channel_id=1, source_target_pairs={{0,8},{8,0},{16,24},{24,16},{32,40},{40,32},{48,56},{56,48},{64,72... | collective-permute-start | bytes 417800 | tf_op jit(solution)/shard_map/ppermute | solution.py:487
  70.9 8.7 %collective-permute-start.14 = (bf16[4,17,8,128]{3,2,1,0:T(8,128)(2,1)S(1)}, bf16[4,17,8,128]{3,2,1,0:T(8,128)(2,1)S(1)}, u32[]{:S(2)}, u32[]{:S(2)}) collective-permute-start(bf16[4,17,8,128]{3,2,1,0:T(8,128)(2,1)S(1)} %get-tuple-element.54), channel_id=1, source_target_pairs={{0,16},{8,24},{16,0},{24,8},{32,48},{40,56},{48,32},{56,40},{64,80... | collective-permute-start | bytes 417800 | tf_op jit(solution)/shard_map/ppermute | solution.py:487
  73.6 7.5 %collective-permute-start.15 = (bf16[4,17,8,128]{3,2,1,0:T(8,128)(2,1)S(1)}, bf16[4,17,8,128]{3,2,1,0:T(8,128)(2,1)S(1)}, u32[]{:S(2)}, u32[]{:S(2)}) collective-permute-start(bf16[4,17,8,128]{3,2,1,0:T(8,128)(2,1)S(1)} %get-tuple-element.55), channel_id=1, source_target_pairs={{0,24},{8,16},{16,8},{24,0},{32,56},{40,48},{48,40},{56,32},{64,88... | collective-permute-start | bytes 417800 | tf_op jit(solution)/shard_map/ppermute | solution.py:487
  82.0 4.5 %collective-permute-start.16 = (bf16[17,8,128]{2,1,0:T(8,128)(2,1)S(1)}, bf16[17,8,128]{2,1,0:T(8,128)(2,1)S(1)}, u32[]{:S(2)}, u32[]{:S(2)}) collective-permute-start(bf16[17,8,128]{2,1,0:T(8,128)(2,1)S(1)} %get-tuple-element.57), channel_id=1, source_target_pairs={{0,32},{8,40},{16,48},{24,56},{32,0},{40,8},{48,16},{56,24},{64,96... | collective-permute-start | bytes 104456 | tf_op jit(solution)/shard_map/ppermute | solution.py:495
  83.5 5.2 %collective-permute-start.17 = (bf16[17,8,128]{2,1,0:T(8,128)(2,1)S(1)}, bf16[17,8,128]{2,1,0:T(8,128)(2,1)S(1)}, u32[]{:S(2)}, u32[]{:S(2)}) collective-permute-start(bf16[17,8,128]{2,1,0:T(8,128)(2,1)S(1)} %get-tuple-element.58), channel_id=1, source_target_pairs={{0,64},{8,72},{16,80},{24,88},{32,96},{40,104},{48,112},{56,120},{... | collective-permute-start | bytes 104456 | tf_op jit(solution)/shard_map/ppermute | solution.py:495
  85.7 5.7 %collective-permute-start.18 = (bf16[17,8,128]{2,1,0:T(8,128)(2,1)S(1)}, bf16[17,8,128]{2,1,0:T(8,128)(2,1)S(1)}, u32[]{:S(2)}, u32[]{:S(2)}) collective-permute-start(bf16[17,8,128]{2,1,0:T(8,128)(2,1)S(1)} %get-tuple-element.59), channel_id=1, source_target_pairs={{0,96},{8,104},{16,112},{24,120},{32,64},{40,72},{48,80},{56,88},{... | collective-permute-start | bytes 104456 | tf_op jit(solution)/shard_map/ppermute | solution.py:495
  (1 other events, 1.0 us)
